TPU v7x, 32 devices: a whole 2x2x4 slice. The times are simulated.
32 devices in a mesh: grp: 2 (over y), dp: 2 (over x), kv: 4 (over z), tp: 2 (over core).
Axes of the slice: x: 2, y: 2, z: 4, core: 2. Of those that a mesh axis runs over, the one named last changes fastest.
Arguments:
- tokens: bfloat16 [32, 2048], P(('grp', 'dp'), ('kv', 'tp')), parts along dimension 0, may hold values from -24 to 24
- memory: float32 [32, 12, 16384], P(('grp', 'dp', 'kv', 'tp')), parts along dimension 0, may hold values from -3 to 3
- mix_gain: float32 [2048], replicated, may hold values from 0.1 to 1.9
- w_query: bfloat16 [2048, 1536], P(None, ('kv', 'tp')), may hold values from -0.125 to 0.125
- w_key: bfloat16 [2048, 1536], P(None, ('kv', 'tp')), may hold values from -0.125 to 0.125
- w_value: bfloat16 [2048, 1536], P(None, ('kv', 'tp')), may hold values from -0.125 to 0.125
- w_gate: bfloat16 [2048, 1536], P(None, ('kv', 'tp')), may hold values from -0.125 to 0.125
- w_beta: bfloat16 [2048, 12], replicated, may hold values from -0.125 to 0.125
- w_decay: bfloat16 [2048, 12], replicated, may hold values from -0.125 to 0.125
- decay_rate: float32 [12], replicated, may hold values from 0.1 to 3
- decay_bias: float32 [12], replicated, may hold values from -2 to 1
- head_gain: float32 [128], replicated, may hold values from 0.1 to 1.9
- w_out: bfloat16 [1536, 2048], P(None, ('kv', 'tp')), may hold values from -0.15625 to 0.15625
- ffn_gain: float32 [2048], replicated, may hold values from 0.1 to 1.9
- w_up: bfloat16 [2048, 8192], P(None, ('kv', 'tp')), may hold values from -0.125 to 0.125
- w_down: bfloat16 [8192, 2048], P(('kv', 'tp')), may hold values from -0.09375 to 0.09375
Outputs:
- layer_out: bfloat16 [32, 2048], P(('grp', 'dp'), ('kv', 'tp')), parts along dimension 0
- new_memory: float32 [32, 12, 16384], P(('grp', 'dp', 'kv', 'tp')), parts along dimension 0
There are 2 independent parts, one for each index of `grp`. A program takes and returns all parts, laid end to end along the dimension named above; an argument that names none is the same for every part. Nothing has to cross between parts.
All inputs are finite; a program needn't handle non-finite values.
Results may differ from a plain program's by a relative error of at most 0.02.
Values may be sent and summed in bfloat16 or wider, within the bound.
No kernel may reach another device: no remote copies, remote signals or barrier semaphores. Data moves between devices by JAX's collectives and lax.ppermute only.
A program may use at most 64 MiB of HBM per device.

v0:
```python
import functools

import jax
import jax.numpy as jnp
from jax import lax
from jax.experimental import pallas as pl
from jax.experimental.pallas import tpu as pltpu
from jax.sharding import PartitionSpec as P


epsilon = 1e-06
axes = ("kv", "tp")


def by_distance(stack, chip):
    count = stack.shape[0]
    rest = stack.shape[1:]
    bit = 1
    while bit < count:
        split = stack.reshape((count // (2 * bit), 2, bit) + rest)
        flipped = jnp.where((chip & bit) != 0, split[:, ::-1], split)
        stack = flipped.reshape((count,) + rest)
        bit *= 2
    return stack


def far(pieces, chips):
    got = [pieces[0]]
    for d in range(1, chips):
        pairs = [(i, i ^ (2 * d + 1)) for i in range(2 * chips)]
        got.append(lax.ppermute(pieces[d], axes, pairs))
    return got


def near(value):
    return lax.ppermute(value, "tp", [(0, 1), (1, 0)])


def merge(mine, other, chip, core):
    count = mine.shape[0]
    own = (jnp.arange(count) == 0).reshape((count,) + (1,) * (mine.ndim - 1))
    low_is_mine = own == (core == 0)
    low = jnp.where(low_is_mine, mine, other)
    high = jnp.where(low_is_mine, other, mine)
    both = by_distance(jnp.stack([low, high], axis=1), chip)
    return both.reshape((2 * count,) + mine.shape[1:])


def gather(piece, chips, chip, core):
    mine = jnp.stack(far([piece] * chips, chips))
    return merge(mine, near(mine), chip, core)


def gather_features(piece, chips, chip, core):
    parts = gather(piece, chips, chip, core)
    return jnp.concatenate([parts[i] for i in range(2 * chips)], axis=1)


def delta_step(queries, keys_in, values, gates, strength, log_decay, memory, head_gain):
    count = queries.shape[0]
    heads = strength.shape[1]
    size = head_gain.shape[0]
    highest = lax.Precision.HIGHEST
    query_wide = queries.astype(jnp.float32).reshape(count, heads, size)
    key_wide = keys_in.astype(jnp.float32).reshape(count, heads, size)
    value_wide = values.astype(jnp.float32).reshape(count, heads, size)
    gate_wide = gates.astype(jnp.float32).reshape(count, heads, size)
    unit_key = key_wide * lax.rsqrt(jnp.sum(key_wide * key_wide, axis=-1, keepdims=True) + epsilon)
    matrix = memory.reshape(count, heads, size, size)
    recall = jnp.einsum("bhk,bhkv->bhv", unit_key, matrix, precision=highest)
    retain = jnp.exp(log_decay)[:, :, None, None]
    scaled = strength[:, :, None]
    erased = matrix - jnp.einsum("bhk,bhv->bhkv", unit_key, scaled * recall, precision=highest)
    written = jnp.einsum("bhk,bhv->bhkv", unit_key, scaled * value_wide, precision=highest)
    updated = retain * erased + written
    readout = jnp.einsum("bhk,bhkv->bhv", query_wide, updated, precision=highest)
    normed = readout * lax.rsqrt(jnp.mean(readout * readout, axis=-1, keepdims=True) + epsilon)
    normed = normed * head_gain * jax.nn.silu(gate_wide)
    return (
        updated.reshape(count, heads, size * size),
        normed.reshape(count, heads * size).astype(jnp.bfloat16),
    )


def plain_device(
    chips,
    tokens,
    memory,
    mix_gain,
    w_query,
    w_key,
    w_value,
    w_gate,
    w_beta,
    w_decay,
    decay_rate,
    decay_bias,
    head_gain,
    w_out,
    ffn_gain,
    w_up,
    w_down,
):
    rows = tokens.shape[0]
    owned = memory.shape[0]
    width = mix_gain.shape[0]
    chip = lax.axis_index("kv")
    core = lax.axis_index("tp")
    own_start = lax.axis_index(axes) * owned
    wide = tokens.astype(jnp.float32)

    def lifted_of(whole, gain):
        whole_wide = whole.astype(jnp.float32)
        scale = lax.rsqrt(jnp.sum(whole_wide * whole_wide, axis=1) / width + epsilon)
        return (whole_wide * gain).astype(jnp.bfloat16), scale[:, None]

    def project(value, weight):
        return jnp.dot(value, weight, preferred_element_type=jnp.float32)

    lifted_in, scale_in = lifted_of(gather_features(tokens, chips, chip, core), mix_gain)
    sent = jnp.stack(
        [
            (project(lifted_in, weight) * scale_in).astype(jnp.bfloat16)
            for weight in (w_query, w_key, w_value, w_gate)
        ],
        axis=1,
    )
    strength_all = jax.nn.sigmoid(project(lifted_in, w_beta) * scale_in)
    decay_all = -decay_rate * jax.nn.softplus(project(lifted_in, w_decay) * scale_in + decay_bias)
    strength = lax.dynamic_slice_in_dim(strength_all, own_start, owned, 0)
    log_decay = lax.dynamic_slice_in_dim(decay_all, own_start, owned, 0)

    part = sent.shape[2]
    leaving = by_distance(sent.reshape(chips, 2, owned, 4, part), chip)
    mine = jnp.stack(far([leaving[d] for d in range(chips)], chips))
    other = near(mine)
    pick = lambda both: jnp.where(core == 0, both[:, 0], both[:, 1])
    whole = merge(pick(mine), pick(other), chip, core)
    whole = jnp.transpose(whole, (2, 1, 0, 3)).reshape(4, owned, 2 * chips * part)
    updated, mixed = delta_step(
        whole[0], whole[1], whole[2], whole[3], strength, log_decay, memory, head_gain
    )

    mixed_all = gather(mixed, chips, chip, core).reshape(rows, mixed.shape[1])
    middle = (wide + project(mixed_all, w_out)).astype(jnp.bfloat16)
    middle_wide = middle.astype(jnp.float32)
    lifted_mid, scale_mid = lifted_of(gather_features(middle, chips, chip, core), ffn_gain)
    raised = project(lifted_mid, w_up)
    hidden = jnp.square(jax.nn.relu(raised * scale_mid)).astype(jnp.bfloat16)
    terms = project(hidden, w_down).astype(jnp.bfloat16)

    features = tokens.shape[1]
    blocks = jnp.stack([terms[:, i * 2 * features : (i + 1) * 2 * features] for i in range(chips)])
    leaving = by_distance(blocks, chip)
    total = sum(
        (got.astype(jnp.float32) for got in far([leaving[d] for d in range(chips)], chips))
    )
    low, high = total[:, :features], total[:, features:]
    arrived = near(jnp.where(core == 0, high, low))
    down = jnp.where(core == 0, low, high) + arrived
    layer_out = (middle_wide + down).astype(jnp.bfloat16)
    return (layer_out, updated)


def place():
    return lax.axis_index("kv"), lax.axis_index("tp")


def mine_lane(d):
    chip, core = place()
    return 2 * (chip ^ d) + (core if d == 0 else 1 - core)


def other_lane(d):
    chip, core = place()
    return 2 * (chip ^ d) + (1 - core if d == 0 else core)


def span(lane, size):
    return pl.ds(pl.multiple_of(lane * size, size), size)


def dot_rows(left, right):
    return lax.dot_general(left, right, (((1,), (1,)), ((), ())), preferred_element_type=jnp.float32)


def dot(left, right):
    return jnp.dot(left, right, preferred_element_type=jnp.float32)


def call(body, outs, args, scratch=(), work=1e9):
    vmem = pl.BlockSpec(memory_space=pltpu.VMEM)
    return pl.pallas_call(
        body,
        out_shape=[jax.ShapeDtypeStruct(shape, kind) for shape, kind in outs],
        in_specs=[vmem] * len(args),
        out_specs=[vmem] * len(outs),
        scratch_shapes=list(scratch),
        compiler_params=pltpu.CompilerParams(vmem_limit_bytes=16 << 20),
        cost_estimate=pl.CostEstimate(flops=int(work), bytes_accessed=0, transcendentals=0),
    )(*args)


def keep_near(tokens, near_ref):
    near_ref[...] = tokens[...]


def project_piece(piece, lane, gain, weights, lifted, parts):
    size = piece.shape[1]
    wide = piece.astype(jnp.float32)
    ready = (wide * gain[:, span(lane, size)]).astype(jnp.bfloat16)
    lifted[:, span(lane, size)] = ready
    stacked = jnp.concatenate([weight[:, span(lane, size)] for weight in weights], axis=0)
    parts.append((dot_rows(ready, stacked), jnp.sum(wide * wide, axis=1, keepdims=True)))


def project_first(chips, tokens, partner, *refs):
    got, (gain, *rest) = refs[: chips - 1], refs[chips - 1 :]
    weights, (total, squares, lifted) = rest[:4], rest[4:]
    lifted[...] = jnp.zeros_like(lifted)
    parts = []
    project_piece(tokens[...], mine_lane(0), gain, weights, lifted, parts)
    project_piece(partner[...], other_lane(0), gain, weights, lifted, parts)
    for d in range(1, chips):
        project_piece(got[d - 1][...], mine_lane(d), gain, weights, lifted, parts)
    total[...] = sum(part[0] for part in parts)
    squares[...] = jnp.broadcast_to(sum(part[1] for part in parts), squares.shape)


def project_rest(chips, others, before, before_squares, before_lifted, gain, *rest):
    weights, (scale_ref, lifted, *leaving), sent = rest[:4], rest[4:-1], rest[-1]
    lifted[...] = before_lifted[...]
    parts = [(before[...], before_squares[:, :1])]
    for d in range(1, chips):
        project_piece(others[d - 1], other_lane(d), gain, weights, lifted, parts)
    squares = sum(part[1] for part in parts)
    scale = lax.rsqrt(squares / lifted.shape[1] + epsilon)
    total = sum(part[0] for part in parts) * scale
    sent[...] = total.astype(jnp.bfloat16).astype(jnp.float32)
    scale_ref[...] = jnp.broadcast_to(scale, scale_ref.shape)
    chip, _ = place()
    for d in range(chips):
        for c in range(2):
            leaving[d][c : c + 1, :] = sent[pl.ds(2 * (chip ^ d) + c, 1), :]


def column(row, heads):
    there = lax.broadcasted_iota(jnp.int32, (heads, heads), 0)
    here = lax.broadcasted_iota(jnp.int32, (heads, heads), 1)
    return jnp.sum(jnp.where(there == here, row, 0.0), axis=1, keepdims=True)


def own_gates(lifted, scale, w_beta, w_decay, rate, bias, strength, retain):
    heads = w_beta.shape[0]
    lane = mine_lane(0)
    scale_own = scale[pl.ds(lane, 1), :][:, :1]

    def own(weight):
        every = dot_rows(weight[...], lifted[...])
        here = lax.broadcasted_iota(jnp.int32, every.shape, 1) == lane
        return jnp.sum(jnp.where(here, every, 0.0), axis=1, keepdims=True) * scale_own

    value = own(w_decay) + column(bias[...], heads)
    soft = jnp.maximum(value, 0.0) + jnp.log1p(jnp.exp(-jnp.abs(value)))
    decay = jnp.exp(-column(rate[...], heads) * soft)
    beta = 1.0 / (1.0 + jnp.exp(-own(w_beta)))
    strength[...] = jnp.broadcast_to(beta, strength.shape)
    retain[...] = jnp.broadcast_to(decay, retain.shape)


def read_memory(chips, *refs):
    mine, other, strength, retain, memory, head_gain, mixed, unit_ref, write_ref, parts = refs
    heads, size = strength.shape
    chip, core = place()
    part = mine.shape[2] // 4
    across = 2 * part // size
    for there in range(chips):
        d = chip ^ there
        own = mine[d, pl.ds(core, 1), :]
        partner = other[d, pl.ds(core, 1), :]
        straight = (d == 0) == (core == 0)
        low = jnp.where(straight, own, partner)
        high = jnp.where(straight, partner, own)
        for t in range(4):
            cut = slice(t * part, (t + 1) * part)
            pair = jnp.concatenate([low[:, cut], high[:, cut]], axis=1)
            for i in range(across):
                h = there * across + i
                parts[t, h : h + 1, :] = pair[:, i * size : (i + 1) * size]
    query, key, value, gate = parts[0], parts[1], parts[2], parts[3]
    unit = key * lax.rsqrt(jnp.sum(key * key, axis=1, keepdims=True) + epsilon)
    padded = -(-heads // 8) * 8
    pad = [jnp.zeros((padded - heads, size), jnp.float32)] if padded > heads else []
    rest = jnp.zeros((size - 2 * padded, size), jnp.float32)
    turned = jnp.concatenate([unit, *pad, query, *pad, rest], axis=0).T
    recalls, reads = [], []
    for h in range(heads):
        matrix = memory[h]
        recalls.append(jnp.sum(matrix * turned[:, h : h + 1], axis=0, keepdims=True))
        at = padded + h
        reads.append(jnp.sum(matrix * turned[:, at : at + 1], axis=0, keepdims=True))
    recall = jnp.concatenate(recalls, axis=0)
    read = jnp.concatenate(reads, axis=0)
    write = strength[...] * (value - retain[...] * recall)
    readout = retain[...] * read + jnp.sum(unit * query, axis=1, keepdims=True) * write
    normed = readout * lax.rsqrt(jnp.mean(readout * readout, axis=1, keepdims=True) + epsilon)
    normed = normed * head_gain[...] * (gate / (1.0 + jnp.exp(-gate)))
    normed = normed.astype(jnp.bfloat16).astype(jnp.float32)
    for h in range(heads):
        mixed[:, h * size : (h + 1) * size] = normed[h : h + 1]
    unit_ref[...] = unit
    write_ref[...] = write


def mix_out(chips, tokens, own, *refs):
    got, (others, weight, middle, rows) = refs[: chips - 1], refs[chips - 1 :]
    rows[pl.ds(mine_lane(0), 1), :] = own[...]
    rows[pl.ds(other_lane(0), 1), :] = others[0:1]
    for d in range(1, chips):
        rows[pl.ds(mine_lane(d), 1), :] = got[d - 1][...]
        rows[pl.ds(other_lane(d), 1), :] = others[d : d + 1]
    branch = dot(rows[...].astype(jnp.bfloat16), weight[...])
    middle[...] = (tokens[...].astype(jnp.float32) + branch).astype(jnp.bfloat16)


def up_piece(piece, lane, gain, weight, parts):
    size = piece.shape[1]
    wide = piece.astype(jnp.float32)
    ready = (wide * gain[:, span(lane, size)]).astype(jnp.bfloat16)
    parts.append((dot(ready, weight[span(lane, size), :]), jnp.sum(wide * wide, axis=1, keepdims=True)))


def up_first(chips, own, *refs):
    got, (gain, weight, total, squares) = refs[: chips - 1], refs[chips - 1 :]
    parts = []
    for d in range(chips):
        up_piece((got[d - 1] if d else own)[...], mine_lane(d), gain, weight, parts)
    total[...] = sum(part[0] for part in parts)
    squares[...] = jnp.broadcast_to(sum(part[1] for part in parts), squares.shape)


def up_rest(chips, others, before, before_squares, gain, weight, down, hidden_ref, leaving):
    parts = [(before[...], before_squares[:, :1])]
    for d in range(chips):
        up_piece(others[d], other_lane(d), gain, weight, parts)
    scale = lax.rsqrt(sum(part[1] for part in parts) / gain.shape[1] + epsilon)
    raised = jnp.maximum(sum(part[0] for part in parts) * scale, 0.0)
    hidden = (raised * raised).astype(jnp.bfloat16)
    hidden_ref[...] = hidden
    size = leaving.shape[2]
    for d in range(chips):
        leaving[d] = dot(hidden, down[:, span(other_lane(d), size)]).astype(jnp.bfloat16)


def down_own(chips, hidden, down, staying):
    size = staying.shape[2]
    for d in range(chips):
        staying[d] = dot(hidden[...], down[:, span(mine_lane(d), size)])


def kernel_device(
    chips,
    tokens,
    memory,
    mix_gain,
    w_query,
    w_key,
    w_value,
    w_gate,
    w_beta,
    w_decay,
    decay_rate,
    decay_bias,
    head_gain,
    w_out,
    ffn_gain,
    w_up,
    w_down,
):
    f32, bf16 = jnp.float32, jnp.bfloat16
    rows, features = tokens.shape
    width = mix_gain.shape[0]
    heads = w_beta.shape[1]
    size = head_gain.shape[0]
    units = w_up.shape[1]
    part = w_query.shape[1]

    got = far([tokens] * chips, chips)[1:]
    partner = near(tokens)
    (tokens,) = call(keep_near, [(tokens.shape, bf16)], [tokens], work=8e9)
    others = near(jnp.stack(got))
    weights = [weight.T for weight in (w_query, w_key, w_value, w_gate)]
    gain_in = mix_gain.reshape(1, width)
    total, squares, lifted = call(
        functools.partial(project_first, chips),
        [((rows, 4 * part), f32), ((rows, 128), f32), ((rows, width), bf16)],
        [tokens, partner, *got, gain_in, *weights],
    )
    scale_in, lifted, *leaving = call(
        functools.partial(project_rest, chips),
        [((rows, 128), f32), ((rows, width), bf16)] + [((2, 4 * part), f32)] * chips,
        [others, total, squares, lifted, gain_in, *weights],
        [pltpu.VMEM((rows, 4 * part), f32)],
    )
    strength, retain = call(
        own_gates,
        [((heads, size), f32)] * 2,
        [lifted, scale_in, w_beta.T, w_decay.T]
        + [value.reshape(1, heads) for value in (decay_rate, decay_bias)],
    )
    mine = jnp.stack(far(leaving, chips))
    matrix = memory.reshape(heads, size, size)
    mixed, unit, write = call(
        functools.partial(read_memory, chips),
        [((1, heads * size), f32), ((heads, size), f32), ((heads, size), f32)],
        [mine, near(mine), strength, retain, matrix, head_gain.reshape(1, size)],
        [pltpu.VMEM((4, heads, size), f32)],
    )
    updated = retain[:, :1, None] * matrix + unit[:, :, None] * write[:, None, :]

    got = far([mixed] * chips, chips)[1:]
    others = near(jnp.concatenate([mixed] + got, axis=0))
    (middle,) = call(
        functools.partial(mix_out, chips),
        [((rows, features), bf16)],
        [tokens, mixed, *got, others, w_out],
        [pltpu.VMEM((rows, heads * size), f32)],
    )

    got = far([middle] * chips, chips)[1:]
    others = near(jnp.stack([middle] + got))
    gain_mid = ffn_gain.reshape(1, width)
    total, squares = call(
        functools.partial(up_first, chips),
        [((rows, units), f32), ((rows, 128), f32)],
        [middle, *got, gain_mid, w_up],
    )
    hidden, leaving = call(
        functools.partial(up_rest, chips),
        [((rows, units), bf16), ((chips, rows, features), bf16)],
        [others, total, squares, gain_mid, w_up, w_down],
    )
    arrived = near(leaving)
    (staying,) = call(
        functools.partial(down_own, chips), [((chips, rows, features), f32)], [hidden, w_down]
    )
    sums = staying + arrived.astype(f32)
    terms = far([sums[0]] + [sums[d].astype(bf16) for d in range(1, chips)], chips)
    down = sum(term.astype(f32) for term in terms)
    layer_out = (middle.astype(f32) + down).astype(bf16)
    return (layer_out, updated.reshape(memory.shape))


def per_device(chips, *arrays):
    tokens, memory, head_gain = arrays[0], arrays[1], arrays[11]
    fits = (
        memory.shape[0] == 1
        and tokens.shape[0] == 2 * chips
        and tokens.shape[1] % 128 == 0
        and arrays[3].shape[1] % 16 == 0
        and 2 * arrays[3].shape[1] % head_gain.shape[0] == 0
        and head_gain.shape[0] == 128
        and memory.shape[1] <= 32
    )
    return (kernel_device if fits else plain_device)(chips, *arrays)


def solution(mesh):
    chips = mesh.shape["kv"]
    placed = (
        P(("grp", "dp"), ("kv", "tp")),
        P(("grp", "dp", "kv", "tp"), None, None),
        P(),
        P(None, ("kv", "tp")),
        P(None, ("kv", "tp")),
        P(None, ("kv", "tp")),
        P(None, ("kv", "tp")),
        P(),
        P(),
        P(),
        P(),
        P(),
        P(None, ("kv", "tp")),
        P(),
        P(None, ("kv", "tp")),
        P(("kv", "tp"), None),
    )

    def step(*arrays):
        return per_device(chips, *arrays)

    return jax.shard_map(
        step,
        mesh=mesh,
        in_specs=placed,
        out_specs=(P(("grp", "dp"), ("kv", "tp")), P(("grp", "dp", "kv", "tp"), None, None)),
        check_vma=False,
    )
```

profile of v0, /device:TPU:0, one launch (start us, length us, event | category | flops | bytes accessed | tf_op | source)
XLA Modules:
  0.0 45.9 jit_solution(3513285503678985071)
XLA Ops:
  0.7 3.6 %collective-permute-start.1 = (bf16[8,256]{1,0:T(8,128)(2,1)}, bf16[8,256]{1,0:T(8,128)(2,1)S(1)}, u32[]{:S(2)}, u32[]{:S(2)}) collective-permute-start(bf16[8,256]{1,0:T(8,128)(2,1)} %tokens.1), channel_id=1, source_target_pairs={{0,5},{1,4},{2,7},{3,6},{4,1},{5,0},{6,3},{7,2},{8,13},{9,12},{10,... | collective-permute-start | bytes 12296 | tf_op jit(solution)/shard_map/ppermute | solution.py:31
  4.3 1.9 %collective-permute-start = (bf16[8,256]{1,0:T(8,128)(2,1)}, bf16[8,256]{1,0:T(8,128)(2,1)S(1)}, u32[]{:S(2)}, u32[]{:S(2)}) collective-permute-start(bf16[8,256]{1,0:T(8,128)(2,1)} %tokens.1), channel_id=1, source_target_pairs={{0,3},{1,2},{2,1},{3,0},{4,7},{5,6},{6,5},{7,4},{8,11},{9,10},{10,... | collective-permute-start | bytes 12296 | tf_op jit(solution)/shard_map/ppermute | solution.py:31
  6.1 0.7 %copy-done.12 = bf16[8,256]{1,0:T(8,128)(2,1)S(1)} copy-done((bf16[8,256]{1,0:T(8,128)(2,1)S(1)}, bf16[8,256]{1,0:T(8,128)(2,1)}, u32[]{:S(2)}) %copy-start.12) | copy-done | bytes 4120
  6.9 0.7 %collective-permute-done.refs_0_ = bf16[8,256]{1,0:T(8,128)(2,1)S(1)} collective-permute-done((bf16[8,256]{1,0:T(8,128)(2,1)}, bf16[8,256]{1,0:T(8,128)(2,1)S(1)}, u32[]{:S(2)}, u32[]{:S(2)}) %collective-permute-start) | collective-permute-done | bytes 4128 | tf_op jit(solution)/shard_map/ppermute | solution.py:31
  7.6 3.5 %collective-permute-done.2.refs_2_ = bf16[8,256]{1,0:T(8,128)(2,1)S(1)} collective-permute-done((bf16[8,256]{1,0:T(8,128)(2,1)}, bf16[8,256]{1,0:T(8,128)(2,1)S(1)}, u32[]{:S(2)}, u32[]{:S(2)}) %collective-permute-start.2) | collective-permute-done | bytes 4128 | tf_op jit(solution)/shard_map/ppermute | solution.py:31
  11.7 0.7 %shard_map.168 = (f32[8,768]{1,0:T(8,128)S(1)}, f32[8,128]{1,0:T(8,128)S(1)}, bf16[8,2048]{1,0:T(8,128)(2,1)S(1)}) custom-call(bf16[8,256]{1,0:T(8,128)(2,1)S(1)} %shard_map.167.tokens, bf16[8,256]{1,0:T(8,128)(2,1)S(1)} %collective-permute-done.4.partner, bf16[8,256]{1,0:T(8,128)(2,1)S(1)} %collective-permute-done.refs_0_, ...), custom_call_target="tpu_custom_call" | custom-call | flops 1000000000 | tf_op jit(solution)/shard_map/pallas_call | solution.py:193
  13.6 3.5 %collective-permute-start.7 = (f32[2,768]{1,0:T(2,128)S(1)}, f32[2,768]{1,0:T(2,128)S(1)}, u32[]{:S(2)}, u32[]{:S(2)}) collective-permute-start(f32[2,768]{1,0:T(2,128)S(1)} %get-tuple-element.26), channel_id=1, source_target_pairs={{0,7},{1,6},{2,5},{3,4},{4,3},{5,2},{6,1},{7,0},{8,15},{9,14},{10,... | collective-permute-start | bytes 18440 | tf_op jit(solution)/shard_map/ppermute | solution.py:31
  17.1 1.4 %collective-permute-done.7 = f32[2,768]{1,0:T(2,128)S(1)} collective-permute-done((f32[2,768]{1,0:T(2,128)S(1)}, f32[2,768]{1,0:T(2,128)S(1)}, u32[]{:S(2)}, u32[]{:S(2)}) %collective-permute-start.7) | collective-permute-done | bytes 6176 | tf_op jit(solution)/shard_map/ppermute | solution.py:31
  19.1 0.7 %collective-permute-done.8.refs_1_ = f32[4,2,768]{2,1,0:T(2,128)S(1)} collective-permute-done((f32[4,2,768]{2,1,0:T(2,128)S(1)}, f32[4,2,768]{2,1,0:T(2,128)S(1)}, u32[]{:S(2)}, u32[]{:S(2)}) %collective-permute-start.8) | collective-permute-done | bytes 24608 | tf_op jit(solution)/shard_map/ppermute | solution.py:36
  19.8 1.0 %shard_map.171 = (f32[1,1536]{1,0:T(1,128)S(1)}, f32[12,128]{1,0:T(8,128)S(1)}, f32[12,128]{1,0:T(8,128)S(1)}) custom-call(f32[4,2,768]{2,1,0:T(2,128)S(1)} %pad_maximum_fusion.refs_0_, f32[4,2,768]{2,1,0:T(2,128)S(1)} %collective-permute-done.8.refs_1_, f32[12,128]{1,0:T(8,128)S(1)} %get-tuple-element.29.refs_2_, f32[12,128]{1,0:T(8,128)S(1)} %get-tuple-element.30.refs_3_, ...), custom_call_target="tpu_custom_call" | custom-call | flops 1000000000 | tf_op jit(solution)/shard_map/pallas_call | solution.py:193
  20.8 3.5 %collective-permute-start.11 = (f32[1,1536]{1,0:T(1,128)S(1)}, f32[1,1536]{1,0:T(1,128)S(1)}, u32[]{:S(2)}, u32[]{:S(2)}) collective-permute-start(f32[1,1536]{1,0:T(1,128)S(1)} %get-tuple-element.31.own), channel_id=1, source_target_pairs={{0,7},{1,6},{2,5},{3,4},{4,3},{5,2},{6,1},{7,0},{8,15},{9,14},{10,... | collective-permute-start | bytes 18440 | tf_op jit(solution)/shard_map/ppermute | solution.py:31
  24.8 1.0 %collective-permute-done.11.refs_2_ = f32[1,1536]{1,0:T(1,128)S(1)} collective-permute-done((f32[1,1536]{1,0:T(1,128)S(1)}, f32[1,1536]{1,0:T(1,128)S(1)}, u32[]{:S(2)}, u32[]{:S(2)}) %collective-permute-start.11) | collective-permute-done | bytes 6176 | tf_op jit(solution)/shard_map/ppermute | solution.py:31
  25.7 2.6 %collective-permute-done.10.refs_1_ = f32[1,1536]{1,0:T(1,128)S(1)} collective-permute-done((f32[1,1536]{1,0:T(1,128)S(1)}, f32[1,1536]{1,0:T(1,128)S(1)}, u32[]{:S(2)}, u32[]{:S(2)}) %collective-permute-start.10) | collective-permute-done | bytes 6176 | tf_op jit(solution)/shard_map/ppermute | solution.py:31
  28.7 0.9 %collective-permute-done.12.refs_3_ = f32[4,1536]{1,0:T(4,128)S(1)} collective-permute-done((f32[4,1536]{1,0:T(4,128)S(1)}, f32[4,1536]{1,0:T(4,128)S(1)}, u32[]{:S(2)}, u32[]{:S(2)}) %collective-permute-start.12) | collective-permute-done | bytes 24608 | tf_op jit(solution)/shard_map/ppermute | solution.py:36
  29.8 1.3 %collective-permute-start.15 = (bf16[8,256]{1,0:T(8,128)(2,1)S(1)}, bf16[8,256]{1,0:T(8,128)(2,1)S(1)}, u32[]{:S(2)}, u32[]{:S(2)}) collective-permute-start(bf16[8,256]{1,0:T(8,128)(2,1)S(1)} %shard_map.172.own), channel_id=1, source_target_pairs={{0,7},{1,6},{2,5},{3,4},{4,3},{5,2},{6,1},{7,0},{8,15},{9,14},{10,... | collective-permute-start | bytes 12296 | tf_op jit(solution)/shard_map/ppermute | solution.py:31
  31.6 2.1 %collective-permute-start.13 = (bf16[8,256]{1,0:T(8,128)(2,1)S(1)}, bf16[8,256]{1,0:T(8,128)(2,1)S(1)}, u32[]{:S(2)}, u32[]{:S(2)}) collective-permute-start(bf16[8,256]{1,0:T(8,128)(2,1)S(1)} %shard_map.172.own), channel_id=1, source_target_pairs={{0,3},{1,2},{2,1},{3,0},{4,7},{5,6},{6,5},{7,4},{8,11},{9,10},{10,... | collective-permute-start | bytes 12296 | tf_op jit(solution)/shard_map/ppermute | solution.py:31
  34.0 0.7 %collective-permute-done.15.refs_2_ = bf16[8,256]{1,0:T(8,128)(2,1)S(1)} collective-permute-done((bf16[8,256]{1,0:T(8,128)(2,1)S(1)}, bf16[8,256]{1,0:T(8,128)(2,1)S(1)}, u32[]{:S(2)}, u32[]{:S(2)}) %collective-permute-start.15) | collective-permute-done | bytes 4128 | tf_op jit(solution)/shard_map/ppermute | solution.py:31
  36.3 0.7 %shard_map.174 = (bf16[8,1024]{1,0:T(8,128)(2,1)S(1)}, bf16[4,8,256]{2,1,0:T(8,128)(2,1)S(1)}) custom-call(bf16[4,8,256]{2,1,0:T(8,128)(2,1)S(1)} %collective-permute-done.16.others, f32[8,1024]{1,0:T(8,128)S(1)} %get-tuple-element.32.before, f32[8,128]{1,0:T(8,128)S(1)} %get-tuple-element.33.before_squares, f32[1,2048]{1,0:T(1,128)S(1)} %bitcast.45, ...), custom_call_target="tpu_custom_call" | custom-call | flops 1000000000 | tf_op jit(solution)/shard_map/pallas_call | solution.py:193
  38.3 1.6 %collective-permute-start.18 = (bf16[8,256]{1,0:T(8,128)(2,1)S(1)}, bf16[8,256]{1,0:T(8,128)(2,1)S(1)}, u32[]{:S(2)}, u32[]{:S(2)}) collective-permute-start(bf16[8,256]{1,0:T(8,128)(2,1)S(1)} %get-tuple-element.40), channel_id=1, source_target_pairs={{0,3},{1,2},{2,1},{3,0},{4,7},{5,6},{6,5},{7,4},{8,11},{9,10},{10,... | collective-permute-start | bytes 12296 | tf_op jit(solution)/shard_map/ppermute | solution.py:31
  39.9 1.4 %collective-permute-start.20 = (bf16[8,256]{1,0:T(8,128)(2,1)S(1)}, bf16[8,256]{1,0:T(8,128)(2,1)S(1)}, u32[]{:S(2)}, u32[]{:S(2)}) collective-permute-start(bf16[8,256]{1,0:T(8,128)(2,1)S(1)} %get-tuple-element.41), channel_id=1, source_target_pairs={{0,7},{1,6},{2,5},{3,4},{4,3},{5,2},{6,1},{7,0},{8,15},{9,14},{10,... | collective-permute-start | bytes 12296 | tf_op jit(solution)/shard_map/ppermute | solution.py:31
  41.4 1.8 %multiply_add_fusion = f32[1,12,16384]{2,0,1:T(1,128)} fusion(f32[1,12,16384]{2,0,1:T(1,128)S(1)} %bitcast.68, f32[1,12,16384]{2,0,1:T(1,128)S(1)} %copy-done.2, f32[12]{0:T(128)S(1)} %slice_reduce_fusion), kind=kLoop, calls=%fused_computation | loop fusion | flops 393216 | bytes 2359344 | tf_op jit(solution)/shard_map/add | solution.py:419
  43.2 1.5 %collective-permute-done.20 = bf16[8,256]{1,0:T(8,128)(2,1)S(1)} collective-permute-done((bf16[8,256]{1,0:T(8,128)(2,1)S(1)}, bf16[8,256]{1,0:T(8,128)(2,1)S(1)}, u32[]{:S(2)}, u32[]{:S(2)}) %collective-permute-start.20) | collective-permute-done | bytes 4128 | tf_op jit(solution)/shard_map/ppermute | solution.py:31
  44.7 0.6 %collective-permute-done.19 = bf16[8,256]{1,0:T(8,128)(2,1)S(1)} collective-permute-done((bf16[8,256]{1,0:T(8,128)(2,1)S(1)}, bf16[8,256]{1,0:T(8,128)(2,1)S(1)}, u32[]{:S(2)}, u32[]{:S(2)}) %collective-permute-start.19) | collective-permute-done | bytes 4128 | tf_op jit(solution)/shard_map/ppermute | solution.py:31
  45.3 0.6 %fusion.4 = bf16[8,256]{1,0:T(8,128)(2,1)} fusion(f32[4,8,256]{2,1,0:T(8,128)S(1)} %get-tuple-element.39, bf16[8,256]{1,0:T(8,128)(2,1)S(1)} %collective-permute-done.20, bf16[8,256]{1,0:T(8,128)(2,1)S(1)} %collective-permute-done.19, bf16[8,256]{1,0:T(8,128)(2,1)S(1)} %collective-permute-done.18, bf16[8,256]{1,0:T(8,128)(2,1)S(1)} %shard_map.172.own), kind=kLoop, calls=%fused_computation.12 | loop fusion | flops 18432 | bytes 28672 | tf_op jit(solution)/shard_map/convert_element_type | solution.py:450
  (69 shorter events, 7.2 us)
Async XLA Ops:
  0.7 6.2 %collective-permute-start.1 = (bf16[8,256]{1,0:T(8,128)(2,1)}, bf16[8,256]{1,0:T(8,128)(2,1)S(1)}, u32[]{:S(2)}, u32[]{:S(2)}) collective-permute-start(bf16[8,256]{1,0:T(8,128)(2,1)} %tokens.1), channel_id=1, source_target_pairs={{0,5},{1,4},{2,7},{3,6},{4,1},{5,0},{6,3},{7,2},{8,13},{9,12},{10,... | collective-permute-start | bytes 12296 | tf_op jit(solution)/shard_map/ppermute | solution.py:31
  4.3 3.4 %collective-permute-start = (bf16[8,256]{1,0:T(8,128)(2,1)}, bf16[8,256]{1,0:T(8,128)(2,1)S(1)}, u32[]{:S(2)}, u32[]{:S(2)}) collective-permute-start(bf16[8,256]{1,0:T(8,128)(2,1)} %tokens.1), channel_id=1, source_target_pairs={{0,3},{1,2},{2,1},{3,0},{4,7},{5,6},{6,5},{7,4},{8,11},{9,10},{10,... | collective-permute-start | bytes 12296 | tf_op jit(solution)/shard_map/ppermute | solution.py:31
  6.1 5.6 %collective-permute-start.4 = (bf16[8,256]{1,0:T(8,128)(2,1)}, bf16[8,256]{1,0:T(8,128)(2,1)S(1)}, u32[]{:S(2)}, u32[]{:S(2)}) collective-permute-start(bf16[8,256]{1,0:T(8,128)(2,1)} %tokens.1), channel_id=1, source_target_pairs={{0,1},{1,0},{2,3},{3,2},{4,5},{5,4},{6,7},{7,6},{8,9},{9,8},{10,11... | collective-permute-start | bytes 12296 | tf_op jit(solution)/shard_map/ppermute | solution.py:36
  6.1 5.0 %collective-permute-start.2 = (bf16[8,256]{1,0:T(8,128)(2,1)}, bf16[8,256]{1,0:T(8,128)(2,1)S(1)}, u32[]{:S(2)}, u32[]{:S(2)}) collective-permute-start(bf16[8,256]{1,0:T(8,128)(2,1)} %tokens.1), channel_id=1, source_target_pairs={{0,7},{1,6},{2,5},{3,4},{4,3},{5,2},{6,1},{7,0},{8,15},{9,14},{10,... | collective-permute-start | bytes 12296 | tf_op jit(solution)/shard_map/ppermute | solution.py:31
  11.2 1.3 %collective-permute-start.3 = (bf16[3,8,256]{2,1,0:T(8,128)(2,1)S(1)}, bf16[3,8,256]{2,1,0:T(8,128)(2,1)S(1)}, u32[]{:S(2)}, u32[]{:S(2)}) collective-permute-start(bf16[3,8,256]{2,1,0:T(8,128)(2,1)S(1)} %pad_maximum_fusion.3), channel_id=1, source_target_pairs={{0,1},{1,0},{2,3},{3,2},{4,5},{5,4},{6,7},{7,6},{8,9},{9,8},{10,11... | collective-permute-start | bytes 36872 | tf_op jit(solution)/shard_map/ppermute | solution.py:36
  13.0 16.6 %copy-start.8 = (bf16[1536,256]{1,0:T(8,128)(2,1)S(1)}, bf16[1536,256]{1,0:T(8,128)(2,1)}, u32[]{:S(2)}) copy-start(bf16[1536,256]{1,0:T(8,128)(2,1)} %refs_4_.2) | copy-start | bytes 2359300
  13.0 4.1 %collective-permute-start.5 = (f32[2,768]{1,0:T(2,128)S(1)}, f32[2,768]{1,0:T(2,128)S(1)}, u32[]{:S(2)}, u32[]{:S(2)}) collective-permute-start(f32[2,768]{1,0:T(2,128)S(1)} %get-tuple-element.24), channel_id=1, source_target_pairs={{0,3},{1,2},{2,1},{3,0},{4,7},{5,6},{6,5},{7,4},{8,11},{9,10},{10,... | collective-permute-start | bytes 18440 | tf_op jit(solution)/shard_map/ppermute | solution.py:31
  13.1 4.0 %collective-permute-start.6 = (f32[2,768]{1,0:T(2,128)S(1)}, f32[2,768]{1,0:T(2,128)S(1)}, u32[]{:S(2)}, u32[]{:S(2)}) collective-permute-start(f32[2,768]{1,0:T(2,128)S(1)} %get-tuple-element.25), channel_id=1, source_target_pairs={{0,5},{1,4},{2,7},{3,6},{4,1},{5,0},{6,3},{7,2},{8,13},{9,12},{10,... | collective-permute-start | bytes 18440 | tf_op jit(solution)/shard_map/ppermute | solution.py:31
  13.6 4.9 %collective-permute-start.7 = (f32[2,768]{1,0:T(2,128)S(1)}, f32[2,768]{1,0:T(2,128)S(1)}, u32[]{:S(2)}, u32[]{:S(2)}) collective-permute-start(f32[2,768]{1,0:T(2,128)S(1)} %get-tuple-element.26), channel_id=1, source_target_pairs={{0,7},{1,6},{2,5},{3,4},{4,3},{5,2},{6,1},{7,0},{8,15},{9,14},{10,... | collective-permute-start | bytes 18440 | tf_op jit(solution)/shard_map/ppermute | solution.py:31
  18.5 1.3 %collective-permute-start.8 = (f32[4,2,768]{2,1,0:T(2,128)S(1)}, f32[4,2,768]{2,1,0:T(2,128)S(1)}, u32[]{:S(2)}, u32[]{:S(2)}) collective-permute-start(f32[4,2,768]{2,1,0:T(2,128)S(1)} %pad_maximum_fusion.refs_0_), channel_id=1, source_target_pairs={{0,1},{1,0},{2,3},{3,2},{4,5},{5,4},{6,7},{7,6},{8,9},{9,8},{10,11... | collective-permute-start | bytes 73736 | tf_op jit(solution)/shard_map/ppermute | solution.py:36
  19.1 16.4 %copy-start = (bf16[2048,1024]{1,0:T(8,128)(2,1)S(1)}, bf16[2048,1024]{1,0:T(8,128)(2,1)}, u32[]{:S(2)}) copy-start(bf16[2048,1024]{1,0:T(8,128)(2,1)} %weight.1) | copy-start | bytes 12582916
  19.1 16.4 %copy-start.3 = (f32[2048]{0:T(1024)S(1)}, f32[2048]{0:T(1024)}, u32[]{:S(2)}) copy-start(f32[2048]{0:T(1024)} %param.29) | copy-start | bytes 24580
  20.8 4.9 %collective-permute-start.11 = (f32[1,1536]{1,0:T(1,128)S(1)}, f32[1,1536]{1,0:T(1,128)S(1)}, u32[]{:S(2)}, u32[]{:S(2)}) collective-permute-start(f32[1,1536]{1,0:T(1,128)S(1)} %get-tuple-element.31.own), channel_id=1, source_target_pairs={{0,7},{1,6},{2,5},{3,4},{4,3},{5,2},{6,1},{7,0},{8,15},{9,14},{10,... | collective-permute-start | bytes 18440 | tf_op jit(solution)/shard_map/ppermute | solution.py:31
  24.3 4.0 %collective-permute-start.10 = (f32[1,1536]{1,0:T(1,128)S(1)}, f32[1,1536]{1,0:T(1,128)S(1)}, u32[]{:S(2)}, u32[]{:S(2)}) collective-permute-start(f32[1,1536]{1,0:T(1,128)S(1)} %get-tuple-element.31.own), channel_id=1, source_target_pairs={{0,5},{1,4},{2,7},{3,6},{4,1},{5,0},{6,3},{7,2},{8,13},{9,12},{10,... | collective-permute-start | bytes 18440 | tf_op jit(solution)/shard_map/ppermute | solution.py:31
  24.3 4.0 %collective-permute-start.9 = (f32[1,1536]{1,0:T(1,128)S(1)}, f32[1,1536]{1,0:T(1,128)S(1)}, u32[]{:S(2)}, u32[]{:S(2)}) collective-permute-start(f32[1,1536]{1,0:T(1,128)S(1)} %get-tuple-element.31.own), channel_id=1, source_target_pairs={{0,3},{1,2},{2,1},{3,0},{4,7},{5,6},{6,5},{7,4},{8,11},{9,10},{10,... | collective-permute-start | bytes 18440 | tf_op jit(solution)/shard_map/ppermute | solution.py:31
  28.3 1.3 %collective-permute-start.12 = (f32[4,1536]{1,0:T(4,128)S(1)}, f32[4,1536]{1,0:T(4,128)S(1)}, u32[]{:S(2)}, u32[]{:S(2)}) collective-permute-start(f32[4,1536]{1,0:T(4,128)S(1)} %pad_maximum_fusion.1), channel_id=1, source_target_pairs={{0,1},{1,0},{2,3},{3,2},{4,5},{5,4},{6,7},{7,6},{8,9},{9,8},{10,11... | collective-permute-start | bytes 73736 | tf_op jit(solution)/shard_map/ppermute | solution.py:36
  29.8 4.8 %collective-permute-start.15 = (bf16[8,256]{1,0:T(8,128)(2,1)S(1)}, bf16[8,256]{1,0:T(8,128)(2,1)S(1)}, u32[]{:S(2)}, u32[]{:S(2)}) collective-permute-start(bf16[8,256]{1,0:T(8,128)(2,1)S(1)} %shard_map.172.own), channel_id=1, source_target_pairs={{0,7},{1,6},{2,5},{3,4},{4,3},{5,2},{6,1},{7,0},{8,15},{9,14},{10,... | collective-permute-start | bytes 12296 | tf_op jit(solution)/shard_map/ppermute | solution.py:31
  31.1 4.0 %collective-permute-start.14 = (bf16[8,256]{1,0:T(8,128)(2,1)S(1)}, bf16[8,256]{1,0:T(8,128)(2,1)S(1)}, u32[]{:S(2)}, u32[]{:S(2)}) collective-permute-start(bf16[8,256]{1,0:T(8,128)(2,1)S(1)} %shard_map.172.own), channel_id=1, source_target_pairs={{0,5},{1,4},{2,7},{3,6},{4,1},{5,0},{6,3},{7,2},{8,13},{9,12},{10,... | collective-permute-start | bytes 12296 | tf_op jit(solution)/shard_map/ppermute | solution.py:31
  31.6 3.4 %collective-permute-start.13 = (bf16[8,256]{1,0:T(8,128)(2,1)S(1)}, bf16[8,256]{1,0:T(8,128)(2,1)S(1)}, u32[]{:S(2)}, u32[]{:S(2)}) collective-permute-start(bf16[8,256]{1,0:T(8,128)(2,1)S(1)} %shard_map.172.own), channel_id=1, source_target_pairs={{0,3},{1,2},{2,1},{3,0},{4,7},{5,6},{6,5},{7,4},{8,11},{9,10},{10,... | collective-permute-start | bytes 12296 | tf_op jit(solution)/shard_map/ppermute | solution.py:31
  35.1 1.2 %collective-permute-start.16 = (bf16[4,8,256]{2,1,0:T(8,128)(2,1)S(1)}, bf16[4,8,256]{2,1,0:T(8,128)(2,1)S(1)}, u32[]{:S(2)}, u32[]{:S(2)}) collective-permute-start(bf16[4,8,256]{2,1,0:T(8,128)(2,1)S(1)} %pad_maximum_fusion.2), channel_id=1, source_target_pairs={{0,1},{1,0},{2,3},{3,2},{4,5},{5,4},{6,7},{7,6},{8,9},{9,8},{10,11... | collective-permute-start | bytes 49160 | tf_op jit(solution)/shard_map/ppermute | solution.py:36
  37.0 1.2 %collective-permute-start.17 = (bf16[4,8,256]{2,1,0:T(8,128)(2,1)S(1)}, bf16[4,8,256]{2,1,0:T(8,128)(2,1)S(1)}, u32[]{:S(2)}, u32[]{:S(2)}) collective-permute-start(bf16[4,8,256]{2,1,0:T(8,128)(2,1)S(1)} %get-tuple-element.35), channel_id=1, source_target_pairs={{0,1},{1,0},{2,3},{3,2},{4,5},{5,4},{6,7},{7,6},{8,9},{9,8},{10,11... | collective-permute-start | bytes 49160 | tf_op jit(solution)/shard_map/ppermute | solution.py:36
  38.3 4.9 %collective-permute-start.18 = (bf16[8,256]{1,0:T(8,128)(2,1)S(1)}, bf16[8,256]{1,0:T(8,128)(2,1)S(1)}, u32[]{:S(2)}, u32[]{:S(2)}) collective-permute-start(bf16[8,256]{1,0:T(8,128)(2,1)S(1)} %get-tuple-element.40), channel_id=1, source_target_pairs={{0,3},{1,2},{2,1},{3,0},{4,7},{5,6},{6,5},{7,4},{8,11},{9,10},{10,... | collective-permute-start | bytes 12296 | tf_op jit(solution)/shard_map/ppermute | solution.py:31
  39.9 4.8 %collective-permute-start.20 = (bf16[8,256]{1,0:T(8,128)(2,1)S(1)}, bf16[8,256]{1,0:T(8,128)(2,1)S(1)}, u32[]{:S(2)}, u32[]{:S(2)}) collective-permute-start(bf16[8,256]{1,0:T(8,128)(2,1)S(1)} %get-tuple-element.41), channel_id=1, source_target_pairs={{0,7},{1,6},{2,5},{3,4},{4,3},{5,2},{6,1},{7,0},{8,15},{9,14},{10,... | collective-permute-start | bytes 12296 | tf_op jit(solution)/shard_map/ppermute | solution.py:31
  41.3 4.0 %collective-permute-start.19 = (bf16[8,256]{1,0:T(8,128)(2,1)S(1)}, bf16[8,256]{1,0:T(8,128)(2,1)S(1)}, u32[]{:S(2)}, u32[]{:S(2)}) collective-permute-start(bf16[8,256]{1,0:T(8,128)(2,1)S(1)} %get-tuple-element.42), channel_id=1, source_target_pairs={{0,5},{1,4},{2,7},{3,6},{4,1},{5,0},{6,3},{7,2},{8,13},{9,12},{10,... | collective-permute-start | bytes 12296 | tf_op jit(solution)/shard_map/ppermute | solution.py:31
  (13 other events, 125.9 us)
where the time goes:
time: 46.1 us; the launch traced here: 45.9 us
  starting transfers between devices  22.2 us (48%)
  waiting for transfers between devices  15.2 us (33%)
  Pallas kernels  4.16 us (9%)
  other arithmetic  2.68 us (6%)
  local copies, waits for them, and re-layouts  0.93 us (2%)
  between operations  0.81 us (2%)
    ppermute x15, starting transfers between devices, far(): got.append(lax.ppermute(pieces[d], axes, pairs))  20.6 us
    ppermute x15, waiting for transfers between devices, far(): got.append(lax.ppermute(pieces[d], axes, pairs))  12.4 us
    pallas_call x9, Pallas kernels, call(): pl.pallas_call(body, out_shape=[jax.ShapeDtypeStruct(shape, kind) for sha...  4.16 us
    ppermute x6, waiting for transfers between devices, near(): return lax.ppermute(value, 'tp', [(0, 1), (1, 0)])  2.74 us
    add x1, other arithmetic, kernel_device(): retain[:, :1, None] * matrix + unit[:, :, None] * write[:, None, :]  1.76 us
    ppermute x6, starting transfers between devices, near(): return lax.ppermute(value, 'tp', [(0, 1), (1, 0)])  1.63 us
  transfers between devices with their start and end apart: 21, of which 14 were waited for; matrix products, arithmetic and copies ran while one was open for 5% of the time, Pallas kernels for 4%

commit v1 on v0

--- a/solution.py
+++ b/solution.py
@@ -269,7 +269,7 @@
 
 
 def read_memory(chips, *refs):
-    mine, other, strength, retain, memory, head_gain, mixed, unit_ref, write_ref, parts = refs
+    mine, other, strength, retain, memory, head_gain, mixed, turned_ref, write_ref, parts = refs
     heads, size = strength.shape
     chip, core = place()
     part = mine.shape[2] // 4
@@ -288,61 +288,82 @@
                 h = there * across + i
                 parts[t, h : h + 1, :] = pair[:, i * size : (i + 1) * size]
     query, key, value, gate = parts[0], parts[1], parts[2], parts[3]
-    unit = key * lax.rsqrt(jnp.sum(key * key, axis=1, keepdims=True) + epsilon)
+    shrink = lax.rsqrt(jnp.sum(key * key, axis=1, keepdims=True) + epsilon)
     padded = -(-heads // 8) * 8
     pad = [jnp.zeros((padded - heads, size), jnp.float32)] if padded > heads else []
     rest = jnp.zeros((size - 2 * padded, size), jnp.float32)
-    turned = jnp.concatenate([unit, *pad, query, *pad, rest], axis=0).T
+    turned = jnp.concatenate([key, *pad, query, *pad, rest], axis=0).T
     recalls, reads = [], []
     for h in range(heads):
         matrix = memory[h]
         recalls.append(jnp.sum(matrix * turned[:, h : h + 1], axis=0, keepdims=True))
         at = padded + h
         reads.append(jnp.sum(matrix * turned[:, at : at + 1], axis=0, keepdims=True))
-    recall = jnp.concatenate(recalls, axis=0)
+    recall = jnp.concatenate(recalls, axis=0) * shrink
     read = jnp.concatenate(reads, axis=0)
-    write = strength[...] * (value - retain[...] * recall)
-    readout = retain[...] * read + jnp.sum(unit * query, axis=1, keepdims=True) * write
+    write = shrink * strength[...] * (value - retain[...] * recall)
+    readout = retain[...] * read + jnp.sum(key * query, axis=1, keepdims=True) * write
     normed = readout * lax.rsqrt(jnp.mean(readout * readout, axis=1, keepdims=True) + epsilon)
     normed = normed * head_gain[...] * (gate / (1.0 + jnp.exp(-gate)))
     normed = normed.astype(jnp.bfloat16).astype(jnp.float32)
     for h in range(heads):
         mixed[:, h * size : (h + 1) * size] = normed[h : h + 1]
-    unit_ref[...] = unit
+    turned_ref[...] = turned
     write_ref[...] = write
 
 
-def mix_out(chips, tokens, own, *refs):
-    got, (others, weight, middle, rows) = refs[: chips - 1], refs[chips - 1 :]
-    rows[pl.ds(mine_lane(0), 1), :] = own[...]
-    rows[pl.ds(other_lane(0), 1), :] = others[0:1]
-    for d in range(1, chips):
-        rows[pl.ds(mine_lane(d), 1), :] = got[d - 1][...]
-        rows[pl.ds(other_lane(d), 1), :] = others[d : d + 1]
-    branch = dot(rows[...].astype(jnp.bfloat16), weight[...])
-    middle[...] = (tokens[...].astype(jnp.float32) + branch).astype(jnp.bfloat16)
-
-
-def up_piece(piece, lane, gain, weight, parts):
+def update_memory(memory, turned, write, retain, updated):
+    for h in range(memory.shape[0]):
+        row = slice(h, h + 1)
+        updated[h] = retain[row, :] * memory[h] + turned[:, row] * write[row, :]
+
+
+def by_core(own, partner):
+    first = place()[1] == 0
+    low, high = jnp.where(first, own, partner), jnp.where(first, partner, own)
+    return jnp.concatenate([low, high], axis=-1)
+
+
+def mix_out(chips, tokens, partner_tokens, own, *refs):
+    got, (weight, partner_weight, half, rows, wide) = refs[: chips - 1], refs[chips - 1 :]
+    for d in range(chips):
+        rows[d : d + 1, :] = (got[d - 1] if d else own)[...]
+    left = rows[...].astype(jnp.bfloat16)
+    branch = by_core(dot(left, weight[...]), dot(left, partner_weight[...]))
+    wide[...] = by_core(tokens[...].astype(jnp.float32), partner_tokens[...].astype(jnp.float32))
+    for d in range(chips):
+        middle = wide[pl.ds(mine_lane(d), 1), :] + branch[d : d + 1]
+        half[d : d + 1, :] = middle.astype(jnp.bfloat16).astype(jnp.float32)
+
+
+def join_rows(chips, half, other, block, own, rows):
+    for d in range(chips):
+        rows[pl.ds(mine_lane(d), 1), :] = half[d : d + 1, :]
+        rows[pl.ds(other_lane(d), 1), :] = other[d : d + 1, :]
+    block[...] = rows[...].astype(jnp.bfloat16)
+    own[...] = rows[:, span(place()[1], own.shape[1])].astype(jnp.bfloat16)
+
+
+def up_piece(piece, there, gain, weight, parts):
     size = piece.shape[1]
     wide = piece.astype(jnp.float32)
-    ready = (wide * gain[:, span(lane, size)]).astype(jnp.bfloat16)
-    parts.append((dot(ready, weight[span(lane, size), :]), jnp.sum(wide * wide, axis=1, keepdims=True)))
-
-
-def up_first(chips, own, *refs):
-    got, (gain, weight, total, squares) = refs[: chips - 1], refs[chips - 1 :]
+    ready = (wide * gain[:, span(there, size)]).astype(jnp.bfloat16)
+    parts.append((dot(ready, weight[span(there, size), :]), jnp.sum(wide * wide, axis=1, keepdims=True)))
+
+
+def up_first(block, gain, weight, total, squares):
     parts = []
-    for d in range(chips):
-        up_piece((got[d - 1] if d else own)[...], mine_lane(d), gain, weight, parts)
-    total[...] = sum(part[0] for part in parts)
-    squares[...] = jnp.broadcast_to(sum(part[1] for part in parts), squares.shape)
-
-
-def up_rest(chips, others, before, before_squares, gain, weight, down, hidden_ref, leaving):
+    up_piece(block[...], place()[0], gain, weight, parts)
+    total[...] = parts[0][0]
+    squares[...] = jnp.broadcast_to(parts[0][1], squares.shape)
+
+
+def up_rest(chips, *refs):
+    got, rest = refs[: chips - 1], refs[chips - 1 :]
+    before, before_squares, gain, weight, down, hidden_ref, leaving = rest
     parts = [(before[...], before_squares[:, :1])]
-    for d in range(chips):
-        up_piece(others[d], other_lane(d), gain, weight, parts)
+    for d in range(1, chips):
+        up_piece(got[d - 1][...], place()[0] ^ d, gain, weight, parts)
     scale = lax.rsqrt(sum(part[1] for part in parts) / gain.shape[1] + epsilon)
     raised = jnp.maximum(sum(part[0] for part in parts) * scale, 0.0)
     hidden = (raised * raised).astype(jnp.bfloat16)
@@ -410,35 +431,38 @@
     )
     mine = jnp.stack(far(leaving, chips))
     matrix = memory.reshape(heads, size, size)
-    mixed, unit, write = call(
+    mixed, turned, write = call(
         functools.partial(read_memory, chips),
-        [((1, heads * size), f32), ((heads, size), f32), ((heads, size), f32)],
+        [((1, heads * size), f32), ((size, size), f32), ((heads, size), f32)],
         [mine, near(mine), strength, retain, matrix, head_gain.reshape(1, size)],
         [pltpu.VMEM((4, heads, size), f32)],
     )
-    updated = retain[:, :1, None] * matrix + unit[:, :, None] * write[:, None, :]
+    (updated,) = call(
+        update_memory, [((heads, size, size), f32)], [matrix, turned, write, retain], work=5e8
+    )
 
     got = far([mixed] * chips, chips)[1:]
-    others = near(jnp.concatenate([mixed] + got, axis=0))
-    (middle,) = call(
+    (half,) = call(
         functools.partial(mix_out, chips),
-        [((rows, features), bf16)],
-        [tokens, mixed, *got, others, w_out],
-        [pltpu.VMEM((rows, heads * size), f32)],
-    )
-
-    got = far([middle] * chips, chips)[1:]
-    others = near(jnp.stack([middle] + got))
+        [((chips, 2 * features), f32)],
+        [tokens, partner, mixed, *got, w_out, near(w_out)],
+        [pltpu.VMEM((chips, heads * size), f32), pltpu.VMEM((rows, 2 * features), f32)],
+    )
+    block, middle = call(
+        functools.partial(join_rows, chips),
+        [((rows, 2 * features), bf16), ((rows, features), bf16)],
+        [half, near(half)],
+        [pltpu.VMEM((rows, 2 * features), f32)],
+    )
+    got = far([block] * chips, chips)[1:]
     gain_mid = ffn_gain.reshape(1, width)
     total, squares = call(
-        functools.partial(up_first, chips),
-        [((rows, units), f32), ((rows, 128), f32)],
-        [middle, *got, gain_mid, w_up],
+        up_first, [((rows, units), f32), ((rows, 128), f32)], [block, gain_mid, w_up]
     )
     hidden, leaving = call(
         functools.partial(up_rest, chips),
         [((rows, units), bf16), ((chips, rows, features), bf16)],
-        [others, total, squares, gain_mid, w_up, w_down],
+        [*got, total, squares, gain_mid, w_up, w_down],
     )
     arrived = near(leaving)
     (staying,) = call(

time: 46.1 us -> 44.3 us (0.961)
  other arithmetic: 2.68 us -> 0.63 us
  waiting for transfers between devices: 15.2 us -> 13.2 us
  starting transfers between devices: 22.2 us -> 23.4 us
  Pallas kernels: 4.16 us -> 5.34 us
    add x1 -> x0, other arithmetic: 1.76 us -> none  [kernel_device(): retain[:, :1, None] * matrix + unit[:, :, None] * write[:, None, :]]
    ppermute x15, waiting for transfers between devices: 12.4 us -> 10.9 us  [far(): got.append(lax.ppermute(pieces[d], axes, pairs))]
    pallas_call x9 -> x11, Pallas kernels: 4.16 us -> 5.34 us  [call(): pl.pallas_call(body, out_shape=[jax.ShapeDtypeStruct(shape, kind) for sha...]
    ppermute x15, starting transfers between devices: 20.6 us -> 21.2 us  [far(): got.append(lax.ppermute(pieces[d], axes, pairs))]
    ppermute x6, starting transfers between devices: 1.63 us -> 2.16 us  [near(): return lax.ppermute(value, 'tp', [(0, 1), (1, 0)])]
    ppermute x6, waiting for transfers between devices: 2.74 us -> 2.26 us  [near(): return lax.ppermute(value, 'tp', [(0, 1), (1, 0)])]
  transfers between devices with their start and end apart: 21 -> 21, of which waited for: 14 -> 13; matrix products, arithmetic and copies ran while one was open for 5% -> 0% of each run, Pallas kernels for 4% -> 9%
where the time goes in v1:
time: 44.3 us; the launch traced here: 44.1 us
  starting transfers between devices  23.4 us (53%)
  waiting for transfers between devices  13.2 us (30%)
  Pallas kernels  5.34 us (12%)
  between operations  0.82 us (2%)
  local copies, waits for them, and re-layouts  0.76 us (2%)
  other arithmetic  0.63 us (1%)
    ppermute x15, starting transfers between devices, far(): got.append(lax.ppermute(pieces[d], axes, pairs))  21.2 us
    ppermute x15, waiting for transfers between devices, far(): got.append(lax.ppermute(pieces[d], axes, pairs))  10.9 us
    pallas_call x11, Pallas kernels, call(): pl.pallas_call(body, out_shape=[jax.ShapeDtypeStruct(shape, kind) for sha...  5.34 us
    ppermute x6, waiting for transfers between devices, near(): return lax.ppermute(value, 'tp', [(0, 1), (1, 0)])  2.26 us
    ppermute x6, starting transfers between devices, near(): return lax.ppermute(value, 'tp', [(0, 1), (1, 0)])  2.16 us
  transfers between devices with their start and end apart: 21, of which 13 were waited for; matrix products, arithmetic and copies ran while one was open for 0% of the time, Pallas kernels for 9%

profile of v1, /device:TPU:0, one launch (start us, length us, event | category | flops | bytes accessed | tf_op | source)
XLA Modules:
  0.0 44.1 jit_solution(6011165689511063921)
XLA Ops:
  1.2 4.7 %collective-permute-start.3 = (bf16[8,256]{1,0:T(8,128)(2,1)}, bf16[8,256]{1,0:T(8,128)(2,1)S(1)}, u32[]{:S(2)}, u32[]{:S(2)}) collective-permute-start(bf16[8,256]{1,0:T(8,128)(2,1)} %tokens.1), channel_id=1, source_target_pairs={{0,7},{1,6},{2,5},{3,4},{4,3},{5,2},{6,1},{7,0},{8,15},{9,14},{10,... | collective-permute-start | bytes 12296 | tf_op jit(solution)/shard_map/ppermute | solution.py:31
  6.6 0.7 %copy-done.12 = bf16[8,256]{1,0:T(8,128)(2,1)S(1)} copy-done((bf16[8,256]{1,0:T(8,128)(2,1)S(1)}, bf16[8,256]{1,0:T(8,128)(2,1)}, u32[]{:S(2)}) %copy-start.12) | copy-done | bytes 4120
  7.5 2.6 %collective-permute-done.2.refs_1_ = bf16[8,256]{1,0:T(8,128)(2,1)S(1)} collective-permute-done((bf16[8,256]{1,0:T(8,128)(2,1)}, bf16[8,256]{1,0:T(8,128)(2,1)S(1)}, u32[]{:S(2)}, u32[]{:S(2)}) %collective-permute-start.2) | collective-permute-done | bytes 4128 | tf_op jit(solution)/shard_map/ppermute | solution.py:31
  10.3 0.7 %shard_map.168 = (f32[8,768]{1,0:T(8,128)S(1)}, f32[8,128]{1,0:T(8,128)S(1)}, bf16[8,2048]{1,0:T(8,128)(2,1)S(1)}) custom-call(bf16[8,256]{1,0:T(8,128)(2,1)S(1)} %shard_map.167.tokens, bf16[8,256]{1,0:T(8,128)(2,1)S(1)} %collective-permute-done.partner.partner_tokens, bf16[8,256]{1,0:T(8,128)(2,1)S(1)} %collective-permute-done.1.refs_0_, ...), custom_call_target="tpu_custom_call" | custom-call | flops 1000000000 | tf_op jit(solution)/shard_map/pallas_call | solution.py:193
  11.8 1.3 %collective-permute-start.7 = (f32[2,768]{1,0:T(2,128)S(1)}, f32[2,768]{1,0:T(2,128)S(1)}, u32[]{:S(2)}, u32[]{:S(2)}) collective-permute-start(f32[2,768]{1,0:T(2,128)S(1)} %get-tuple-element.28), channel_id=1, source_target_pairs={{0,7},{1,6},{2,5},{3,4},{4,3},{5,2},{6,1},{7,0},{8,15},{9,14},{10,... | collective-permute-start | bytes 18440 | tf_op jit(solution)/shard_map/ppermute | solution.py:31
  13.6 2.1 %collective-permute-start.5 = (f32[2,768]{1,0:T(2,128)S(1)}, f32[2,768]{1,0:T(2,128)S(1)}, u32[]{:S(2)}, u32[]{:S(2)}) collective-permute-start(f32[2,768]{1,0:T(2,128)S(1)} %get-tuple-element.26), channel_id=1, source_target_pairs={{0,3},{1,2},{2,1},{3,0},{4,7},{5,6},{6,5},{7,4},{8,11},{9,10},{10,... | collective-permute-start | bytes 18440 | tf_op jit(solution)/shard_map/ppermute | solution.py:31
  15.8 1.0 %collective-permute-done.7 = f32[2,768]{1,0:T(2,128)S(1)} collective-permute-done((f32[2,768]{1,0:T(2,128)S(1)}, f32[2,768]{1,0:T(2,128)S(1)}, u32[]{:S(2)}, u32[]{:S(2)}) %collective-permute-start.7) | collective-permute-done | bytes 6176 | tf_op jit(solution)/shard_map/ppermute | solution.py:31
  17.9 0.6 %collective-permute-done.8.refs_1_ = f32[4,2,768]{2,1,0:T(2,128)S(1)} collective-permute-done((f32[4,2,768]{2,1,0:T(2,128)S(1)}, f32[4,2,768]{2,1,0:T(2,128)S(1)}, u32[]{:S(2)}, u32[]{:S(2)}) %collective-permute-start.8) | collective-permute-done | bytes 24608 | tf_op jit(solution)/shard_map/ppermute | solution.py:36
  18.5 0.9 %shard_map.171 = (f32[1,1536]{1,0:T(1,128)S(1)}, f32[128,128]{1,0:T(8,128)S(1)}, f32[12,128]{1,0:T(8,128)S(1)}) custom-call(f32[4,2,768]{2,1,0:T(2,128)S(1)} %pad_maximum_fusion.refs_0_, f32[4,2,768]{2,1,0:T(2,128)S(1)} %collective-permute-done.8.refs_1_, f32[12,128]{1,0:T(8,128)S(1)} %get-tuple-element.31.refs_2_, ...), custom_call_target="tpu_custom_call" | custom-call | flops 1000000000 | tf_op jit(solution)/shard_map/pallas_call | solution.py:193
  19.4 1.7 %collective-permute-start.9 = (f32[1,1536]{1,0:T(1,128)S(1)}, f32[1,1536]{1,0:T(1,128)S(1)}, u32[]{:S(2)}, u32[]{:S(2)}) collective-permute-start(f32[1,1536]{1,0:T(1,128)S(1)} %get-tuple-element.33.own), channel_id=1, source_target_pairs={{0,3},{1,2},{2,1},{3,0},{4,7},{5,6},{6,5},{7,4},{8,11},{9,10},{10,... | collective-permute-start | bytes 18440 | tf_op jit(solution)/shard_map/ppermute | solution.py:31
  21.1 0.9 %collective-permute-start.10 = (f32[1,1536]{1,0:T(1,128)S(1)}, f32[1,1536]{1,0:T(1,128)S(1)}, u32[]{:S(2)}, u32[]{:S(2)}) collective-permute-start(f32[1,1536]{1,0:T(1,128)S(1)} %get-tuple-element.33.own), channel_id=1, source_target_pairs={{0,5},{1,4},{2,7},{3,6},{4,1},{5,0},{6,3},{7,2},{8,13},{9,12},{10,... | collective-permute-start | bytes 18440 | tf_op jit(solution)/shard_map/ppermute | solution.py:31
  22.0 1.5 %collective-permute-start.11 = (f32[1,1536]{1,0:T(1,128)S(1)}, f32[1,1536]{1,0:T(1,128)S(1)}, u32[]{:S(2)}, u32[]{:S(2)}) collective-permute-start(f32[1,1536]{1,0:T(1,128)S(1)} %get-tuple-element.33.own), channel_id=1, source_target_pairs={{0,7},{1,6},{2,5},{3,4},{4,3},{5,2},{6,1},{7,0},{8,15},{9,14},{10,... | collective-permute-start | bytes 18440 | tf_op jit(solution)/shard_map/ppermute | solution.py:31
  23.5 1.6 %collective-permute-done.10.refs_1_ = f32[1,1536]{1,0:T(1,128)S(1)} collective-permute-done((f32[1,1536]{1,0:T(1,128)S(1)}, f32[1,1536]{1,0:T(1,128)S(1)}, u32[]{:S(2)}, u32[]{:S(2)}) %collective-permute-start.10) | collective-permute-done | bytes 6176 | tf_op jit(solution)/shard_map/ppermute | solution.py:31
  25.1 1.8 %collective-permute-done.11.refs_2_ = f32[1,1536]{1,0:T(1,128)S(1)} collective-permute-done((f32[1,1536]{1,0:T(1,128)S(1)}, f32[1,1536]{1,0:T(1,128)S(1)}, u32[]{:S(2)}, u32[]{:S(2)}) %collective-permute-start.11) | collective-permute-done | bytes 6176 | tf_op jit(solution)/shard_map/ppermute | solution.py:31
  27.7 0.8 %collective-permute-done.13.other = f32[4,512]{1,0:T(4,128)S(1)} collective-permute-done((f32[4,512]{1,0:T(4,128)S(1)}, f32[4,512]{1,0:T(4,128)S(1)}, u32[]{:S(2)}, u32[]{:S(2)}) %collective-permute-start.13) | collective-permute-done | bytes 8224 | tf_op jit(solution)/shard_map/ppermute | solution.py:36
  28.6 1.9 %collective-permute-start.15 = (bf16[8,512]{1,0:T(8,128)(2,1)S(1)}, bf16[8,512]{1,0:T(8,128)(2,1)S(1)}, u32[]{:S(2)}, u32[]{:S(2)}) collective-permute-start(bf16[8,512]{1,0:T(8,128)(2,1)S(1)} %get-tuple-element.35.block), channel_id=1, source_target_pairs={{0,5},{1,4},{2,7},{3,6},{4,1},{5,0},{6,3},{7,2},{8,13},{9,12},{10,... | collective-permute-start | bytes 24584 | tf_op jit(solution)/shard_map/ppermute | solution.py:31
  30.4 2.2 %collective-permute-start.16 = (bf16[8,512]{1,0:T(8,128)(2,1)S(1)}, bf16[8,512]{1,0:T(8,128)(2,1)S(1)}, u32[]{:S(2)}, u32[]{:S(2)}) collective-permute-start(bf16[8,512]{1,0:T(8,128)(2,1)S(1)} %get-tuple-element.35.block), channel_id=1, source_target_pairs={{0,7},{1,6},{2,5},{3,4},{4,3},{5,2},{6,1},{7,0},{8,15},{9,14},{10,... | collective-permute-start | bytes 24584 | tf_op jit(solution)/shard_map/ppermute | solution.py:31
  32.9 2.4 %collective-permute-done.16.refs_2_ = bf16[8,512]{1,0:T(8,128)(2,1)S(1)} collective-permute-done((bf16[8,512]{1,0:T(8,128)(2,1)S(1)}, bf16[8,512]{1,0:T(8,128)(2,1)S(1)}, u32[]{:S(2)}, u32[]{:S(2)}) %collective-permute-start.16) | collective-permute-done | bytes 8224 | tf_op jit(solution)/shard_map/ppermute | solution.py:31
  35.3 0.8 %shard_map.175 = (bf16[8,1024]{1,0:T(8,128)(2,1)S(1)}, bf16[4,8,256]{2,1,0:T(8,128)(2,1)S(1)}) custom-call(bf16[8,512]{1,0:T(8,128)(2,1)S(1)} %collective-permute-done.14.refs_0_, bf16[8,512]{1,0:T(8,128)(2,1)S(1)} %collective-permute-done.15.refs_1_, bf16[8,512]{1,0:T(8,128)(2,1)S(1)} %collective-permute-done.16.refs_2_, ...), custom_call_target="tpu_custom_call" | custom-call | flops 1000000000 | tf_op jit(solution)/shard_map/pallas_call | solution.py:193
  37.3 2.3 %collective-permute-start.20 = (bf16[8,256]{1,0:T(8,128)(2,1)S(1)}, bf16[8,256]{1,0:T(8,128)(2,1)S(1)}, u32[]{:S(2)}, u32[]{:S(2)}) collective-permute-start(bf16[8,256]{1,0:T(8,128)(2,1)S(1)} %get-tuple-element.49), channel_id=1, source_target_pairs={{0,7},{1,6},{2,5},{3,4},{4,3},{5,2},{6,1},{7,0},{8,15},{9,14},{10,... | collective-permute-start | bytes 12296 | tf_op jit(solution)/shard_map/ppermute | solution.py:31
  39.6 1.8 %collective-permute-start.18 = (bf16[8,256]{1,0:T(8,128)(2,1)S(1)}, bf16[8,256]{1,0:T(8,128)(2,1)S(1)}, u32[]{:S(2)}, u32[]{:S(2)}) collective-permute-start(bf16[8,256]{1,0:T(8,128)(2,1)S(1)} %get-tuple-element.48), channel_id=1, source_target_pairs={{0,3},{1,2},{2,1},{3,0},{4,7},{5,6},{6,5},{7,4},{8,11},{9,10},{10,... | collective-permute-start | bytes 12296 | tf_op jit(solution)/shard_map/ppermute | solution.py:31
  41.4 1.2 %shard_map.177 = f32[12,128,128]{2,1,0:T(8,128)} custom-call(f32[12,128,128]{2,1,0:T(8,128)S(1)} %bitcast.53, f32[128,128]{1,0:T(8,128)S(1)} %get-tuple-element.40.turned, f32[12,128]{1,0:T(8,128)S(1)} %get-tuple-element.41.write, f32[12,128]{1,0:T(8,128)S(1)} %get-tuple-element.32.refs_3_.retain), custom_call_target="tpu_custom_call" | custom-call | flops 500000000 | tf_op jit(solution)/shard_map/pallas_call | solution.py:193
  42.6 0.9 %collective-permute-done.19 = bf16[8,256]{1,0:T(8,128)(2,1)S(1)} collective-permute-done((bf16[8,256]{1,0:T(8,128)(2,1)S(1)}, bf16[8,256]{1,0:T(8,128)(2,1)S(1)}, u32[]{:S(2)}, u32[]{:S(2)}) %collective-permute-start.19) | collective-permute-done | bytes 4128 | tf_op jit(solution)/shard_map/ppermute | solution.py:31
  43.5 0.6 %fusion.4 = bf16[8,256]{1,0:T(8,128)(2,1)} fusion(f32[4,8,256]{2,1,0:T(8,128)S(1)} %get-tuple-element.47, bf16[8,256]{1,0:T(8,128)(2,1)S(1)} %collective-permute-done.20, bf16[8,256]{1,0:T(8,128)(2,1)S(1)} %collective-permute-done.19, bf16[8,256]{1,0:T(8,128)(2,1)S(1)} %collective-permute-done.18, bf16[8,256]{1,0:T(8,128)(2,1)S(1)} %get-tuple-element.34), kind=kLoop, calls=%fused_computation.8 | loop fusion | flops 18432 | bytes 28672 | tf_op jit(solution)/shard_map/convert_element_type | solution.py:474
  (66 shorter events, 6.5 us)
Async XLA Ops:
  0.7 9.6 %collective-permute-start = (bf16[8,256]{1,0:T(8,128)(2,1)}, bf16[8,256]{1,0:T(8,128)(2,1)S(1)}, u32[]{:S(2)}, u32[]{:S(2)}) collective-permute-start(bf16[8,256]{1,0:T(8,128)(2,1)} %tokens.1), channel_id=1, source_target_pairs={{0,1},{1,0},{2,3},{3,2},{4,5},{5,4},{6,7},{7,6},{8,9},{9,8},{10,11... | collective-permute-start | bytes 12296 | tf_op jit(solution)/shard_map/ppermute | solution.py:36
  1.2 6.2 %collective-permute-start.3 = (bf16[8,256]{1,0:T(8,128)(2,1)}, bf16[8,256]{1,0:T(8,128)(2,1)S(1)}, u32[]{:S(2)}, u32[]{:S(2)}) collective-permute-start(bf16[8,256]{1,0:T(8,128)(2,1)} %tokens.1), channel_id=1, source_target_pairs={{0,7},{1,6},{2,5},{3,4},{4,3},{5,2},{6,1},{7,0},{8,15},{9,14},{10,... | collective-permute-start | bytes 12296 | tf_op jit(solution)/shard_map/ppermute | solution.py:31
  5.9 4.1 %collective-permute-start.2 = (bf16[8,256]{1,0:T(8,128)(2,1)}, bf16[8,256]{1,0:T(8,128)(2,1)S(1)}, u32[]{:S(2)}, u32[]{:S(2)}) collective-permute-start(bf16[8,256]{1,0:T(8,128)(2,1)} %tokens.1), channel_id=1, source_target_pairs={{0,5},{1,4},{2,7},{3,6},{4,1},{5,0},{6,3},{7,2},{8,13},{9,12},{10,... | collective-permute-start | bytes 12296 | tf_op jit(solution)/shard_map/ppermute | solution.py:31
  5.9 4.1 %collective-permute-start.1 = (bf16[8,256]{1,0:T(8,128)(2,1)}, bf16[8,256]{1,0:T(8,128)(2,1)S(1)}, u32[]{:S(2)}, u32[]{:S(2)}) collective-permute-start(bf16[8,256]{1,0:T(8,128)(2,1)} %tokens.1), channel_id=1, source_target_pairs={{0,3},{1,2},{2,1},{3,0},{4,7},{5,6},{6,5},{7,4},{8,11},{9,10},{10,... | collective-permute-start | bytes 12296 | tf_op jit(solution)/shard_map/ppermute | solution.py:31
  6.3 20.6 %collective-permute-start.12 = (bf16[1536,256]{1,0:T(8,128)(2,1)}, bf16[1536,256]{1,0:T(8,128)(2,1)S(1)}, u32[]{:S(2)}, u32[]{:S(2)}) collective-permute-start(bf16[1536,256]{1,0:T(8,128)(2,1)} %refs_3_.1), channel_id=1, source_target_pairs={{0,1},{1,0},{2,3},{3,2},{4,5},{5,4},{6,7},{7,6},{8,9},{9,8},{10,11... | collective-permute-start | bytes 2359304 | tf_op jit(solution)/shard_map/ppermute | solution.py:36
  10.1 1.2 %collective-permute-start.4 = (bf16[3,8,256]{2,1,0:T(8,128)(2,1)S(1)}, bf16[3,8,256]{2,1,0:T(8,128)(2,1)S(1)}, u32[]{:S(2)}, u32[]{:S(2)}) collective-permute-start(bf16[3,8,256]{2,1,0:T(8,128)(2,1)S(1)} %pad_maximum_fusion.1), channel_id=1, source_target_pairs={{0,1},{1,0},{2,3},{3,2},{4,5},{5,4},{6,7},{7,6},{8,9},{9,8},{10,11... | collective-permute-start | bytes 36872 | tf_op jit(solution)/shard_map/ppermute | solution.py:36
  11.8 15.1 %copy-start.7 = (bf16[1536,256]{1,0:T(8,128)(2,1)S(1)}, bf16[1536,256]{1,0:T(8,128)(2,1)}, u32[]{:S(2)}) copy-start(bf16[1536,256]{1,0:T(8,128)(2,1)} %refs_3_.1) | copy-start | bytes 2359300
  11.8 4.9 %collective-permute-start.7 = (f32[2,768]{1,0:T(2,128)S(1)}, f32[2,768]{1,0:T(2,128)S(1)}, u32[]{:S(2)}, u32[]{:S(2)}) collective-permute-start(f32[2,768]{1,0:T(2,128)S(1)} %get-tuple-element.28), channel_id=1, source_target_pairs={{0,7},{1,6},{2,5},{3,4},{4,3},{5,2},{6,1},{7,0},{8,15},{9,14},{10,... | collective-permute-start | bytes 18440 | tf_op jit(solution)/shard_map/ppermute | solution.py:31
  13.1 4.0 %collective-permute-start.6 = (f32[2,768]{1,0:T(2,128)S(1)}, f32[2,768]{1,0:T(2,128)S(1)}, u32[]{:S(2)}, u32[]{:S(2)}) collective-permute-start(f32[2,768]{1,0:T(2,128)S(1)} %get-tuple-element.27), channel_id=1, source_target_pairs={{0,5},{1,4},{2,7},{3,6},{4,1},{5,0},{6,3},{7,2},{8,13},{9,12},{10,... | collective-permute-start | bytes 18440 | tf_op jit(solution)/shard_map/ppermute | solution.py:31
  13.6 3.6 %collective-permute-start.5 = (f32[2,768]{1,0:T(2,128)S(1)}, f32[2,768]{1,0:T(2,128)S(1)}, u32[]{:S(2)}, u32[]{:S(2)}) collective-permute-start(f32[2,768]{1,0:T(2,128)S(1)} %get-tuple-element.26), channel_id=1, source_target_pairs={{0,3},{1,2},{2,1},{3,0},{4,7},{5,6},{6,5},{7,4},{8,11},{9,10},{10,... | collective-permute-start | bytes 18440 | tf_op jit(solution)/shard_map/ppermute | solution.py:31
  17.2 1.3 %collective-permute-start.8 = (f32[4,2,768]{2,1,0:T(2,128)S(1)}, f32[4,2,768]{2,1,0:T(2,128)S(1)}, u32[]{:S(2)}, u32[]{:S(2)}) collective-permute-start(f32[4,2,768]{2,1,0:T(2,128)S(1)} %pad_maximum_fusion.refs_0_), channel_id=1, source_target_pairs={{0,1},{1,0},{2,3},{3,2},{4,5},{5,4},{6,7},{7,6},{8,9},{9,8},{10,11... | collective-permute-start | bytes 73736 | tf_op jit(solution)/shard_map/ppermute | solution.py:36
  19.4 13.2 %copy-start = (bf16[2048,1024]{1,0:T(8,128)(2,1)S(1)}, bf16[2048,1024]{1,0:T(8,128)(2,1)}, u32[]{:S(2)}) copy-start(bf16[2048,1024]{1,0:T(8,128)(2,1)} %refs_6_.1) | copy-start | bytes 12582916
  19.4 13.2 %copy-start.2 = (f32[2048]{0:T(1024)S(1)}, f32[2048]{0:T(1024)}, u32[]{:S(2)}) copy-start(f32[2048]{0:T(1024)} %param.29) | copy-start | bytes 24580
  19.4 4.1 %collective-permute-start.9 = (f32[1,1536]{1,0:T(1,128)S(1)}, f32[1,1536]{1,0:T(1,128)S(1)}, u32[]{:S(2)}, u32[]{:S(2)}) collective-permute-start(f32[1,1536]{1,0:T(1,128)S(1)} %get-tuple-element.33.own), channel_id=1, source_target_pairs={{0,3},{1,2},{2,1},{3,0},{4,7},{5,6},{6,5},{7,4},{8,11},{9,10},{10,... | collective-permute-start | bytes 18440 | tf_op jit(solution)/shard_map/ppermute | solution.py:31
  21.1 4.0 %collective-permute-start.10 = (f32[1,1536]{1,0:T(1,128)S(1)}, f32[1,1536]{1,0:T(1,128)S(1)}, u32[]{:S(2)}, u32[]{:S(2)}) collective-permute-start(f32[1,1536]{1,0:T(1,128)S(1)} %get-tuple-element.33.own), channel_id=1, source_target_pairs={{0,5},{1,4},{2,7},{3,6},{4,1},{5,0},{6,3},{7,2},{8,13},{9,12},{10,... | collective-permute-start | bytes 18440 | tf_op jit(solution)/shard_map/ppermute | solution.py:31
  22.0 4.9 %collective-permute-start.11 = (f32[1,1536]{1,0:T(1,128)S(1)}, f32[1,1536]{1,0:T(1,128)S(1)}, u32[]{:S(2)}, u32[]{:S(2)}) collective-permute-start(f32[1,1536]{1,0:T(1,128)S(1)} %get-tuple-element.33.own), channel_id=1, source_target_pairs={{0,7},{1,6},{2,5},{3,4},{4,3},{5,2},{6,1},{7,0},{8,15},{9,14},{10,... | collective-permute-start | bytes 18440 | tf_op jit(solution)/shard_map/ppermute | solution.py:31
  27.2 1.2 %collective-permute-start.13 = (f32[4,512]{1,0:T(4,128)S(1)}, f32[4,512]{1,0:T(4,128)S(1)}, u32[]{:S(2)}, u32[]{:S(2)}) collective-permute-start(f32[4,512]{1,0:T(4,128)S(1)} %shard_map.172.half), channel_id=1, source_target_pairs={{0,1},{1,0},{2,3},{3,2},{4,5},{5,4},{6,7},{7,6},{8,9},{9,8},{10,11... | collective-permute-start | bytes 24584 | tf_op jit(solution)/shard_map/ppermute | solution.py:36
  28.5 4.4 %collective-permute-start.14 = (bf16[8,512]{1,0:T(8,128)(2,1)S(1)}, bf16[8,512]{1,0:T(8,128)(2,1)S(1)}, u32[]{:S(2)}, u32[]{:S(2)}) collective-permute-start(bf16[8,512]{1,0:T(8,128)(2,1)S(1)} %get-tuple-element.35.block), channel_id=1, source_target_pairs={{0,3},{1,2},{2,1},{3,0},{4,7},{5,6},{6,5},{7,4},{8,11},{9,10},{10,... | collective-permute-start | bytes 24584 | tf_op jit(solution)/shard_map/ppermute | solution.py:31
  28.6 4.3 %collective-permute-start.15 = (bf16[8,512]{1,0:T(8,128)(2,1)S(1)}, bf16[8,512]{1,0:T(8,128)(2,1)S(1)}, u32[]{:S(2)}, u32[]{:S(2)}) collective-permute-start(bf16[8,512]{1,0:T(8,128)(2,1)S(1)} %get-tuple-element.35.block), channel_id=1, source_target_pairs={{0,5},{1,4},{2,7},{3,6},{4,1},{5,0},{6,3},{7,2},{8,13},{9,12},{10,... | collective-permute-start | bytes 24584 | tf_op jit(solution)/shard_map/ppermute | solution.py:31
  30.4 4.9 %collective-permute-start.16 = (bf16[8,512]{1,0:T(8,128)(2,1)S(1)}, bf16[8,512]{1,0:T(8,128)(2,1)S(1)}, u32[]{:S(2)}, u32[]{:S(2)}) collective-permute-start(bf16[8,512]{1,0:T(8,128)(2,1)S(1)} %get-tuple-element.35.block), channel_id=1, source_target_pairs={{0,7},{1,6},{2,5},{3,4},{4,3},{5,2},{6,1},{7,0},{8,15},{9,14},{10,... | collective-permute-start | bytes 24584 | tf_op jit(solution)/shard_map/ppermute | solution.py:31
  36.1 1.2 %collective-permute-start.17 = (bf16[4,8,256]{2,1,0:T(8,128)(2,1)S(1)}, bf16[4,8,256]{2,1,0:T(8,128)(2,1)S(1)}, u32[]{:S(2)}, u32[]{:S(2)}) collective-permute-start(bf16[4,8,256]{2,1,0:T(8,128)(2,1)S(1)} %get-tuple-element.39), channel_id=1, source_target_pairs={{0,1},{1,0},{2,3},{3,2},{4,5},{5,4},{6,7},{7,6},{8,9},{9,8},{10,11... | collective-permute-start | bytes 49160 | tf_op jit(solution)/shard_map/ppermute | solution.py:36
  37.3 5.2 %collective-permute-start.20 = (bf16[8,256]{1,0:T(8,128)(2,1)S(1)}, bf16[8,256]{1,0:T(8,128)(2,1)S(1)}, u32[]{:S(2)}, u32[]{:S(2)}) collective-permute-start(bf16[8,256]{1,0:T(8,128)(2,1)S(1)} %get-tuple-element.49), channel_id=1, source_target_pairs={{0,7},{1,6},{2,5},{3,4},{4,3},{5,2},{6,1},{7,0},{8,15},{9,14},{10,... | collective-permute-start | bytes 12296 | tf_op jit(solution)/shard_map/ppermute | solution.py:31
  39.6 3.9 %collective-permute-start.19 = (bf16[8,256]{1,0:T(8,128)(2,1)S(1)}, bf16[8,256]{1,0:T(8,128)(2,1)S(1)}, u32[]{:S(2)}, u32[]{:S(2)}) collective-permute-start(bf16[8,256]{1,0:T(8,128)(2,1)S(1)} %get-tuple-element.50), channel_id=1, source_target_pairs={{0,5},{1,4},{2,7},{3,6},{4,1},{5,0},{6,3},{7,2},{8,13},{9,12},{10,... | collective-permute-start | bytes 12296 | tf_op jit(solution)/shard_map/ppermute | solution.py:31
  39.6 3.9 %collective-permute-start.18 = (bf16[8,256]{1,0:T(8,128)(2,1)S(1)}, bf16[8,256]{1,0:T(8,128)(2,1)S(1)}, u32[]{:S(2)}, u32[]{:S(2)}) collective-permute-start(bf16[8,256]{1,0:T(8,128)(2,1)S(1)} %get-tuple-element.48), channel_id=1, source_target_pairs={{0,3},{1,2},{2,1},{3,0},{4,7},{5,6},{6,5},{7,4},{8,11},{9,10},{10,... | collective-permute-start | bytes 12296 | tf_op jit(solution)/shard_map/ppermute | solution.py:31
  (13 other events, 113.0 us)

commit v2 on v1

--- a/solution.py
+++ b/solution.py
@@ -250,34 +250,34 @@
     return jnp.sum(jnp.where(there == here, row, 0.0), axis=1, keepdims=True)
 
 
-def own_gates(lifted, scale, w_beta, w_decay, rate, bias, strength, retain):
+def gates(lifted, scale, w_beta, w_decay, rate, bias, *outs):
     heads = w_beta.shape[0]
-    lane = mine_lane(0)
-    scale_own = scale[pl.ds(lane, 1), :][:, :1]
-
-    def own(weight):
-        every = dot_rows(weight[...], lifted[...])
-        here = lax.broadcasted_iota(jnp.int32, every.shape, 1) == lane
-        return jnp.sum(jnp.where(here, every, 0.0), axis=1, keepdims=True) * scale_own
-
-    value = own(w_decay) + column(bias[...], heads)
-    soft = jnp.maximum(value, 0.0) + jnp.log1p(jnp.exp(-jnp.abs(value)))
-    decay = jnp.exp(-column(rate[...], heads) * soft)
-    beta = 1.0 / (1.0 + jnp.exp(-own(w_beta)))
-    strength[...] = jnp.broadcast_to(beta, strength.shape)
-    retain[...] = jnp.broadcast_to(decay, retain.shape)
-
-
-def read_memory(chips, *refs):
-    mine, other, strength, retain, memory, head_gain, mixed, turned_ref, write_ref, parts = refs
+    beta_all, decay_all = dot_rows(w_beta[...], lifted[...]), dot_rows(w_decay[...], lifted[...])
+    bias_column, rate_column = column(bias[...], heads), column(rate[...], heads)
+    for lane, (strength, retain) in ((mine_lane(0), outs[:2]), (other_lane(0), outs[2:])):
+        scale_own = scale[pl.ds(lane, 1), :][:, :1]
+        here = lax.broadcasted_iota(jnp.int32, beta_all.shape, 1) == lane
+
+        def own(every):
+            return jnp.sum(jnp.where(here, every, 0.0), axis=1, keepdims=True) * scale_own
+
+        value = own(decay_all) + bias_column
+        soft = jnp.maximum(value, 0.0) + jnp.log1p(jnp.exp(-jnp.abs(value)))
+        decay = jnp.exp(-rate_column * soft)
+        beta = 1.0 / (1.0 + jnp.exp(-own(beta_all)))
+        strength[...] = jnp.broadcast_to(beta, strength.shape)
+        retain[...] = jnp.broadcast_to(decay, retain.shape)
+
+
+def read_row(chips, row, mine, other, strength, retain, terms, head_gain, parts):
     heads, size = strength.shape
     chip, core = place()
     part = mine.shape[2] // 4
     across = 2 * part // size
     for there in range(chips):
         d = chip ^ there
-        own = mine[d, pl.ds(core, 1), :]
-        partner = other[d, pl.ds(core, 1), :]
+        own = mine[d, pl.ds(row, 1), :]
+        partner = other[d, pl.ds(row, 1), :]
         straight = (d == 0) == (core == 0)
         low = jnp.where(straight, own, partner)
         high = jnp.where(straight, partner, own)
@@ -289,31 +289,53 @@
                 parts[t, h : h + 1, :] = pair[:, i * size : (i + 1) * size]
     query, key, value, gate = parts[0], parts[1], parts[2], parts[3]
     shrink = lax.rsqrt(jnp.sum(key * key, axis=1, keepdims=True) + epsilon)
-    padded = -(-heads // 8) * 8
+    padded = -(-heads // 16) * 16
     pad = [jnp.zeros((padded - heads, size), jnp.float32)] if padded > heads else []
-    rest = jnp.zeros((size - 2 * padded, size), jnp.float32)
-    turned = jnp.concatenate([key, *pad, query, *pad, rest], axis=0).T
-    recalls, reads = [], []
-    for h in range(heads):
-        matrix = memory[h]
-        recalls.append(jnp.sum(matrix * turned[:, h : h + 1], axis=0, keepdims=True))
-        at = padded + h
-        reads.append(jnp.sum(matrix * turned[:, at : at + 1], axis=0, keepdims=True))
-    recall = jnp.concatenate(recalls, axis=0) * shrink
-    read = jnp.concatenate(reads, axis=0)
+    left = jnp.concatenate([key, *pad, query, *pad], axis=0).astype(jnp.bfloat16)
+    at = lax.rem(lax.broadcasted_iota(jnp.int32, (2 * padded, 3 * size), 0), padded)
+    found = sum(jnp.where(at == h, dot(left, terms[h]), 0.0) for h in range(heads))
+    found = found[:, :size] + found[:, size : 2 * size] + found[:, 2 * size :]
+    recall, read = found[:heads] * shrink, found[padded : padded + heads]
     write = shrink * strength[...] * (value - retain[...] * recall)
     readout = retain[...] * read + jnp.sum(key * query, axis=1, keepdims=True) * write
     normed = readout * lax.rsqrt(jnp.mean(readout * readout, axis=1, keepdims=True) + epsilon)
     normed = normed * head_gain[...] * (gate / (1.0 + jnp.exp(-gate)))
-    normed = normed.astype(jnp.bfloat16).astype(jnp.float32)
+    return normed.astype(jnp.bfloat16).astype(jnp.float32), key, write
+
+
+def read_memory(chips, mine, other, *refs):
+    outer, (head_gain, mixed, key_ref, write_ref, parts) = refs[:6], refs[6:]
+    heads, size = key_ref.shape
+    _, core = place()
+    given = ((core, outer[0:3]), (1 - core, outer[3:6]))
+    rows = [
+        read_row(chips, row, mine, other, *three, head_gain, parts.at[i])
+        for i, (row, three) in enumerate(given)
+    ]
+    own, partner = rows[0][0], rows[1][0]
+    ordered = jnp.where(core == 0, own, partner), jnp.where(core == 0, partner, own)
     for h in range(heads):
-        mixed[:, h * size : (h + 1) * size] = normed[h : h + 1]
-    turned_ref[...] = turned
-    write_ref[...] = write
-
-
-def update_memory(memory, turned, write, retain, updated):
+        for c in range(2):
+            mixed[c : c + 1, h * size : (h + 1) * size] = ordered[c][h : h + 1]
+    key_ref[...] = rows[0][1]
+    write_ref[...] = rows[0][2]
+
+
+def split_memory(memory, terms):
+    size = memory.shape[2]
     for h in range(memory.shape[0]):
+        left = memory[h]
+        for i in range(3):
+            term = left.astype(jnp.bfloat16)
+            terms[h, :, i * size : (i + 1) * size] = term
+            left = left - term.astype(jnp.float32)
+
+
+def update_memory(memory, key, write, retain, updated):
+    heads, size = key.shape
+    rest = jnp.zeros((size - heads, size), jnp.float32)
+    turned = jnp.concatenate([key[...], rest], axis=0).T
+    for h in range(heads):
         row = slice(h, h + 1)
         updated[h] = retain[row, :] * memory[h] + turned[:, row] * write[row, :]
 
@@ -325,23 +347,17 @@
 
 
 def mix_out(chips, tokens, partner_tokens, own, *refs):
-    got, (weight, partner_weight, half, rows, wide) = refs[: chips - 1], refs[chips - 1 :]
+    got, (weight, partner_weight, block, middle, rows, wide) = refs[: chips - 1], refs[chips - 1 :]
+    chip, core = place()
     for d in range(chips):
-        rows[d : d + 1, :] = (got[d - 1] if d else own)[...]
+        for c in range(2):
+            rows[pl.ds(2 * (chip ^ d) + c, 1), :] = (got[d - 1] if d else own)[c : c + 1, :]
     left = rows[...].astype(jnp.bfloat16)
     branch = by_core(dot(left, weight[...]), dot(left, partner_weight[...]))
-    wide[...] = by_core(tokens[...].astype(jnp.float32), partner_tokens[...].astype(jnp.float32))
-    for d in range(chips):
-        middle = wide[pl.ds(mine_lane(d), 1), :] + branch[d : d + 1]
-        half[d : d + 1, :] = middle.astype(jnp.bfloat16).astype(jnp.float32)
-
-
-def join_rows(chips, half, other, block, own, rows):
-    for d in range(chips):
-        rows[pl.ds(mine_lane(d), 1), :] = half[d : d + 1, :]
-        rows[pl.ds(other_lane(d), 1), :] = other[d : d + 1, :]
-    block[...] = rows[...].astype(jnp.bfloat16)
-    own[...] = rows[:, span(place()[1], own.shape[1])].astype(jnp.bfloat16)
+    whole = branch + by_core(tokens[...].astype(jnp.float32), partner_tokens[...].astype(jnp.float32))
+    block[...] = whole.astype(jnp.bfloat16)
+    wide[...] = whole
+    middle[...] = wide[:, span(core, middle.shape[1])].astype(jnp.bfloat16)
 
 
 def up_piece(piece, there, gain, weight, parts):
@@ -351,18 +367,19 @@
     parts.append((dot(ready, weight[span(there, size), :]), jnp.sum(wide * wide, axis=1, keepdims=True)))
 
 
-def up_first(block, gain, weight, total, squares):
+def up_first(chips, block, farthest, gain, weight, total, squares):
     parts = []
     up_piece(block[...], place()[0], gain, weight, parts)
-    total[...] = parts[0][0]
-    squares[...] = jnp.broadcast_to(parts[0][1], squares.shape)
+    up_piece(farthest[...], place()[0] ^ (chips - 1), gain, weight, parts)
+    total[...] = sum(part[0] for part in parts)
+    squares[...] = jnp.broadcast_to(sum(part[1] for part in parts), squares.shape)
 
 
 def up_rest(chips, *refs):
-    got, rest = refs[: chips - 1], refs[chips - 1 :]
+    got, rest = refs[: chips - 2], refs[chips - 2 :]
     before, before_squares, gain, weight, down, hidden_ref, leaving = rest
     parts = [(before[...], before_squares[:, :1])]
-    for d in range(1, chips):
+    for d in range(1, chips - 1):
         up_piece(got[d - 1][...], place()[0] ^ d, gain, weight, parts)
     scale = lax.rsqrt(sum(part[1] for part in parts) / gain.shape[1] + epsilon)
     raised = jnp.maximum(sum(part[0] for part in parts) * scale, 0.0)
@@ -423,46 +440,46 @@
         [others, total, squares, lifted, gain_in, *weights],
         [pltpu.VMEM((rows, 4 * part), f32)],
     )
-    strength, retain = call(
-        own_gates,
-        [((heads, size), f32)] * 2,
+    strength, retain, partner_strength, partner_retain = call(
+        gates,
+        [((heads, size), f32)] * 4,
         [lifted, scale_in, w_beta.T, w_decay.T]
         + [value.reshape(1, heads) for value in (decay_rate, decay_bias)],
     )
     mine = jnp.stack(far(leaving, chips))
     matrix = memory.reshape(heads, size, size)
-    mixed, turned, write = call(
+    shape = ((heads, size, 3 * size), bf16)
+    (terms,) = call(split_memory, [shape], [matrix], work=5e8)
+    (partner_terms,) = call(split_memory, [shape], [near(matrix)], work=5e8)
+    mixed, key, write = call(
         functools.partial(read_memory, chips),
-        [((1, heads * size), f32), ((size, size), f32), ((heads, size), f32)],
-        [mine, near(mine), strength, retain, matrix, head_gain.reshape(1, size)],
-        [pltpu.VMEM((4, heads, size), f32)],
+        [((2, heads * size), f32), ((heads, size), f32), ((heads, size), f32)],
+        [mine, near(mine), strength, retain, terms, partner_strength, partner_retain, partner_terms]
+        + [head_gain.reshape(1, size)],
+        [pltpu.VMEM((2, 4, heads, size), f32)],
     )
     (updated,) = call(
-        update_memory, [((heads, size, size), f32)], [matrix, turned, write, retain], work=5e8
+        update_memory, [((heads, size, size), f32)], [matrix, key, write, retain], work=5e8
     )
 
     got = far([mixed] * chips, chips)[1:]
-    (half,) = call(
+    block, middle = call(
         functools.partial(mix_out, chips),
-        [((chips, 2 * features), f32)],
+        [((rows, 2 * features), bf16), ((rows, features), bf16)],
         [tokens, partner, mixed, *got, w_out, near(w_out)],
-        [pltpu.VMEM((chips, heads * size), f32), pltpu.VMEM((rows, 2 * features), f32)],
-    )
-    block, middle = call(
-        functools.partial(join_rows, chips),
-        [((rows, 2 * features), bf16), ((rows, features), bf16)],
-        [half, near(half)],
-        [pltpu.VMEM((rows, 2 * features), f32)],
+        [pltpu.VMEM((rows, heads * size), f32), pltpu.VMEM((rows, 2 * features), f32)],
     )
     got = far([block] * chips, chips)[1:]
     gain_mid = ffn_gain.reshape(1, width)
     total, squares = call(
-        up_first, [((rows, units), f32), ((rows, 128), f32)], [block, gain_mid, w_up]
+        functools.partial(up_first, chips),
+        [((rows, units), f32), ((rows, 128), f32)],
+        [block, got[-1], gain_mid, w_up],
     )
     hidden, leaving = call(
         functools.partial(up_rest, chips),
         [((rows, units), bf16), ((chips, rows, features), bf16)],
-        [*got, total, squares, gain_mid, w_up, w_down],
+        [*got[:-1], total, squares, gain_mid, w_up, w_down],
     )
     arrived = near(leaving)
     (staying,) = call(
@@ -484,7 +501,7 @@
         and arrays[3].shape[1] % 16 == 0
         and 2 * arrays[3].shape[1] % head_gain.shape[0] == 0
         and head_gain.shape[0] == 128
-        and memory.shape[1] <= 32
+        and memory.shape[1] <= 128
     )
     return (kernel_device if fits else plain_device)(chips, *arrays)
 

time: 44.3 us -> 43 us (0.971)
  starting transfers between devices: 23.4 us -> 22.1 us
  waiting for transfers between devices: 13.2 us -> 12.4 us
    ppermute x6, starting transfers between devices: 2.16 us -> 1.46 us  [near(): return lax.ppermute(value, 'tp', [(0, 1), (1, 0)])]
    ppermute x6, waiting for transfers between devices: 2.26 us -> 1.6 us  [near(): return lax.ppermute(value, 'tp', [(0, 1), (1, 0)])]
    ppermute x15, starting transfers between devices: 21.2 us -> 20.7 us  [far(): got.append(lax.ppermute(pieces[d], axes, pairs))]
    pallas_call x11 -> x12, Pallas kernels: 5.34 us -> 5.68 us  [call(): pl.pallas_call(body, out_shape=[jax.ShapeDtypeStruct(shape, kind) for sha...]
  transfers between devices with their start and end apart: 21 -> 21, of which waited for: 13 -> 12; matrix products, arithmetic and copies ran while one was open for 0% -> 0% of each run, Pallas kernels for 9% -> 11%
where the time goes in v2:
time: 43 us; the launch traced here: 42.8 us
  starting transfers between devices  22.1 us (51%)
  waiting for transfers between devices  12.4 us (29%)
  Pallas kernels  5.68 us (13%)
  local copies, waits for them, and re-layouts  1.07 us (2%)
  between operations  0.84 us (2%)
  other arithmetic  0.62 us (1%)
    ppermute x15, starting transfers between devices, far(): got.append(lax.ppermute(pieces[d], axes, pairs))  20.7 us
    ppermute x15, waiting for transfers between devices, far(): got.append(lax.ppermute(pieces[d], axes, pairs))  10.8 us
    pallas_call x12, Pallas kernels, call(): pl.pallas_call(body, out_shape=[jax.ShapeDtypeStruct(shape, kind) for sha...  5.68 us
    ppermute x6, waiting for transfers between devices, near(): return lax.ppermute(value, 'tp', [(0, 1), (1, 0)])  1.6 us
    ppermute x6, starting transfers between devices, near(): return lax.ppermute(value, 'tp', [(0, 1), (1, 0)])  1.46 us
    unnamed x32, local copies, waits for them, and re-layouts  1.06 us
  transfers between devices with their start and end apart: 21, of which 12 were waited for; matrix products, arithmetic and copies ran while one was open for 0% of the time, Pallas kernels for 11%

profile of v2, /device:TPU:0, one launch (start us, length us, event | category | flops | bytes accessed | tf_op | source)
XLA Modules:
  0.0 42.8 jit_solution(9576259789764687543)
XLA Ops:
  0.6 2.6 %collective-permute-start.1 = (bf16[8,256]{1,0:T(8,128)(2,1)}, bf16[8,256]{1,0:T(8,128)(2,1)S(1)}, u32[]{:S(2)}, u32[]{:S(2)}) collective-permute-start(bf16[8,256]{1,0:T(8,128)(2,1)} %tokens.1), channel_id=1, source_target_pairs={{0,3},{1,2},{2,1},{3,0},{4,7},{5,6},{6,5},{7,4},{8,11},{9,10},{10,... | collective-permute-start | bytes 12296 | tf_op jit(solution)/shard_map/ppermute | solution.py:31
  3.2 2.9 %collective-permute-start.2 = (bf16[8,256]{1,0:T(8,128)(2,1)}, bf16[8,256]{1,0:T(8,128)(2,1)S(1)}, u32[]{:S(2)}, u32[]{:S(2)}) collective-permute-start(bf16[8,256]{1,0:T(8,128)(2,1)} %tokens.1), channel_id=1, source_target_pairs={{0,5},{1,4},{2,7},{3,6},{4,1},{5,0},{6,3},{7,2},{8,13},{9,12},{10,... | collective-permute-start | bytes 12296 | tf_op jit(solution)/shard_map/ppermute | solution.py:31
  6.7 1.0 %copy-done.12 = bf16[8,256]{1,0:T(8,128)(2,1)S(1)} copy-done((bf16[8,256]{1,0:T(8,128)(2,1)S(1)}, bf16[8,256]{1,0:T(8,128)(2,1)}, u32[]{:S(2)}) %copy-start.12) | copy-done | bytes 4120
  8.1 3.0 %collective-permute-done.3.refs_2_ = bf16[8,256]{1,0:T(8,128)(2,1)S(1)} collective-permute-done((bf16[8,256]{1,0:T(8,128)(2,1)}, bf16[8,256]{1,0:T(8,128)(2,1)S(1)}, u32[]{:S(2)}, u32[]{:S(2)}) %collective-permute-start.3) | collective-permute-done | bytes 4128 | tf_op jit(solution)/shard_map/ppermute | solution.py:31
  11.3 0.7 %shard_map.168 = (f32[8,768]{1,0:T(8,128)S(1)}, f32[8,128]{1,0:T(8,128)S(1)}, bf16[8,2048]{1,0:T(8,128)(2,1)S(1)}) custom-call(bf16[8,256]{1,0:T(8,128)(2,1)S(1)} %shard_map.167.tokens, bf16[8,256]{1,0:T(8,128)(2,1)S(1)} %collective-permute-done.partner.partner_tokens, bf16[8,256]{1,0:T(8,128)(2,1)S(1)} %collective-permute-done.1.refs_0_, ...), custom_call_target="tpu_custom_call" | custom-call | flops 1000000000 | tf_op jit(solution)/shard_map/pallas_call | solution.py:193
  12.9 1.8 %collective-permute-start.7 = (f32[2,768]{1,0:T(2,128)S(1)}, f32[2,768]{1,0:T(2,128)S(1)}, u32[]{:S(2)}, u32[]{:S(2)}) collective-permute-start(f32[2,768]{1,0:T(2,128)S(1)} %get-tuple-element.30), channel_id=1, source_target_pairs={{0,7},{1,6},{2,5},{3,4},{4,3},{5,2},{6,1},{7,0},{8,15},{9,14},{10,... | collective-permute-start | bytes 18440 | tf_op jit(solution)/shard_map/ppermute | solution.py:31
  14.7 1.2 %collective-permute-start.5 = (f32[2,768]{1,0:T(2,128)S(1)}, f32[2,768]{1,0:T(2,128)S(1)}, u32[]{:S(2)}, u32[]{:S(2)}) collective-permute-start(f32[2,768]{1,0:T(2,128)S(1)} %get-tuple-element.28), channel_id=1, source_target_pairs={{0,3},{1,2},{2,1},{3,0},{4,7},{5,6},{6,5},{7,4},{8,11},{9,10},{10,... | collective-permute-start | bytes 18440 | tf_op jit(solution)/shard_map/ppermute | solution.py:31
  16.8 1.0 %collective-permute-done.7 = f32[2,768]{1,0:T(2,128)S(1)} collective-permute-done((f32[2,768]{1,0:T(2,128)S(1)}, f32[2,768]{1,0:T(2,128)S(1)}, u32[]{:S(2)}, u32[]{:S(2)}) %collective-permute-start.7) | collective-permute-done | bytes 6176 | tf_op jit(solution)/shard_map/ppermute | solution.py:31
  18.3 0.8 %collective-permute-done.8.other = f32[4,2,768]{2,1,0:T(2,128)S(1)} collective-permute-done((f32[4,2,768]{2,1,0:T(2,128)S(1)}, f32[4,2,768]{2,1,0:T(2,128)S(1)}, u32[]{:S(2)}, u32[]{:S(2)}) %collective-permute-start.8) | collective-permute-done | bytes 24608 | tf_op jit(solution)/shard_map/ppermute | solution.py:36
  19.1 0.7 %shard_map.173 = (f32[2,1536]{1,0:T(2,128)S(1)}, f32[12,128]{1,0:T(8,128)S(1)}, f32[12,128]{1,0:T(8,128)S(1)}) custom-call(f32[4,2,768]{2,1,0:T(2,128)S(1)} %pad_maximum_fusion.mine, f32[4,2,768]{2,1,0:T(2,128)S(1)} %collective-permute-done.8.other, f32[12,128]{1,0:T(8,128)S(1)} %get-tuple-element.33.refs_0_, ...), custom_call_target="tpu_custom_call" | custom-call | flops 1000000000 | tf_op jit(solution)/shard_map/pallas_call | solution.py:193
  19.8 1.2 %collective-permute-start.10 = (f32[2,1536]{1,0:T(2,128)S(1)}, f32[2,1536]{1,0:T(2,128)S(1)}, u32[]{:S(2)}, u32[]{:S(2)}) collective-permute-start(f32[2,1536]{1,0:T(2,128)S(1)} %get-tuple-element.37.own), channel_id=1, source_target_pairs={{0,3},{1,2},{2,1},{3,0},{4,7},{5,6},{6,5},{7,4},{8,11},{9,10},{10,... | collective-permute-start | bytes 36872 | tf_op jit(solution)/shard_map/ppermute | solution.py:31
  21.0 1.0 %collective-permute-start.11 = (f32[2,1536]{1,0:T(2,128)S(1)}, f32[2,1536]{1,0:T(2,128)S(1)}, u32[]{:S(2)}, u32[]{:S(2)}) collective-permute-start(f32[2,1536]{1,0:T(2,128)S(1)} %get-tuple-element.37.own), channel_id=1, source_target_pairs={{0,5},{1,4},{2,7},{3,6},{4,1},{5,0},{6,3},{7,2},{8,13},{9,12},{10,... | collective-permute-start | bytes 36872 | tf_op jit(solution)/shard_map/ppermute | solution.py:31
  22.0 1.7 %collective-permute-start.12 = (f32[2,1536]{1,0:T(2,128)S(1)}, f32[2,1536]{1,0:T(2,128)S(1)}, u32[]{:S(2)}, u32[]{:S(2)}) collective-permute-start(f32[2,1536]{1,0:T(2,128)S(1)} %get-tuple-element.37.own), channel_id=1, source_target_pairs={{0,7},{1,6},{2,5},{3,4},{4,3},{5,2},{6,1},{7,0},{8,15},{9,14},{10,... | collective-permute-start | bytes 36872 | tf_op jit(solution)/shard_map/ppermute | solution.py:31
  23.8 1.2 %collective-permute-done.11.refs_1_ = f32[2,1536]{1,0:T(2,128)S(1)} collective-permute-done((f32[2,1536]{1,0:T(2,128)S(1)}, f32[2,1536]{1,0:T(2,128)S(1)}, u32[]{:S(2)}, u32[]{:S(2)}) %collective-permute-start.11) | collective-permute-done | bytes 12320 | tf_op jit(solution)/shard_map/ppermute | solution.py:31
  25.0 1.9 %collective-permute-done.12.refs_2_ = f32[2,1536]{1,0:T(2,128)S(1)} collective-permute-done((f32[2,1536]{1,0:T(2,128)S(1)}, f32[2,1536]{1,0:T(2,128)S(1)}, u32[]{:S(2)}, u32[]{:S(2)}) %collective-permute-start.12) | collective-permute-done | bytes 12320 | tf_op jit(solution)/shard_map/ppermute | solution.py:31
  27.3 1.8 %collective-permute-start.16 = (bf16[8,512]{1,0:T(8,128)(2,1)S(1)}, bf16[8,512]{1,0:T(8,128)(2,1)S(1)}, u32[]{:S(2)}, u32[]{:S(2)}) collective-permute-start(bf16[8,512]{1,0:T(8,128)(2,1)S(1)} %get-tuple-element.39.block), channel_id=1, source_target_pairs={{0,7},{1,6},{2,5},{3,4},{4,3},{5,2},{6,1},{7,0},{8,15},{9,14},{10,... | collective-permute-start | bytes 24584 | tf_op jit(solution)/shard_map/ppermute | solution.py:31
  29.0 2.3 %collective-permute-start.15 = (bf16[8,512]{1,0:T(8,128)(2,1)S(1)}, bf16[8,512]{1,0:T(8,128)(2,1)S(1)}, u32[]{:S(2)}, u32[]{:S(2)}) collective-permute-start(bf16[8,512]{1,0:T(8,128)(2,1)S(1)} %get-tuple-element.39.block), channel_id=1, source_target_pairs={{0,5},{1,4},{2,7},{3,6},{4,1},{5,0},{6,3},{7,2},{8,13},{9,12},{10,... | collective-permute-start | bytes 24584 | tf_op jit(solution)/shard_map/ppermute | solution.py:31
  31.3 0.9 %collective-permute-done.16.farthest = bf16[8,512]{1,0:T(8,128)(2,1)S(1)} collective-permute-done((bf16[8,512]{1,0:T(8,128)(2,1)S(1)}, bf16[8,512]{1,0:T(8,128)(2,1)S(1)}, u32[]{:S(2)}, u32[]{:S(2)}) %collective-permute-start.16) | collective-permute-done | bytes 8224 | tf_op jit(solution)/shard_map/ppermute | solution.py:31
  33.0 0.7 %shard_map.176 = (bf16[8,1024]{1,0:T(8,128)(2,1)S(1)}, bf16[4,8,256]{2,1,0:T(8,128)(2,1)S(1)}) custom-call(bf16[8,512]{1,0:T(8,128)(2,1)S(1)} %collective-permute-done.14.refs_0_, bf16[8,512]{1,0:T(8,128)(2,1)S(1)} %collective-permute-done.15.refs_1_, f32[8,1024]{1,0:T(8,128)S(1)} %get-tuple-element.40.refs_2_, f32[8,128]{1,0:T(8,128)S(1)} %get-tuple-element.41.refs_3_, ...), custom_call_target="tpu_custom_call" | custom-call | flops 1000000000 | tf_op jit(solution)/shard_map/pallas_call | solution.py:193
  34.9 1.8 %collective-permute-start.18 = (bf16[8,256]{1,0:T(8,128)(2,1)S(1)}, bf16[8,256]{1,0:T(8,128)(2,1)S(1)}, u32[]{:S(2)}, u32[]{:S(2)}) collective-permute-start(bf16[8,256]{1,0:T(8,128)(2,1)S(1)} %get-tuple-element.52), channel_id=1, source_target_pairs={{0,3},{1,2},{2,1},{3,0},{4,7},{5,6},{6,5},{7,4},{8,11},{9,10},{10,... | collective-permute-start | bytes 12296 | tf_op jit(solution)/shard_map/ppermute | solution.py:31
  36.7 0.6 %collective-permute-start.19 = (bf16[8,256]{1,0:T(8,128)(2,1)S(1)}, bf16[8,256]{1,0:T(8,128)(2,1)S(1)}, u32[]{:S(2)}, u32[]{:S(2)}) collective-permute-start(bf16[8,256]{1,0:T(8,128)(2,1)S(1)} %get-tuple-element.54), channel_id=1, source_target_pairs={{0,5},{1,4},{2,7},{3,6},{4,1},{5,0},{6,3},{7,2},{8,13},{9,12},{10,... | collective-permute-start | bytes 12296 | tf_op jit(solution)/shard_map/ppermute | solution.py:31
  37.3 1.7 %collective-permute-start.20 = (bf16[8,256]{1,0:T(8,128)(2,1)S(1)}, bf16[8,256]{1,0:T(8,128)(2,1)S(1)}, u32[]{:S(2)}, u32[]{:S(2)}) collective-permute-start(bf16[8,256]{1,0:T(8,128)(2,1)S(1)} %get-tuple-element.53), channel_id=1, source_target_pairs={{0,7},{1,6},{2,5},{3,4},{4,3},{5,2},{6,1},{7,0},{8,15},{9,14},{10,... | collective-permute-start | bytes 12296 | tf_op jit(solution)/shard_map/ppermute | solution.py:31
  39.1 1.3 %shard_map.178 = f32[12,128,128]{2,1,0:T(8,128)} custom-call(f32[12,128,128]{2,1,0:T(8,128)S(1)} %bitcast.40, f32[12,128]{1,0:T(8,128)S(1)} %get-tuple-element.44.key, f32[12,128]{1,0:T(8,128)S(1)} %get-tuple-element.45.write, f32[12,128]{1,0:T(8,128)S(1)} %get-tuple-element.34.refs_1_.retain), custom_call_target="tpu_custom_call" | custom-call | flops 500000000 | tf_op jit(solution)/shard_map/pallas_call | solution.py:193
  40.6 1.5 %collective-permute-done.20 = bf16[8,256]{1,0:T(8,128)(2,1)S(1)} collective-permute-done((bf16[8,256]{1,0:T(8,128)(2,1)S(1)}, bf16[8,256]{1,0:T(8,128)(2,1)S(1)}, u32[]{:S(2)}, u32[]{:S(2)}) %collective-permute-start.20) | collective-permute-done | bytes 4128 | tf_op jit(solution)/shard_map/ppermute | solution.py:31
  (67 shorter events, 6.7 us)
Async XLA Ops:
  0.6 7.3 %collective-permute-start.1 = (bf16[8,256]{1,0:T(8,128)(2,1)}, bf16[8,256]{1,0:T(8,128)(2,1)S(1)}, u32[]{:S(2)}, u32[]{:S(2)}) collective-permute-start(bf16[8,256]{1,0:T(8,128)(2,1)} %tokens.1), channel_id=1, source_target_pairs={{0,3},{1,2},{2,1},{3,0},{4,7},{5,6},{6,5},{7,4},{8,11},{9,10},{10,... | collective-permute-start | bytes 12296 | tf_op jit(solution)/shard_map/ppermute | solution.py:31
  3.2 5.0 %collective-permute-start.2 = (bf16[8,256]{1,0:T(8,128)(2,1)}, bf16[8,256]{1,0:T(8,128)(2,1)S(1)}, u32[]{:S(2)}, u32[]{:S(2)}) collective-permute-start(bf16[8,256]{1,0:T(8,128)(2,1)} %tokens.1), channel_id=1, source_target_pairs={{0,5},{1,4},{2,7},{3,6},{4,1},{5,0},{6,3},{7,2},{8,13},{9,12},{10,... | collective-permute-start | bytes 12296 | tf_op jit(solution)/shard_map/ppermute | solution.py:31
  6.1 5.1 %collective-permute-start.3 = (bf16[8,256]{1,0:T(8,128)(2,1)}, bf16[8,256]{1,0:T(8,128)(2,1)S(1)}, u32[]{:S(2)}, u32[]{:S(2)}) collective-permute-start(bf16[8,256]{1,0:T(8,128)(2,1)} %tokens.1), channel_id=1, source_target_pairs={{0,7},{1,6},{2,5},{3,4},{4,3},{5,2},{6,1},{7,0},{8,15},{9,14},{10,... | collective-permute-start | bytes 12296 | tf_op jit(solution)/shard_map/ppermute | solution.py:31
  6.1 11.9 %collective-permute-start.9 = (f32[12,128,128]{2,1,0:T(8,128)}, f32[12,128,128]{2,1,0:T(8,128)S(1)}, u32[]{:S(2)}, u32[]{:S(2)}) collective-permute-start(f32[12,128,128]{2,1,0:T(8,128)} %bitcast.38), channel_id=1, source_target_pairs={{0,1},{1,0},{2,3},{3,2},{4,5},{5,4},{6,7},{7,6},{8,9},{9,8},{10,11... | collective-permute-start | bytes 2359304 | tf_op jit(solution)/shard_map/ppermute | solution.py:36
  6.2 17.6 %collective-permute-start.13 = (bf16[1536,256]{1,0:T(8,128)(2,1)}, bf16[1536,256]{1,0:T(8,128)(2,1)S(1)}, u32[]{:S(2)}, u32[]{:S(2)}) collective-permute-start(bf16[1536,256]{1,0:T(8,128)(2,1)} %refs_3_.1), channel_id=1, source_target_pairs={{0,1},{1,0},{2,3},{3,2},{4,5},{5,4},{6,7},{7,6},{8,9},{9,8},{10,11... | collective-permute-start | bytes 2359304 | tf_op jit(solution)/shard_map/ppermute | solution.py:36
  7.9 3.3 %collective-permute-start = (bf16[8,256]{1,0:T(8,128)(2,1)S(1)}, bf16[8,256]{1,0:T(8,128)(2,1)S(1)}, u32[]{:S(2)}, u32[]{:S(2)}) collective-permute-start(bf16[8,256]{1,0:T(8,128)(2,1)S(1)} %copy-done.12), channel_id=1, source_target_pairs={{0,1},{1,0},{2,3},{3,2},{4,5},{5,4},{6,7},{7,6},{8,9},{9,8},{10,11... | collective-permute-start | bytes 12296 | tf_op jit(solution)/shard_map/ppermute | solution.py:36
  11.1 1.2 %collective-permute-start.4 = (bf16[3,8,256]{2,1,0:T(8,128)(2,1)S(1)}, bf16[3,8,256]{2,1,0:T(8,128)(2,1)S(1)}, u32[]{:S(2)}, u32[]{:S(2)}) collective-permute-start(bf16[3,8,256]{2,1,0:T(8,128)(2,1)S(1)} %pad_maximum_fusion.1), channel_id=1, source_target_pairs={{0,1},{1,0},{2,3},{3,2},{4,5},{5,4},{6,7},{7,6},{8,9},{9,8},{10,11... | collective-permute-start | bytes 36872 | tf_op jit(solution)/shard_map/ppermute | solution.py:36
  12.8 4.0 %collective-permute-start.6 = (f32[2,768]{1,0:T(2,128)S(1)}, f32[2,768]{1,0:T(2,128)S(1)}, u32[]{:S(2)}, u32[]{:S(2)}) collective-permute-start(f32[2,768]{1,0:T(2,128)S(1)} %get-tuple-element.29), channel_id=1, source_target_pairs={{0,5},{1,4},{2,7},{3,6},{4,1},{5,0},{6,3},{7,2},{8,13},{9,12},{10,... | collective-permute-start | bytes 18440 | tf_op jit(solution)/shard_map/ppermute | solution.py:31
  12.9 4.9 %collective-permute-start.7 = (f32[2,768]{1,0:T(2,128)S(1)}, f32[2,768]{1,0:T(2,128)S(1)}, u32[]{:S(2)}, u32[]{:S(2)}) collective-permute-start(f32[2,768]{1,0:T(2,128)S(1)} %get-tuple-element.30), channel_id=1, source_target_pairs={{0,7},{1,6},{2,5},{3,4},{4,3},{5,2},{6,1},{7,0},{8,15},{9,14},{10,... | collective-permute-start | bytes 18440 | tf_op jit(solution)/shard_map/ppermute | solution.py:31
  14.7 3.1 %collective-permute-start.5 = (f32[2,768]{1,0:T(2,128)S(1)}, f32[2,768]{1,0:T(2,128)S(1)}, u32[]{:S(2)}, u32[]{:S(2)}) collective-permute-start(f32[2,768]{1,0:T(2,128)S(1)} %get-tuple-element.28), channel_id=1, source_target_pairs={{0,3},{1,2},{2,1},{3,0},{4,7},{5,6},{6,5},{7,4},{8,11},{9,10},{10,... | collective-permute-start | bytes 18440 | tf_op jit(solution)/shard_map/ppermute | solution.py:31
  17.8 1.3 %collective-permute-start.8 = (f32[4,2,768]{2,1,0:T(2,128)S(1)}, f32[4,2,768]{2,1,0:T(2,128)S(1)}, u32[]{:S(2)}, u32[]{:S(2)}) collective-permute-start(f32[4,2,768]{2,1,0:T(2,128)S(1)} %pad_maximum_fusion.mine), channel_id=1, source_target_pairs={{0,1},{1,0},{2,3},{3,2},{4,5},{5,4},{6,7},{7,6},{8,9},{9,8},{10,11... | collective-permute-start | bytes 73736 | tf_op jit(solution)/shard_map/ppermute | solution.py:36
  18.3 13.9 %copy-start = (bf16[2048,1024]{1,0:T(8,128)(2,1)S(1)}, bf16[2048,1024]{1,0:T(8,128)(2,1)}, u32[]{:S(2)}) copy-start(bf16[2048,1024]{1,0:T(8,128)(2,1)} %refs_5_.1) | copy-start | bytes 12582916
  18.3 13.9 %copy-start.3 = (f32[2048]{0:T(1024)S(1)}, f32[2048]{0:T(1024)}, u32[]{:S(2)}) copy-start(f32[2048]{0:T(1024)} %param.29) | copy-start | bytes 24580
  19.8 13.2 %copy-start.1 = (bf16[1024,2048]{1,0:T(8,128)(2,1)S(1)}, bf16[1024,2048]{1,0:T(8,128)(2,1)}, u32[]{:S(2)}) copy-start(bf16[1024,2048]{1,0:T(8,128)(2,1)} %down.1) | copy-start | bytes 12582916
  19.8 3.9 %collective-permute-start.10 = (f32[2,1536]{1,0:T(2,128)S(1)}, f32[2,1536]{1,0:T(2,128)S(1)}, u32[]{:S(2)}, u32[]{:S(2)}) collective-permute-start(f32[2,1536]{1,0:T(2,128)S(1)} %get-tuple-element.37.own), channel_id=1, source_target_pairs={{0,3},{1,2},{2,1},{3,0},{4,7},{5,6},{6,5},{7,4},{8,11},{9,10},{10,... | collective-permute-start | bytes 36872 | tf_op jit(solution)/shard_map/ppermute | solution.py:31
  21.0 4.0 %collective-permute-start.11 = (f32[2,1536]{1,0:T(2,128)S(1)}, f32[2,1536]{1,0:T(2,128)S(1)}, u32[]{:S(2)}, u32[]{:S(2)}) collective-permute-start(f32[2,1536]{1,0:T(2,128)S(1)} %get-tuple-element.37.own), channel_id=1, source_target_pairs={{0,5},{1,4},{2,7},{3,6},{4,1},{5,0},{6,3},{7,2},{8,13},{9,12},{10,... | collective-permute-start | bytes 36872 | tf_op jit(solution)/shard_map/ppermute | solution.py:31
  22.0 4.9 %collective-permute-start.12 = (f32[2,1536]{1,0:T(2,128)S(1)}, f32[2,1536]{1,0:T(2,128)S(1)}, u32[]{:S(2)}, u32[]{:S(2)}) collective-permute-start(f32[2,1536]{1,0:T(2,128)S(1)} %get-tuple-element.37.own), channel_id=1, source_target_pairs={{0,7},{1,6},{2,5},{3,4},{4,3},{5,2},{6,1},{7,0},{8,15},{9,14},{10,... | collective-permute-start | bytes 36872 | tf_op jit(solution)/shard_map/ppermute | solution.py:31
  27.3 4.9 %collective-permute-start.16 = (bf16[8,512]{1,0:T(8,128)(2,1)S(1)}, bf16[8,512]{1,0:T(8,128)(2,1)S(1)}, u32[]{:S(2)}, u32[]{:S(2)}) collective-permute-start(bf16[8,512]{1,0:T(8,128)(2,1)S(1)} %get-tuple-element.39.block), channel_id=1, source_target_pairs={{0,7},{1,6},{2,5},{3,4},{4,3},{5,2},{6,1},{7,0},{8,15},{9,14},{10,... | collective-permute-start | bytes 24584 | tf_op jit(solution)/shard_map/ppermute | solution.py:31
  29.0 3.5 %collective-permute-start.14 = (bf16[8,512]{1,0:T(8,128)(2,1)S(1)}, bf16[8,512]{1,0:T(8,128)(2,1)S(1)}, u32[]{:S(2)}, u32[]{:S(2)}) collective-permute-start(bf16[8,512]{1,0:T(8,128)(2,1)S(1)} %get-tuple-element.39.block), channel_id=1, source_target_pairs={{0,3},{1,2},{2,1},{3,0},{4,7},{5,6},{6,5},{7,4},{8,11},{9,10},{10,... | collective-permute-start | bytes 24584 | tf_op jit(solution)/shard_map/ppermute | solution.py:31
  29.0 4.0 %collective-permute-start.15 = (bf16[8,512]{1,0:T(8,128)(2,1)S(1)}, bf16[8,512]{1,0:T(8,128)(2,1)S(1)}, u32[]{:S(2)}, u32[]{:S(2)}) collective-permute-start(bf16[8,512]{1,0:T(8,128)(2,1)S(1)} %get-tuple-element.39.block), channel_id=1, source_target_pairs={{0,5},{1,4},{2,7},{3,6},{4,1},{5,0},{6,3},{7,2},{8,13},{9,12},{10,... | collective-permute-start | bytes 24584 | tf_op jit(solution)/shard_map/ppermute | solution.py:31
  33.7 1.2 %collective-permute-start.17 = (bf16[4,8,256]{2,1,0:T(8,128)(2,1)S(1)}, bf16[4,8,256]{2,1,0:T(8,128)(2,1)S(1)}, u32[]{:S(2)}, u32[]{:S(2)}) collective-permute-start(bf16[4,8,256]{2,1,0:T(8,128)(2,1)S(1)} %get-tuple-element.43), channel_id=1, source_target_pairs={{0,1},{1,0},{2,3},{3,2},{4,5},{5,4},{6,7},{7,6},{8,9},{9,8},{10,11... | collective-permute-start | bytes 49160 | tf_op jit(solution)/shard_map/ppermute | solution.py:36
  34.9 5.5 %collective-permute-start.18 = (bf16[8,256]{1,0:T(8,128)(2,1)S(1)}, bf16[8,256]{1,0:T(8,128)(2,1)S(1)}, u32[]{:S(2)}, u32[]{:S(2)}) collective-permute-start(bf16[8,256]{1,0:T(8,128)(2,1)S(1)} %get-tuple-element.52), channel_id=1, source_target_pairs={{0,3},{1,2},{2,1},{3,0},{4,7},{5,6},{6,5},{7,4},{8,11},{9,10},{10,... | collective-permute-start | bytes 12296 | tf_op jit(solution)/shard_map/ppermute | solution.py:31
  36.7 3.9 %collective-permute-start.19 = (bf16[8,256]{1,0:T(8,128)(2,1)S(1)}, bf16[8,256]{1,0:T(8,128)(2,1)S(1)}, u32[]{:S(2)}, u32[]{:S(2)}) collective-permute-start(bf16[8,256]{1,0:T(8,128)(2,1)S(1)} %get-tuple-element.54), channel_id=1, source_target_pairs={{0,5},{1,4},{2,7},{3,6},{4,1},{5,0},{6,3},{7,2},{8,13},{9,12},{10,... | collective-permute-start | bytes 12296 | tf_op jit(solution)/shard_map/ppermute | solution.py:31
  37.3 4.8 %collective-permute-start.20 = (bf16[8,256]{1,0:T(8,128)(2,1)S(1)}, bf16[8,256]{1,0:T(8,128)(2,1)S(1)}, u32[]{:S(2)}, u32[]{:S(2)}) collective-permute-start(bf16[8,256]{1,0:T(8,128)(2,1)S(1)} %get-tuple-element.53), channel_id=1, source_target_pairs={{0,7},{1,6},{2,5},{3,4},{4,3},{5,2},{6,1},{7,0},{8,15},{9,14},{10,... | collective-permute-start | bytes 12296 | tf_op jit(solution)/shard_map/ppermute | solution.py:31
  (13 other events, 78.1 us)

commit v3 on v2

--- a/solution.py
+++ b/solution.py
@@ -30,6 +30,19 @@
         pairs = [(i, i ^ (2 * d + 1)) for i in range(2 * chips)]
         got.append(lax.ppermute(pieces[d], axes, pairs))
     return got
+
+
+def shared(piece, chips):
+    falling = list(range(chips - 1, 0, -1))
+    direct, passed = [], []
+    for at in range(0, len(falling), 2):
+        far_one, less = falling[at], falling[min(at + 1, len(falling) - 1)]
+        pairs = [(i, i ^ (2 * (far_one if i % 2 else less))) for i in range(2 * chips)]
+        got = lax.ppermute(piece, axes, pairs)
+        direct.append((got, (less, far_one)))
+        if less != far_one:
+            passed.append((near(got), (far_one, less)))
+    return direct, passed
 
 
 def near(value):
@@ -292,9 +305,9 @@
     padded = -(-heads // 16) * 16
     pad = [jnp.zeros((padded - heads, size), jnp.float32)] if padded > heads else []
     left = jnp.concatenate([key, *pad, query, *pad], axis=0).astype(jnp.bfloat16)
-    at = lax.rem(lax.broadcasted_iota(jnp.int32, (2 * padded, 3 * size), 0), padded)
+    at = lax.rem(lax.broadcasted_iota(jnp.int32, (2 * padded, 2 * size), 0), padded)
     found = sum(jnp.where(at == h, dot(left, terms[h]), 0.0) for h in range(heads))
-    found = found[:, :size] + found[:, size : 2 * size] + found[:, 2 * size :]
+    found = found[:, :size] + found[:, size:]
     recall, read = found[:heads] * shrink, found[padded : padded + heads]
     write = shrink * strength[...] * (value - retain[...] * recall)
     readout = retain[...] * read + jnp.sum(key * query, axis=1, keepdims=True) * write
@@ -325,7 +338,7 @@
     size = memory.shape[2]
     for h in range(memory.shape[0]):
         left = memory[h]
-        for i in range(3):
+        for i in range(2):
             term = left.astype(jnp.bfloat16)
             terms[h, :, i * size : (i + 1) * size] = term
             left = left - term.astype(jnp.float32)
@@ -346,41 +359,49 @@
     return jnp.concatenate([low, high], axis=-1)
 
 
-def mix_out(chips, tokens, partner_tokens, own, *refs):
-    got, (weight, partner_weight, block, middle, rows, wide) = refs[: chips - 1], refs[chips - 1 :]
+def chip_at(distance):
     chip, core = place()
-    for d in range(chips):
+    return chip ^ jnp.where(core == 0, distance[0], distance[1])
+
+
+def mix_out(distances, tokens, partner_tokens, *refs):
+    count = len(distances)
+    got, (weight, partner_weight, block, middle, rows, wide) = refs[:count], refs[count:]
+    for piece, distance in zip(got, distances):
         for c in range(2):
-            rows[pl.ds(2 * (chip ^ d) + c, 1), :] = (got[d - 1] if d else own)[c : c + 1, :]
+            rows[pl.ds(2 * chip_at(distance) + c, 1), :] = piece[c : c + 1, :]
     left = rows[...].astype(jnp.bfloat16)
     branch = by_core(dot(left, weight[...]), dot(left, partner_weight[...]))
     whole = branch + by_core(tokens[...].astype(jnp.float32), partner_tokens[...].astype(jnp.float32))
     block[...] = whole.astype(jnp.bfloat16)
     wide[...] = whole
-    middle[...] = wide[:, span(core, middle.shape[1])].astype(jnp.bfloat16)
-
-
-def up_piece(piece, there, gain, weight, parts):
-    size = piece.shape[1]
-    wide = piece.astype(jnp.float32)
-    ready = (wide * gain[:, span(there, size)]).astype(jnp.bfloat16)
-    parts.append((dot(ready, weight[span(there, size), :]), jnp.sum(wide * wide, axis=1, keepdims=True)))
-
-
-def up_first(chips, block, farthest, gain, weight, total, squares):
+    middle[...] = wide[:, span(place()[1], middle.shape[1])].astype(jnp.bfloat16)
+
+
+def up_pieces(got, distances, gain, weight, parts):
+    for piece, distance in zip(got, distances):
+        size, there = piece.shape[1], chip_at(distance)
+        wide = piece[...].astype(jnp.float32)
+        ready = (wide * gain[:, span(there, size)]).astype(jnp.bfloat16)
+        squares = jnp.sum(wide * wide, axis=1, keepdims=True)
+        parts.append((dot(ready, weight[span(there, size), :]), squares))
+
+
+def up_first(distances, *refs):
+    count = len(distances)
+    got, (gain, weight, total, squares) = refs[:count], refs[count:]
     parts = []
-    up_piece(block[...], place()[0], gain, weight, parts)
-    up_piece(farthest[...], place()[0] ^ (chips - 1), gain, weight, parts)
+    up_pieces(got, distances, gain, weight, parts)
     total[...] = sum(part[0] for part in parts)
     squares[...] = jnp.broadcast_to(sum(part[1] for part in parts), squares.shape)
 
 
-def up_rest(chips, *refs):
-    got, rest = refs[: chips - 2], refs[chips - 2 :]
-    before, before_squares, gain, weight, down, hidden_ref, leaving = rest
-    parts = [(before[...], before_squares[:, :1])]
-    for d in range(1, chips - 1):
-        up_piece(got[d - 1][...], place()[0] ^ d, gain, weight, parts)
+def up_rest(chips, distances, *refs):
+    count = len(distances)
+    got, rest = refs[:count], refs[count:]
+    *before, gain, weight, down, hidden_ref, leaving = rest
+    parts = [(a[...], b[:, :1]) for a, b in zip(before[::2], before[1::2])]
+    up_pieces(got, distances, gain, weight, parts)
     scale = lax.rsqrt(sum(part[1] for part in parts) / gain.shape[1] + epsilon)
     raised = jnp.maximum(sum(part[0] for part in parts) * scale, 0.0)
     hidden = (raised * raised).astype(jnp.bfloat16)
@@ -448,7 +469,7 @@
     )
     mine = jnp.stack(far(leaving, chips))
     matrix = memory.reshape(heads, size, size)
-    shape = ((heads, size, 3 * size), bf16)
+    shape = ((heads, size, 2 * size), bf16)
     (terms,) = call(split_memory, [shape], [matrix], work=5e8)
     (partner_terms,) = call(split_memory, [shape], [near(matrix)], work=5e8)
     mixed, key, write = call(
@@ -462,24 +483,27 @@
         update_memory, [((heads, size, size), f32)], [matrix, key, write, retain], work=5e8
     )
 
-    got = far([mixed] * chips, chips)[1:]
+    here = (0, 0)
+    direct, passed = shared(mixed, chips)
+    got, distances = zip((mixed, here), *direct, *passed)
     block, middle = call(
-        functools.partial(mix_out, chips),
+        functools.partial(mix_out, distances),
         [((rows, 2 * features), bf16), ((rows, features), bf16)],
-        [tokens, partner, mixed, *got, w_out, near(w_out)],
+        [tokens, partner, *got, w_out, near(w_out)],
         [pltpu.VMEM((rows, heads * size), f32), pltpu.VMEM((rows, 2 * features), f32)],
     )
-    got = far([block] * chips, chips)[1:]
+
+    direct, passed = shared(block, chips)
     gain_mid = ffn_gain.reshape(1, width)
-    total, squares = call(
-        functools.partial(up_first, chips),
-        [((rows, units), f32), ((rows, 128), f32)],
-        [block, got[-1], gain_mid, w_up],
-    )
+    sums = [((rows, units), f32), ((rows, 128), f32)]
+    early = []
+    for piece, distance in [(block, here), *direct[:-1]]:
+        early += call(functools.partial(up_first, [distance]), sums, [piece, gain_mid, w_up])
+    got, distances = zip(direct[-1], *passed)
     hidden, leaving = call(
-        functools.partial(up_rest, chips),
+        functools.partial(up_rest, chips, distances),
         [((rows, units), bf16), ((chips, rows, features), bf16)],
-        [*got[:-1], total, squares, gain_mid, w_up, w_down],
+        [*got, *early, gain_mid, w_up, w_down],
     )
     arrived = near(leaving)
     (staying,) = call(

time: 43 us -> 41.3 us (0.960)
  starting transfers between devices: 22.1 us -> 18.7 us
  waiting for transfers between devices: 12.4 us -> 14.6 us
    ppermute x15 -> x9, starting transfers between devices: 20.7 us -> 12.4 us  [far(): got.append(lax.ppermute(pieces[d], axes, pairs))]
    ppermute x0 -> x4, waiting for transfers between devices: none -> 5.22 us  [shared(): got = lax.ppermute(piece, axes, pairs)]
    ppermute x0 -> x4, starting transfers between devices: none -> 4.97 us  [shared(): got = lax.ppermute(piece, axes, pairs)]
    ppermute x15 -> x9, waiting for transfers between devices: 10.8 us -> 6.52 us  [far(): got.append(lax.ppermute(pieces[d], axes, pairs))]
    ppermute x6 -> x8, waiting for transfers between devices: 1.6 us -> 2.82 us  [near(): return lax.ppermute(value, 'tp', [(0, 1), (1, 0)])]
    pallas_call x12 -> x13, Pallas kernels: 5.68 us -> 5.39 us  [call(): pl.pallas_call(body, out_shape=[jax.ShapeDtypeStruct(shape, kind) for sha...]
    ppermute x6 -> x8, starting transfers between devices: 1.46 us -> 1.28 us  [near(): return lax.ppermute(value, 'tp', [(0, 1), (1, 0)])]
  transfers between devices with their start and end apart: 21 -> 21, of which waited for: 12 -> 13; matrix products, arithmetic and copies ran while one was open for 0% -> 0% of each run, Pallas kernels for 11% -> 11%
where the time goes in v3:
time: 41.3 us; the launch traced here: 41.1 us
  starting transfers between devices  18.7 us (45%)
  waiting for transfers between devices  14.6 us (35%)
  Pallas kernels  5.39 us (13%)
  local copies, waits for them, and re-layouts  1.07 us (3%)
  between operations  0.83 us (2%)
  other arithmetic  0.63 us (2%)
    ppermute x9, starting transfers between devices, far(): got.append(lax.ppermute(pieces[d], axes, pairs))  12.4 us
    ppermute x9, waiting for transfers between devices, far(): got.append(lax.ppermute(pieces[d], axes, pairs))  6.52 us
    pallas_call x13, Pallas kernels, call(): pl.pallas_call(body, out_shape=[jax.ShapeDtypeStruct(shape, kind) for sha...  5.39 us
    ppermute x4, waiting for transfers between devices, shared(): got = lax.ppermute(piece, axes, pairs)  5.22 us
    ppermute x4, starting transfers between devices, shared(): got = lax.ppermute(piece, axes, pairs)  4.97 us
    ppermute x8, waiting for transfers between devices, near(): return lax.ppermute(value, 'tp', [(0, 1), (1, 0)])  2.82 us
    ppermute x8, starting transfers between devices, near(): return lax.ppermute(value, 'tp', [(0, 1), (1, 0)])  1.28 us
    unnamed x32, local copies, waits for them, and re-layouts  1.06 us
  transfers between devices with their start and end apart: 21, of which 13 were waited for; matrix products, arithmetic and copies ran while one was open for 0% of the time, Pallas kernels for 11%

profile of v3, /device:TPU:0, one launch (start us, length us, event | category | flops | bytes accessed | tf_op | source)
XLA Modules:
  0.0 41.1 jit_solution(9764006574546029208)
XLA Ops:
  0.6 2.6 %collective-permute-start.1 = (bf16[8,256]{1,0:T(8,128)(2,1)}, bf16[8,256]{1,0:T(8,128)(2,1)S(1)}, u32[]{:S(2)}, u32[]{:S(2)}) collective-permute-start(bf16[8,256]{1,0:T(8,128)(2,1)} %tokens.1), channel_id=1, source_target_pairs={{0,3},{1,2},{2,1},{3,0},{4,7},{5,6},{6,5},{7,4},{8,11},{9,10},{10,... | collective-permute-start | bytes 12296 | tf_op jit(solution)/shard_map/ppermute | solution.py:31
  3.2 2.9 %collective-permute-start.2 = (bf16[8,256]{1,0:T(8,128)(2,1)}, bf16[8,256]{1,0:T(8,128)(2,1)S(1)}, u32[]{:S(2)}, u32[]{:S(2)}) collective-permute-start(bf16[8,256]{1,0:T(8,128)(2,1)} %tokens.1), channel_id=1, source_target_pairs={{0,5},{1,4},{2,7},{3,6},{4,1},{5,0},{6,3},{7,2},{8,13},{9,12},{10,... | collective-permute-start | bytes 12296 | tf_op jit(solution)/shard_map/ppermute | solution.py:31
  6.7 1.0 %copy-done.12 = bf16[8,256]{1,0:T(8,128)(2,1)S(1)} copy-done((bf16[8,256]{1,0:T(8,128)(2,1)S(1)}, bf16[8,256]{1,0:T(8,128)(2,1)}, u32[]{:S(2)}) %copy-start.12) | copy-done | bytes 4120
  8.1 3.1 %collective-permute-done.3.refs_2_ = bf16[8,256]{1,0:T(8,128)(2,1)S(1)} collective-permute-done((bf16[8,256]{1,0:T(8,128)(2,1)}, bf16[8,256]{1,0:T(8,128)(2,1)S(1)}, u32[]{:S(2)}, u32[]{:S(2)}) %collective-permute-start.3) | collective-permute-done | bytes 4128 | tf_op jit(solution)/shard_map/ppermute | solution.py:31
  11.3 0.7 %shard_map.168 = (f32[8,768]{1,0:T(8,128)S(1)}, f32[8,128]{1,0:T(8,128)S(1)}, bf16[8,2048]{1,0:T(8,128)(2,1)S(1)}) custom-call(bf16[8,256]{1,0:T(8,128)(2,1)S(1)} %shard_map.167.tokens, bf16[8,256]{1,0:T(8,128)(2,1)S(1)} %collective-permute-done.partner.partner_tokens, bf16[8,256]{1,0:T(8,128)(2,1)S(1)} %collective-permute-done.1.refs_0_, ...), custom_call_target="tpu_custom_call" | custom-call | flops 1000000000 | tf_op jit(solution)/shard_map/pallas_call | solution.py:206
  12.9 1.8 %collective-permute-start.7 = (f32[2,768]{1,0:T(2,128)S(1)}, f32[2,768]{1,0:T(2,128)S(1)}, u32[]{:S(2)}, u32[]{:S(2)}) collective-permute-start(f32[2,768]{1,0:T(2,128)S(1)} %get-tuple-element.32), channel_id=1, source_target_pairs={{0,7},{1,6},{2,5},{3,4},{4,3},{5,2},{6,1},{7,0},{8,15},{9,14},{10,... | collective-permute-start | bytes 18440 | tf_op jit(solution)/shard_map/ppermute | solution.py:31
  14.7 1.2 %collective-permute-start.5 = (f32[2,768]{1,0:T(2,128)S(1)}, f32[2,768]{1,0:T(2,128)S(1)}, u32[]{:S(2)}, u32[]{:S(2)}) collective-permute-start(f32[2,768]{1,0:T(2,128)S(1)} %get-tuple-element.30), channel_id=1, source_target_pairs={{0,3},{1,2},{2,1},{3,0},{4,7},{5,6},{6,5},{7,4},{8,11},{9,10},{10,... | collective-permute-start | bytes 18440 | tf_op jit(solution)/shard_map/ppermute | solution.py:31
  16.2 0.6 %collective-permute-done.6 = f32[2,768]{1,0:T(2,128)S(1)} collective-permute-done((f32[2,768]{1,0:T(2,128)S(1)}, f32[2,768]{1,0:T(2,128)S(1)}, u32[]{:S(2)}, u32[]{:S(2)}) %collective-permute-start.6) | collective-permute-done | bytes 6176 | tf_op jit(solution)/shard_map/ppermute | solution.py:31
  16.8 1.0 %collective-permute-done.7 = f32[2,768]{1,0:T(2,128)S(1)} collective-permute-done((f32[2,768]{1,0:T(2,128)S(1)}, f32[2,768]{1,0:T(2,128)S(1)}, u32[]{:S(2)}, u32[]{:S(2)}) %collective-permute-start.7) | collective-permute-done | bytes 6176 | tf_op jit(solution)/shard_map/ppermute | solution.py:31
  18.2 0.9 %collective-permute-done.8.other = f32[4,2,768]{2,1,0:T(2,128)S(1)} collective-permute-done((f32[4,2,768]{2,1,0:T(2,128)S(1)}, f32[4,2,768]{2,1,0:T(2,128)S(1)}, u32[]{:S(2)}, u32[]{:S(2)}) %collective-permute-start.8) | collective-permute-done | bytes 24608 | tf_op jit(solution)/shard_map/ppermute | solution.py:49
  19.6 1.7 %collective-permute-start.10 = (f32[2,1536]{1,0:T(2,128)S(1)}, f32[2,1536]{1,0:T(2,128)S(1)}, u32[]{:S(2)}, u32[]{:S(2)}) collective-permute-start(f32[2,1536]{1,0:T(2,128)S(1)} %get-tuple-element.39.refs_0_), channel_id=1, source_target_pairs={{0,4},{1,7},{2,6},{3,5},{4,0},{5,3},{6,2},{7,1},{8,12},{9,15},{10,... | collective-permute-start | bytes 36872 | tf_op jit(solution)/shard_map/ppermute | solution.py:41
  21.3 0.8 %collective-permute-start.11 = (f32[2,1536]{1,0:T(2,128)S(1)}, f32[2,1536]{1,0:T(2,128)S(1)}, u32[]{:S(2)}, u32[]{:S(2)}) collective-permute-start(f32[2,1536]{1,0:T(2,128)S(1)} %get-tuple-element.39.refs_0_), channel_id=1, source_target_pairs={{0,2},{1,3},{2,0},{3,1},{4,6},{5,7},{6,4},{7,5},{8,10},{9,11},{10,... | collective-permute-start | bytes 36872 | tf_op jit(solution)/shard_map/ppermute | solution.py:41
  22.1 2.2 %collective-permute-done.10.refs_1_ = f32[2,1536]{1,0:T(2,128)S(1)} collective-permute-done((f32[2,1536]{1,0:T(2,128)S(1)}, f32[2,1536]{1,0:T(2,128)S(1)}, u32[]{:S(2)}, u32[]{:S(2)}) %collective-permute-start.10) | collective-permute-done | bytes 12320 | tf_op jit(solution)/shard_map/ppermute | solution.py:41
  24.3 0.7 %collective-permute-done.11.refs_2_ = f32[2,1536]{1,0:T(2,128)S(1)} collective-permute-done((f32[2,1536]{1,0:T(2,128)S(1)}, f32[2,1536]{1,0:T(2,128)S(1)}, u32[]{:S(2)}, u32[]{:S(2)}) %collective-permute-start.11) | collective-permute-done | bytes 12320 | tf_op jit(solution)/shard_map/ppermute | solution.py:41
  25.8 1.6 %collective-permute-start.15 = (bf16[8,512]{1,0:T(8,128)(2,1)S(1)}, bf16[8,512]{1,0:T(8,128)(2,1)S(1)}, u32[]{:S(2)}, u32[]{:S(2)}) collective-permute-start(bf16[8,512]{1,0:T(8,128)(2,1)S(1)} %get-tuple-element.41.refs_0_), channel_id=1, source_target_pairs={{0,4},{1,7},{2,6},{3,5},{4,0},{5,3},{6,2},{7,1},{8,12},{9,15},{10,... | collective-permute-start | bytes 24584 | tf_op jit(solution)/shard_map/ppermute | solution.py:41
  27.4 0.9 %collective-permute-start.14 = (bf16[8,512]{1,0:T(8,128)(2,1)S(1)}, bf16[8,512]{1,0:T(8,128)(2,1)S(1)}, u32[]{:S(2)}, u32[]{:S(2)}) collective-permute-start(bf16[8,512]{1,0:T(8,128)(2,1)S(1)} %get-tuple-element.41.refs_0_), channel_id=1, source_target_pairs={{0,2},{1,3},{2,0},{3,1},{4,6},{5,7},{6,4},{7,5},{8,10},{9,11},{10,... | collective-permute-start | bytes 24584 | tf_op jit(solution)/shard_map/ppermute | solution.py:41
  28.6 1.8 %collective-permute-done.15.refs_0_ = bf16[8,512]{1,0:T(8,128)(2,1)S(1)} collective-permute-done((bf16[8,512]{1,0:T(8,128)(2,1)S(1)}, bf16[8,512]{1,0:T(8,128)(2,1)S(1)}, u32[]{:S(2)}, u32[]{:S(2)}) %collective-permute-start.15) | collective-permute-done | bytes 8224 | tf_op jit(solution)/shard_map/ppermute | solution.py:41
  31.6 0.7 %shard_map.177 = (bf16[8,1024]{1,0:T(8,128)(2,1)S(1)}, bf16[4,8,256]{2,1,0:T(8,128)(2,1)S(1)}) custom-call(bf16[8,512]{1,0:T(8,128)(2,1)S(1)} %collective-permute-done.14.refs_0_, bf16[8,512]{1,0:T(8,128)(2,1)S(1)} %collective-permute-done.16.refs_1_, f32[8,1024]{1,0:T(8,128)S(1)} %get-tuple-element.42.refs_2_, f32[8,128]{1,0:T(8,128)S(1)} %get-tuple-element.43.refs_3_, ...), custom_call_target="tpu_custom_call" | custom-call | flops 1000000000 | tf_op jit(solution)/shard_map/pallas_call | solution.py:206
  32.8 0.6 %collective-permute-done.17 = bf16[4,8,256]{2,1,0:T(8,128)(2,1)S(1)} collective-permute-done((bf16[4,8,256]{2,1,0:T(8,128)(2,1)S(1)}, bf16[4,8,256]{2,1,0:T(8,128)(2,1)S(1)}, u32[]{:S(2)}, u32[]{:S(2)}) %collective-permute-start.17) | collective-permute-done | bytes 16416 | tf_op jit(solution)/shard_map/ppermute | solution.py:49
  33.5 1.1 %collective-permute-start.18 = (bf16[8,256]{1,0:T(8,128)(2,1)S(1)}, bf16[8,256]{1,0:T(8,128)(2,1)S(1)}, u32[]{:S(2)}, u32[]{:S(2)}) collective-permute-start(bf16[8,256]{1,0:T(8,128)(2,1)S(1)} %get-tuple-element.56), channel_id=1, source_target_pairs={{0,3},{1,2},{2,1},{3,0},{4,7},{5,6},{6,5},{7,4},{8,11},{9,10},{10,... | collective-permute-start | bytes 12296 | tf_op jit(solution)/shard_map/ppermute | solution.py:31
  34.6 1.1 %collective-permute-start.19 = (bf16[8,256]{1,0:T(8,128)(2,1)S(1)}, bf16[8,256]{1,0:T(8,128)(2,1)S(1)}, u32[]{:S(2)}, u32[]{:S(2)}) collective-permute-start(bf16[8,256]{1,0:T(8,128)(2,1)S(1)} %get-tuple-element.58), channel_id=1, source_target_pairs={{0,5},{1,4},{2,7},{3,6},{4,1},{5,0},{6,3},{7,2},{8,13},{9,12},{10,... | collective-permute-start | bytes 12296 | tf_op jit(solution)/shard_map/ppermute | solution.py:31
  35.7 1.7 %collective-permute-start.20 = (bf16[8,256]{1,0:T(8,128)(2,1)S(1)}, bf16[8,256]{1,0:T(8,128)(2,1)S(1)}, u32[]{:S(2)}, u32[]{:S(2)}) collective-permute-start(bf16[8,256]{1,0:T(8,128)(2,1)S(1)} %get-tuple-element.57), channel_id=1, source_target_pairs={{0,7},{1,6},{2,5},{3,4},{4,3},{5,2},{6,1},{7,0},{8,15},{9,14},{10,... | collective-permute-start | bytes 12296 | tf_op jit(solution)/shard_map/ppermute | solution.py:31
  37.4 1.3 %shard_map.179 = f32[12,128,128]{2,1,0:T(8,128)} custom-call(f32[12,128,128]{2,1,0:T(8,128)S(1)} %bitcast.55, f32[12,128]{1,0:T(8,128)S(1)} %get-tuple-element.48.key, f32[12,128]{1,0:T(8,128)S(1)} %get-tuple-element.49.write, f32[12,128]{1,0:T(8,128)S(1)} %get-tuple-element.36.refs_1_.retain), custom_call_target="tpu_custom_call" | custom-call | flops 500000000 | tf_op jit(solution)/shard_map/pallas_call | solution.py:206
  38.7 1.8 %collective-permute-done.20 = bf16[8,256]{1,0:T(8,128)(2,1)S(1)} collective-permute-done((bf16[8,256]{1,0:T(8,128)(2,1)S(1)}, bf16[8,256]{1,0:T(8,128)(2,1)S(1)}, u32[]{:S(2)}, u32[]{:S(2)}) %collective-permute-start.20) | collective-permute-done | bytes 4128 | tf_op jit(solution)/shard_map/ppermute | solution.py:31
  (68 shorter events, 6.6 us)
Async XLA Ops:
  0.6 7.2 %collective-permute-start.1 = (bf16[8,256]{1,0:T(8,128)(2,1)}, bf16[8,256]{1,0:T(8,128)(2,1)S(1)}, u32[]{:S(2)}, u32[]{:S(2)}) collective-permute-start(bf16[8,256]{1,0:T(8,128)(2,1)} %tokens.1), channel_id=1, source_target_pairs={{0,3},{1,2},{2,1},{3,0},{4,7},{5,6},{6,5},{7,4},{8,11},{9,10},{10,... | collective-permute-start | bytes 12296 | tf_op jit(solution)/shard_map/ppermute | solution.py:31
  3.2 4.9 %collective-permute-start.2 = (bf16[8,256]{1,0:T(8,128)(2,1)}, bf16[8,256]{1,0:T(8,128)(2,1)S(1)}, u32[]{:S(2)}, u32[]{:S(2)}) collective-permute-start(bf16[8,256]{1,0:T(8,128)(2,1)} %tokens.1), channel_id=1, source_target_pairs={{0,5},{1,4},{2,7},{3,6},{4,1},{5,0},{6,3},{7,2},{8,13},{9,12},{10,... | collective-permute-start | bytes 12296 | tf_op jit(solution)/shard_map/ppermute | solution.py:31
  6.1 5.1 %collective-permute-start.3 = (bf16[8,256]{1,0:T(8,128)(2,1)}, bf16[8,256]{1,0:T(8,128)(2,1)S(1)}, u32[]{:S(2)}, u32[]{:S(2)}) collective-permute-start(bf16[8,256]{1,0:T(8,128)(2,1)} %tokens.1), channel_id=1, source_target_pairs={{0,7},{1,6},{2,5},{3,4},{4,3},{5,2},{6,1},{7,0},{8,15},{9,14},{10,... | collective-permute-start | bytes 12296 | tf_op jit(solution)/shard_map/ppermute | solution.py:31
  6.1 12.0 %collective-permute-start.9 = (f32[12,128,128]{2,1,0:T(8,128)}, f32[12,128,128]{2,1,0:T(8,128)S(1)}, u32[]{:S(2)}, u32[]{:S(2)}) collective-permute-start(f32[12,128,128]{2,1,0:T(8,128)} %bitcast.53), channel_id=1, source_target_pairs={{0,1},{1,0},{2,3},{3,2},{4,5},{5,4},{6,7},{7,6},{8,9},{9,8},{10,11... | collective-permute-start | bytes 2359304 | tf_op jit(solution)/shard_map/ppermute | solution.py:49
  6.2 18.1 %collective-permute-start.13 = (bf16[1536,256]{1,0:T(8,128)(2,1)}, bf16[1536,256]{1,0:T(8,128)(2,1)S(1)}, u32[]{:S(2)}, u32[]{:S(2)}) collective-permute-start(bf16[1536,256]{1,0:T(8,128)(2,1)} %refs_4_.1), channel_id=1, source_target_pairs={{0,1},{1,0},{2,3},{3,2},{4,5},{5,4},{6,7},{7,6},{8,9},{9,8},{10,11... | collective-permute-start | bytes 2359304 | tf_op jit(solution)/shard_map/ppermute | solution.py:49
  7.9 3.4 %collective-permute-start = (bf16[8,256]{1,0:T(8,128)(2,1)S(1)}, bf16[8,256]{1,0:T(8,128)(2,1)S(1)}, u32[]{:S(2)}, u32[]{:S(2)}) collective-permute-start(bf16[8,256]{1,0:T(8,128)(2,1)S(1)} %copy-done.12), channel_id=1, source_target_pairs={{0,1},{1,0},{2,3},{3,2},{4,5},{5,4},{6,7},{7,6},{8,9},{9,8},{10,11... | collective-permute-start | bytes 12296 | tf_op jit(solution)/shard_map/ppermute | solution.py:49
  11.1 1.2 %collective-permute-start.4 = (bf16[3,8,256]{2,1,0:T(8,128)(2,1)S(1)}, bf16[3,8,256]{2,1,0:T(8,128)(2,1)S(1)}, u32[]{:S(2)}, u32[]{:S(2)}) collective-permute-start(bf16[3,8,256]{2,1,0:T(8,128)(2,1)S(1)} %pad_maximum_fusion.1), channel_id=1, source_target_pairs={{0,1},{1,0},{2,3},{3,2},{4,5},{5,4},{6,7},{7,6},{8,9},{9,8},{10,11... | collective-permute-start | bytes 36872 | tf_op jit(solution)/shard_map/ppermute | solution.py:49
  12.8 4.0 %collective-permute-start.6 = (f32[2,768]{1,0:T(2,128)S(1)}, f32[2,768]{1,0:T(2,128)S(1)}, u32[]{:S(2)}, u32[]{:S(2)}) collective-permute-start(f32[2,768]{1,0:T(2,128)S(1)} %get-tuple-element.31), channel_id=1, source_target_pairs={{0,5},{1,4},{2,7},{3,6},{4,1},{5,0},{6,3},{7,2},{8,13},{9,12},{10,... | collective-permute-start | bytes 18440 | tf_op jit(solution)/shard_map/ppermute | solution.py:31
  12.9 4.9 %collective-permute-start.7 = (f32[2,768]{1,0:T(2,128)S(1)}, f32[2,768]{1,0:T(2,128)S(1)}, u32[]{:S(2)}, u32[]{:S(2)}) collective-permute-start(f32[2,768]{1,0:T(2,128)S(1)} %get-tuple-element.32), channel_id=1, source_target_pairs={{0,7},{1,6},{2,5},{3,4},{4,3},{5,2},{6,1},{7,0},{8,15},{9,14},{10,... | collective-permute-start | bytes 18440 | tf_op jit(solution)/shard_map/ppermute | solution.py:31
  14.7 3.1 %collective-permute-start.5 = (f32[2,768]{1,0:T(2,128)S(1)}, f32[2,768]{1,0:T(2,128)S(1)}, u32[]{:S(2)}, u32[]{:S(2)}) collective-permute-start(f32[2,768]{1,0:T(2,128)S(1)} %get-tuple-element.30), channel_id=1, source_target_pairs={{0,3},{1,2},{2,1},{3,0},{4,7},{5,6},{6,5},{7,4},{8,11},{9,10},{10,... | collective-permute-start | bytes 18440 | tf_op jit(solution)/shard_map/ppermute | solution.py:31
  15.8 9.6 %copy-start.7 = (bf16[1536,256]{1,0:T(8,128)(2,1)S(1)}, bf16[1536,256]{1,0:T(8,128)(2,1)}, u32[]{:S(2)}) copy-start(bf16[1536,256]{1,0:T(8,128)(2,1)} %refs_4_.1) | copy-start | bytes 2359300
  17.8 10.5 %copy-start = (bf16[2048,1024]{1,0:T(8,128)(2,1)S(1)}, bf16[2048,1024]{1,0:T(8,128)(2,1)}, u32[]{:S(2)}) copy-start(bf16[2048,1024]{1,0:T(8,128)(2,1)} %refs_7_.1) | copy-start | bytes 12582916
  17.8 10.5 %copy-start.2 = (f32[2048]{0:T(1024)S(1)}, f32[2048]{0:T(1024)}, u32[]{:S(2)}) copy-start(f32[2048]{0:T(1024)} %param.29) | copy-start | bytes 24580
  17.8 1.3 %collective-permute-start.8 = (f32[4,2,768]{2,1,0:T(2,128)S(1)}, f32[4,2,768]{2,1,0:T(2,128)S(1)}, u32[]{:S(2)}, u32[]{:S(2)}) collective-permute-start(f32[4,2,768]{2,1,0:T(2,128)S(1)} %pad_maximum_fusion.mine), channel_id=1, source_target_pairs={{0,1},{1,0},{2,3},{3,2},{4,5},{5,4},{6,7},{7,6},{8,9},{9,8},{10,11... | collective-permute-start | bytes 73736 | tf_op jit(solution)/shard_map/ppermute | solution.py:49
  19.6 4.7 %collective-permute-start.10 = (f32[2,1536]{1,0:T(2,128)S(1)}, f32[2,1536]{1,0:T(2,128)S(1)}, u32[]{:S(2)}, u32[]{:S(2)}) collective-permute-start(f32[2,1536]{1,0:T(2,128)S(1)} %get-tuple-element.39.refs_0_), channel_id=1, source_target_pairs={{0,4},{1,7},{2,6},{3,5},{4,0},{5,3},{6,2},{7,1},{8,12},{9,15},{10,... | collective-permute-start | bytes 36872 | tf_op jit(solution)/shard_map/ppermute | solution.py:41
  21.3 3.7 %collective-permute-start.11 = (f32[2,1536]{1,0:T(2,128)S(1)}, f32[2,1536]{1,0:T(2,128)S(1)}, u32[]{:S(2)}, u32[]{:S(2)}) collective-permute-start(f32[2,1536]{1,0:T(2,128)S(1)} %get-tuple-element.39.refs_0_), channel_id=1, source_target_pairs={{0,2},{1,3},{2,0},{3,1},{4,6},{5,7},{6,4},{7,5},{8,10},{9,11},{10,... | collective-permute-start | bytes 36872 | tf_op jit(solution)/shard_map/ppermute | solution.py:41
  24.3 1.2 %collective-permute-start.12 = (f32[2,1536]{1,0:T(2,128)S(1)}, f32[2,1536]{1,0:T(2,128)S(1)}, u32[]{:S(2)}, u32[]{:S(2)}) collective-permute-start(f32[2,1536]{1,0:T(2,128)S(1)} %collective-permute-done.10.refs_1_), channel_id=1, source_target_pairs={{0,1},{1,0},{2,3},{3,2},{4,5},{5,4},{6,7},{7,6},{8,9},{9,8},{10,11... | collective-permute-start | bytes 36872 | tf_op jit(solution)/shard_map/ppermute | solution.py:49
  25.8 4.6 %collective-permute-start.15 = (bf16[8,512]{1,0:T(8,128)(2,1)S(1)}, bf16[8,512]{1,0:T(8,128)(2,1)S(1)}, u32[]{:S(2)}, u32[]{:S(2)}) collective-permute-start(bf16[8,512]{1,0:T(8,128)(2,1)S(1)} %get-tuple-element.41.refs_0_), channel_id=1, source_target_pairs={{0,4},{1,7},{2,6},{3,5},{4,0},{5,3},{6,2},{7,1},{8,12},{9,15},{10,... | collective-permute-start | bytes 24584 | tf_op jit(solution)/shard_map/ppermute | solution.py:41
  27.4 3.7 %collective-permute-start.14 = (bf16[8,512]{1,0:T(8,128)(2,1)S(1)}, bf16[8,512]{1,0:T(8,128)(2,1)S(1)}, u32[]{:S(2)}, u32[]{:S(2)}) collective-permute-start(bf16[8,512]{1,0:T(8,128)(2,1)S(1)} %get-tuple-element.41.refs_0_), channel_id=1, source_target_pairs={{0,2},{1,3},{2,0},{3,1},{4,6},{5,7},{6,4},{7,5},{8,10},{9,11},{10,... | collective-permute-start | bytes 24584 | tf_op jit(solution)/shard_map/ppermute | solution.py:41
  30.4 1.2 %collective-permute-start.16 = (bf16[8,512]{1,0:T(8,128)(2,1)S(1)}, bf16[8,512]{1,0:T(8,128)(2,1)S(1)}, u32[]{:S(2)}, u32[]{:S(2)}) collective-permute-start(bf16[8,512]{1,0:T(8,128)(2,1)S(1)} %collective-permute-done.15.refs_0_), channel_id=1, source_target_pairs={{0,1},{1,0},{2,3},{3,2},{4,5},{5,4},{6,7},{7,6},{8,9},{9,8},{10,11... | collective-permute-start | bytes 24584 | tf_op jit(solution)/shard_map/ppermute | solution.py:49
  32.2 1.2 %collective-permute-start.17 = (bf16[4,8,256]{2,1,0:T(8,128)(2,1)S(1)}, bf16[4,8,256]{2,1,0:T(8,128)(2,1)S(1)}, u32[]{:S(2)}, u32[]{:S(2)}) collective-permute-start(bf16[4,8,256]{2,1,0:T(8,128)(2,1)S(1)} %get-tuple-element.47), channel_id=1, source_target_pairs={{0,1},{1,0},{2,3},{3,2},{4,5},{5,4},{6,7},{7,6},{8,9},{9,8},{10,11... | collective-permute-start | bytes 49160 | tf_op jit(solution)/shard_map/ppermute | solution.py:49
  33.5 5.2 %collective-permute-start.18 = (bf16[8,256]{1,0:T(8,128)(2,1)S(1)}, bf16[8,256]{1,0:T(8,128)(2,1)S(1)}, u32[]{:S(2)}, u32[]{:S(2)}) collective-permute-start(bf16[8,256]{1,0:T(8,128)(2,1)S(1)} %get-tuple-element.56), channel_id=1, source_target_pairs={{0,3},{1,2},{2,1},{3,0},{4,7},{5,6},{6,5},{7,4},{8,11},{9,10},{10,... | collective-permute-start | bytes 12296 | tf_op jit(solution)/shard_map/ppermute | solution.py:31
  34.6 4.1 %collective-permute-start.19 = (bf16[8,256]{1,0:T(8,128)(2,1)S(1)}, bf16[8,256]{1,0:T(8,128)(2,1)S(1)}, u32[]{:S(2)}, u32[]{:S(2)}) collective-permute-start(bf16[8,256]{1,0:T(8,128)(2,1)S(1)} %get-tuple-element.58), channel_id=1, source_target_pairs={{0,5},{1,4},{2,7},{3,6},{4,1},{5,0},{6,3},{7,2},{8,13},{9,12},{10,... | collective-permute-start | bytes 12296 | tf_op jit(solution)/shard_map/ppermute | solution.py:31
  35.7 4.8 %collective-permute-start.20 = (bf16[8,256]{1,0:T(8,128)(2,1)S(1)}, bf16[8,256]{1,0:T(8,128)(2,1)S(1)}, u32[]{:S(2)}, u32[]{:S(2)}) collective-permute-start(bf16[8,256]{1,0:T(8,128)(2,1)S(1)} %get-tuple-element.57), channel_id=1, source_target_pairs={{0,7},{1,6},{2,5},{3,4},{4,3},{5,2},{6,1},{7,0},{8,15},{9,14},{10,... | collective-permute-start | bytes 12296 | tf_op jit(solution)/shard_map/ppermute | solution.py:31
  (13 other events, 70.7 us)

commit v4 on v3

--- a/solution.py
+++ b/solution.py
@@ -241,7 +241,7 @@
 
 
 def project_rest(chips, others, before, before_squares, before_lifted, gain, *rest):
-    weights, (scale_ref, lifted, *leaving), sent = rest[:4], rest[4:-1], rest[-1]
+    weights, (scale_ref, lifted, early, farthest), sent = rest[:4], rest[4:-1], rest[-1]
     lifted[...] = before_lifted[...]
     parts = [(before[...], before_squares[:, :1])]
     for d in range(1, chips):
@@ -254,7 +254,11 @@
     chip, _ = place()
     for d in range(chips):
         for c in range(2):
-            leaving[d][c : c + 1, :] = sent[pl.ds(2 * (chip ^ d) + c, 1), :]
+            row = sent[pl.ds(2 * (chip ^ d) + c, 1), :]
+            if d < chips - 1:
+                early[d, c : c + 1, :] = row
+            else:
+                farthest[c : c + 1, :] = row
 
 
 def column(row, heads):
@@ -399,7 +403,7 @@
 def up_rest(chips, distances, *refs):
     count = len(distances)
     got, rest = refs[:count], refs[count:]
-    *before, gain, weight, down, hidden_ref, leaving = rest
+    *before, gain, weight, down, hidden_ref, leaving, farthest = rest
     parts = [(a[...], b[:, :1]) for a, b in zip(before[::2], before[1::2])]
     up_pieces(got, distances, gain, weight, parts)
     scale = lax.rsqrt(sum(part[1] for part in parts) / gain.shape[1] + epsilon)
@@ -407,14 +411,25 @@
     hidden = (raised * raised).astype(jnp.bfloat16)
     hidden_ref[...] = hidden
     size = leaving.shape[2]
-    for d in range(chips):
+    for d in range(chips - 1):
         leaving[d] = dot(hidden, down[:, span(other_lane(d), size)]).astype(jnp.bfloat16)
+    across = span(place()[0] ^ (chips - 1), 2 * size)
+    farthest[...] = dot(hidden, down[:, across]).astype(jnp.bfloat16)
 
 
 def down_own(chips, hidden, down, staying):
     size = staying.shape[2]
-    for d in range(chips):
+    for d in range(chips - 1):
         staying[d] = dot(hidden[...], down[:, span(mine_lane(d), size)])
+
+
+def add_up(middle, own, farthest, passed, *refs):
+    *got, out = refs
+    half = span(place()[1], out.shape[1])
+    total = own[...]
+    for piece in (farthest[:, half], passed[:, half], *(piece[...] for piece in got)):
+        total = total + piece.astype(jnp.float32)
+    out[...] = (middle[...].astype(jnp.float32) + total).astype(jnp.bfloat16)
 
 
 def kernel_device(
@@ -455,9 +470,10 @@
         [((rows, 4 * part), f32), ((rows, 128), f32), ((rows, width), bf16)],
         [tokens, partner, *got, gain_in, *weights],
     )
-    scale_in, lifted, *leaving = call(
+    scale_in, lifted, early, farthest = call(
         functools.partial(project_rest, chips),
-        [((rows, 128), f32), ((rows, width), bf16)] + [((2, 4 * part), f32)] * chips,
+        [((rows, 128), f32), ((rows, width), bf16)]
+        + [((chips - 1, 2, 4 * part), f32), ((2, 4 * part), f32)],
         [others, total, squares, lifted, gain_in, *weights],
         [pltpu.VMEM((rows, 4 * part), f32)],
     )
@@ -467,15 +483,20 @@
         [lifted, scale_in, w_beta.T, w_decay.T]
         + [value.reshape(1, heads) for value in (decay_rate, decay_bias)],
     )
-    mine = jnp.stack(far(leaving, chips))
+    passed = near(early)
+    both = [jnp.stack([early[d], passed[d]]) for d in range(chips - 1)]
+    got = far(both + [farthest], chips)
+    mine = jnp.stack([piece[0] for piece in got[:-1]] + [got[-1]])
+    other = jnp.stack([piece[1] for piece in got[:-1]] + [near(got[-1])])
     matrix = memory.reshape(heads, size, size)
     shape = ((heads, size, 2 * size), bf16)
     (terms,) = call(split_memory, [shape], [matrix], work=5e8)
-    (partner_terms,) = call(split_memory, [shape], [near(matrix)], work=5e8)
+    moved = near(matrix)
+    (partner_terms,) = call(split_memory, [shape], [moved], work=5e8)
     mixed, key, write = call(
         functools.partial(read_memory, chips),
         [((2, heads * size), f32), ((heads, size), f32), ((heads, size), f32)],
-        [mine, near(mine), strength, retain, terms, partner_strength, partner_retain, partner_terms]
+        [mine, other, strength, retain, terms, partner_strength, partner_retain, partner_terms]
         + [head_gain.reshape(1, size)],
         [pltpu.VMEM((2, 4, heads, size), f32)],
     )
@@ -500,19 +521,25 @@
     for piece, distance in [(block, here), *direct[:-1]]:
         early += call(functools.partial(up_first, [distance]), sums, [piece, gain_mid, w_up])
     got, distances = zip(direct[-1], *passed)
-    hidden, leaving = call(
+    hidden, leaving, farthest = call(
         functools.partial(up_rest, chips, distances),
-        [((rows, units), bf16), ((chips, rows, features), bf16)],
+        [((rows, units), bf16), ((chips - 1, rows, features), bf16), ((rows, 2 * features), bf16)],
         [*got, *early, gain_mid, w_up, w_down],
     )
     arrived = near(leaving)
     (staying,) = call(
-        functools.partial(down_own, chips), [((chips, rows, features), f32)], [hidden, w_down]
+        functools.partial(down_own, chips),
+        [((chips - 1, rows, features), f32)],
+        [hidden, w_down],
     )
     sums = staying + arrived.astype(f32)
-    terms = far([sums[0]] + [sums[d].astype(bf16) for d in range(1, chips)], chips)
-    down = sum(term.astype(f32) for term in terms)
-    layer_out = (middle.astype(f32) + down).astype(bf16)
+    terms = [sums[d].astype(bf16) for d in range(chips - 1)] + [farthest]
+    *got, farthest = far(terms, chips)[1:]
+    (layer_out,) = call(
+        add_up,
+        [((rows, features), bf16)],
+        [middle, sums[0], farthest, near(farthest), *got],
+    )
     return (layer_out, updated.reshape(memory.shape))
 
 

time: 41.3 us -> 46.6 us (1.13)
  waiting for transfers between devices: 14.6 us -> 18.6 us
  starting transfers between devices: 18.7 us -> 19.7 us
  Pallas kernels: 5.39 us -> 6.1 us
  other arithmetic: 0.63 us -> 0.06 us
    ppermute x9, waiting for transfers between devices: 6.52 us -> 13.3 us  [far(): got.append(lax.ppermute(pieces[d], axes, pairs))]
    ppermute x8 -> x10, waiting for transfers between devices: 2.82 us -> 0.55 us  [near(): return lax.ppermute(value, 'tp', [(0, 1), (1, 0)])]
    ppermute x8 -> x10, starting transfers between devices: 1.28 us -> 2.93 us  [near(): return lax.ppermute(value, 'tp', [(0, 1), (1, 0)])]
    pallas_call x13 -> x14, Pallas kernels: 5.39 us -> 6.1 us  [call(): pl.pallas_call(body, out_shape=[jax.ShapeDtypeStruct(shape, kind) for sha...]
    convert_element_type x1 -> x0, other arithmetic: 0.6 us -> none  [kernel_device(): layer_out = (middle.astype(f32) + down).astype(bf16)]
  transfers between devices with their start and end apart: 21 -> 23, of which waited for: 13 -> 12; matrix products, arithmetic and copies ran while one was open for 0% -> 0% of each run, Pallas kernels for 11% -> 9%
where the time goes in v4:
time: 46.6 us; the launch traced here: 46.4 us
  starting transfers between devices  19.7 us (42%)
  waiting for transfers between devices  18.6 us (40%)
  Pallas kernels  6.1 us (13%)
  local copies, waits for them, and re-layouts  1.04 us (2%)
  between operations  0.89 us (2%)
    ppermute x9, waiting for transfers between devices, far(): got.append(lax.ppermute(pieces[d], axes, pairs))  13.3 us
    ppermute x9, starting transfers between devices, far(): got.append(lax.ppermute(pieces[d], axes, pairs))  12.2 us
    pallas_call x14, Pallas kernels, call(): pl.pallas_call(body, out_shape=[jax.ShapeDtypeStruct(shape, kind) for sha...  6.1 us
    ppermute x4, waiting for transfers between devices, shared(): got = lax.ppermute(piece, axes, pairs)  4.77 us
    ppermute x4, starting transfers between devices, shared(): got = lax.ppermute(piece, axes, pairs)  4.58 us
    ppermute x10, starting transfers between devices, near(): return lax.ppermute(value, 'tp', [(0, 1), (1, 0)])  2.93 us
    unnamed x32, local copies, waits for them, and re-layouts  1.02 us
  transfers between devices with their start and end apart: 23, of which 12 were waited for; matrix products, arithmetic and copies ran while one was open for 0% of the time, Pallas kernels for 9%

profile of v4, /device:TPU:0, one launch (start us, length us, event | category | flops | bytes accessed | tf_op | source)
XLA Modules:
  0.0 46.4 jit_solution(7862652004107372275)
XLA Ops:
  0.6 0.6 %collective-permute-start = (bf16[8,256]{1,0:T(8,128)(2,1)}, bf16[8,256]{1,0:T(8,128)(2,1)S(1)}, u32[]{:S(2)}, u32[]{:S(2)}) collective-permute-start(bf16[8,256]{1,0:T(8,128)(2,1)} %tokens.1), channel_id=1, source_target_pairs={{0,1},{1,0},{2,3},{3,2},{4,5},{5,4},{6,7},{7,6},{8,9},{9,8},{10,11... | collective-permute-start | bytes 12296 | tf_op jit(solution)/shard_map/ppermute | solution.py:49
  1.2 2.7 %collective-permute-start.1 = (bf16[8,256]{1,0:T(8,128)(2,1)}, bf16[8,256]{1,0:T(8,128)(2,1)S(1)}, u32[]{:S(2)}, u32[]{:S(2)}) collective-permute-start(bf16[8,256]{1,0:T(8,128)(2,1)} %tokens.1), channel_id=1, source_target_pairs={{0,3},{1,2},{2,1},{3,0},{4,7},{5,6},{6,5},{7,4},{8,11},{9,10},{10,... | collective-permute-start | bytes 12296 | tf_op jit(solution)/shard_map/ppermute | solution.py:31
  3.9 2.3 %collective-permute-start.2 = (bf16[8,256]{1,0:T(8,128)(2,1)}, bf16[8,256]{1,0:T(8,128)(2,1)S(1)}, u32[]{:S(2)}, u32[]{:S(2)}) collective-permute-start(bf16[8,256]{1,0:T(8,128)(2,1)} %tokens.1), channel_id=1, source_target_pairs={{0,5},{1,4},{2,7},{3,6},{4,1},{5,0},{6,3},{7,2},{8,13},{9,12},{10,... | collective-permute-start | bytes 12296 | tf_op jit(solution)/shard_map/ppermute | solution.py:31
  6.7 0.9 %copy-done.12 = bf16[8,256]{1,0:T(8,128)(2,1)S(1)} copy-done((bf16[8,256]{1,0:T(8,128)(2,1)S(1)}, bf16[8,256]{1,0:T(8,128)(2,1)}, u32[]{:S(2)}) %copy-start.12) | copy-done | bytes 4120
  8.0 3.2 %collective-permute-done.3.refs_2_ = bf16[8,256]{1,0:T(8,128)(2,1)S(1)} collective-permute-done((bf16[8,256]{1,0:T(8,128)(2,1)}, bf16[8,256]{1,0:T(8,128)(2,1)S(1)}, u32[]{:S(2)}, u32[]{:S(2)}) %collective-permute-start.3) | collective-permute-done | bytes 4128 | tf_op jit(solution)/shard_map/ppermute | solution.py:31
  11.7 0.7 %shard_map.168 = (f32[8,768]{1,0:T(8,128)S(1)}, f32[8,128]{1,0:T(8,128)S(1)}, bf16[8,2048]{1,0:T(8,128)(2,1)S(1)}) custom-call(bf16[8,256]{1,0:T(8,128)(2,1)S(1)} %shard_map.167.tokens, bf16[8,256]{1,0:T(8,128)(2,1)S(1)} %collective-permute-done.partner.partner_tokens, bf16[8,256]{1,0:T(8,128)(2,1)S(1)} %collective-permute-done.1.refs_0_, ...), custom_call_target="tpu_custom_call" | custom-call | flops 1000000000 | tf_op jit(solution)/shard_map/pallas_call | solution.py:206
  13.3 1.1 %collective-permute-start.8 = (f32[2,768]{1,0:T(2,128)S(1)}, f32[2,768]{1,0:T(2,128)S(1)}, u32[]{:S(2)}, u32[]{:S(2)}) collective-permute-start(f32[2,768]{1,0:T(2,128)S(1)} %get-tuple-element.29), channel_id=1, source_target_pairs={{0,7},{1,6},{2,5},{3,4},{4,3},{5,2},{6,1},{7,0},{8,15},{9,14},{10,... | collective-permute-start | bytes 18440 | tf_op jit(solution)/shard_map/ppermute | solution.py:31
  14.8 3.4 %collective-permute-done.8 = f32[2,768]{1,0:T(2,128)S(1)} collective-permute-done((f32[2,768]{1,0:T(2,128)S(1)}, f32[2,768]{1,0:T(2,128)S(1)}, u32[]{:S(2)}, u32[]{:S(2)}) %collective-permute-start.8) | collective-permute-done | bytes 6176 | tf_op jit(solution)/shard_map/ppermute | solution.py:31
  18.5 1.6 %collective-permute-start.7 = (f32[2,2,768]{2,1,0:T(2,128)S(1)}, f32[2,2,768]{2,1,0:T(2,128)S(1)}, u32[]{:S(2)}, u32[]{:S(2)}) collective-permute-start(f32[2,2,768]{2,1,0:T(2,128)S(1)} %pad_maximum_fusion.4), channel_id=1, source_target_pairs={{0,5},{1,4},{2,7},{3,6},{4,1},{5,0},{6,3},{7,2},{8,13},{9,12},{10,... | collective-permute-start | bytes 36872 | tf_op jit(solution)/shard_map/ppermute | solution.py:31
  20.1 1.5 %collective-permute-done.6 = f32[2,2,768]{2,1,0:T(2,128)S(1)} collective-permute-done((f32[2,2,768]{2,1,0:T(2,128)S(1)}, f32[2,2,768]{2,1,0:T(2,128)S(1)}, u32[]{:S(2)}, u32[]{:S(2)}) %collective-permute-start.6) | collective-permute-done | bytes 12320 | tf_op jit(solution)/shard_map/ppermute | solution.py:31
  21.6 1.0 %collective-permute-done.7 = f32[2,2,768]{2,1,0:T(2,128)S(1)} collective-permute-done((f32[2,2,768]{2,1,0:T(2,128)S(1)}, f32[2,2,768]{2,1,0:T(2,128)S(1)}, u32[]{:S(2)}, u32[]{:S(2)}) %collective-permute-start.7) | collective-permute-done | bytes 12320 | tf_op jit(solution)/shard_map/ppermute | solution.py:31
  23.3 1.8 %collective-permute-start.11 = (f32[2,1536]{1,0:T(2,128)S(1)}, f32[2,1536]{1,0:T(2,128)S(1)}, u32[]{:S(2)}, u32[]{:S(2)}) collective-permute-start(f32[2,1536]{1,0:T(2,128)S(1)} %get-tuple-element.36.refs_0_), channel_id=1, source_target_pairs={{0,4},{1,7},{2,6},{3,5},{4,0},{5,3},{6,2},{7,1},{8,12},{9,15},{10,... | collective-permute-start | bytes 36872 | tf_op jit(solution)/shard_map/ppermute | solution.py:41
  25.4 2.6 %collective-permute-done.11.refs_1_ = f32[2,1536]{1,0:T(2,128)S(1)} collective-permute-done((f32[2,1536]{1,0:T(2,128)S(1)}, f32[2,1536]{1,0:T(2,128)S(1)}, u32[]{:S(2)}, u32[]{:S(2)}) %collective-permute-start.11) | collective-permute-done | bytes 12320 | tf_op jit(solution)/shard_map/ppermute | solution.py:41
  28.1 1.3 %shard_map.180 = f32[12,128,128]{2,1,0:T(8,128)} custom-call(f32[12,128,128]{2,1,0:T(8,128)S(1)} %bitcast.40, f32[12,128]{1,0:T(8,128)S(1)} %get-tuple-element.46.key, f32[12,128]{1,0:T(8,128)S(1)} %get-tuple-element.47.write, f32[12,128]{1,0:T(8,128)S(1)} %get-tuple-element.33.refs_1_.retain), custom_call_target="tpu_custom_call" | custom-call | flops 500000000 | tf_op jit(solution)/shard_map/pallas_call | solution.py:206
  29.7 1.7 %collective-permute-start.16 = (bf16[8,512]{1,0:T(8,128)(2,1)S(1)}, bf16[8,512]{1,0:T(8,128)(2,1)S(1)}, u32[]{:S(2)}, u32[]{:S(2)}) collective-permute-start(bf16[8,512]{1,0:T(8,128)(2,1)S(1)} %get-tuple-element.38.refs_0_), channel_id=1, source_target_pairs={{0,4},{1,7},{2,6},{3,5},{4,0},{5,3},{6,2},{7,1},{8,12},{9,15},{10,... | collective-permute-start | bytes 24584 | tf_op jit(solution)/shard_map/ppermute | solution.py:41
  31.4 0.9 %collective-permute-start.15 = (bf16[8,512]{1,0:T(8,128)(2,1)S(1)}, bf16[8,512]{1,0:T(8,128)(2,1)S(1)}, u32[]{:S(2)}, u32[]{:S(2)}) collective-permute-start(bf16[8,512]{1,0:T(8,128)(2,1)S(1)} %get-tuple-element.38.refs_0_), channel_id=1, source_target_pairs={{0,2},{1,3},{2,0},{3,1},{4,6},{5,7},{6,4},{7,5},{8,10},{9,11},{10,... | collective-permute-start | bytes 24584 | tf_op jit(solution)/shard_map/ppermute | solution.py:41
  32.5 1.8 %collective-permute-done.16.refs_0_ = bf16[8,512]{1,0:T(8,128)(2,1)S(1)} collective-permute-done((bf16[8,512]{1,0:T(8,128)(2,1)S(1)}, bf16[8,512]{1,0:T(8,128)(2,1)S(1)}, u32[]{:S(2)}, u32[]{:S(2)}) %collective-permute-start.16) | collective-permute-done | bytes 8224 | tf_op jit(solution)/shard_map/ppermute | solution.py:41
  35.4 0.8 %shard_map.177 = (bf16[8,1024]{1,0:T(8,128)(2,1)S(1)}, bf16[3,8,256]{2,1,0:T(8,128)(2,1)S(1)}, bf16[8,512]{1,0:T(8,128)(2,1)S(1)}) custom-call(bf16[8,512]{1,0:T(8,128)(2,1)S(1)} %collective-permute-done.15.refs_0_, bf16[8,512]{1,0:T(8,128)(2,1)S(1)} %collective-permute-done.17.refs_1_, f32[8,1024]{1,0:T(8,128)S(1)} %get-tuple-element.39.refs_2_, ...), custom_call_target="tpu_custom_call" | custom-call | flops 1000000000 | tf_op jit(solution)/shard_map/pallas_call | solution.py:206
  36.4 2.0 %collective-permute-start.19 = (bf16[8,512]{1,0:T(8,128)(2,1)S(1)}, bf16[8,512]{1,0:T(8,128)(2,1)S(1)}, u32[]{:S(2)}, u32[]{:S(2)}) collective-permute-start(bf16[8,512]{1,0:T(8,128)(2,1)S(1)} %get-tuple-element.45), channel_id=1, source_target_pairs={{0,7},{1,6},{2,5},{3,4},{4,3},{5,2},{6,1},{7,0},{8,15},{9,14},{10,... | collective-permute-start | bytes 24584 | tf_op jit(solution)/shard_map/ppermute | solution.py:31
  38.8 2.6 %collective-permute-done.19.farthest = bf16[8,512]{1,0:T(8,128)(2,1)S(1)} collective-permute-done((bf16[8,512]{1,0:T(8,128)(2,1)S(1)}, bf16[8,512]{1,0:T(8,128)(2,1)S(1)}, u32[]{:S(2)}, u32[]{:S(2)}) %collective-permute-start.19) | collective-permute-done | bytes 8224 | tf_op jit(solution)/shard_map/ppermute | solution.py:31
  41.8 2.4 %collective-permute-start.22 = (bf16[8,256]{1,0:T(8,128)(2,1)S(1)}, bf16[8,256]{1,0:T(8,128)(2,1)S(1)}, u32[]{:S(2)}, u32[]{:S(2)}) collective-permute-start(bf16[8,256]{1,0:T(8,128)(2,1)S(1)} %get-tuple-element.60), channel_id=1, source_target_pairs={{0,5},{1,4},{2,7},{3,6},{4,1},{5,0},{6,3},{7,2},{8,13},{9,12},{10,... | collective-permute-start | bytes 12296 | tf_op jit(solution)/shard_map/ppermute | solution.py:31
  44.1 0.7 %collective-permute-done.21.refs_0_ = bf16[8,256]{1,0:T(8,128)(2,1)S(1)} collective-permute-done((bf16[8,256]{1,0:T(8,128)(2,1)S(1)}, bf16[8,256]{1,0:T(8,128)(2,1)S(1)}, u32[]{:S(2)}, u32[]{:S(2)}) %collective-permute-start.21) | collective-permute-done | bytes 4128 | tf_op jit(solution)/shard_map/ppermute | solution.py:31
  44.8 1.0 %collective-permute-done.22.refs_1_ = bf16[8,256]{1,0:T(8,128)(2,1)S(1)} collective-permute-done((bf16[8,256]{1,0:T(8,128)(2,1)S(1)}, bf16[8,256]{1,0:T(8,128)(2,1)S(1)}, u32[]{:S(2)}, u32[]{:S(2)}) %collective-permute-start.22) | collective-permute-done | bytes 4128 | tf_op jit(solution)/shard_map/ppermute | solution.py:31
  45.8 0.6 %shard_map.179 = bf16[8,256]{1,0:T(8,128)(2,1)} custom-call(bf16[8,256]{1,0:T(8,128)(2,1)S(1)} %get-tuple-element.37.middle, f32[8,256]{1,0:T(8,128)S(1)} %slice_bitcast_fusion.own, bf16[8,512]{1,0:T(8,128)(2,1)S(1)} %collective-permute-done.19.farthest, bf16[8,512]{1,0:T(8,128)(2,1)S(1)} %collective-permute-done.20.passed, ...), custom_call_target="tpu_custom_call" | custom-call | flops 1000000000 | tf_op jit(solution)/shard_map/pallas_call | solution.py:206
  (80 shorter events, 6.5 us)
Async XLA Ops:
  0.6 11.0 %collective-permute-start = (bf16[8,256]{1,0:T(8,128)(2,1)}, bf16[8,256]{1,0:T(8,128)(2,1)S(1)}, u32[]{:S(2)}, u32[]{:S(2)}) collective-permute-start(bf16[8,256]{1,0:T(8,128)(2,1)} %tokens.1), channel_id=1, source_target_pairs={{0,1},{1,0},{2,3},{3,2},{4,5},{5,4},{6,7},{7,6},{8,9},{9,8},{10,11... | collective-permute-start | bytes 12296 | tf_op jit(solution)/shard_map/ppermute | solution.py:49
  1.2 6.6 %collective-permute-start.1 = (bf16[8,256]{1,0:T(8,128)(2,1)}, bf16[8,256]{1,0:T(8,128)(2,1)S(1)}, u32[]{:S(2)}, u32[]{:S(2)}) collective-permute-start(bf16[8,256]{1,0:T(8,128)(2,1)} %tokens.1), channel_id=1, source_target_pairs={{0,3},{1,2},{2,1},{3,0},{4,7},{5,6},{6,5},{7,4},{8,11},{9,10},{10,... | collective-permute-start | bytes 12296 | tf_op jit(solution)/shard_map/ppermute | solution.py:31
  3.9 4.1 %collective-permute-start.2 = (bf16[8,256]{1,0:T(8,128)(2,1)}, bf16[8,256]{1,0:T(8,128)(2,1)S(1)}, u32[]{:S(2)}, u32[]{:S(2)}) collective-permute-start(bf16[8,256]{1,0:T(8,128)(2,1)} %tokens.1), channel_id=1, source_target_pairs={{0,5},{1,4},{2,7},{3,6},{4,1},{5,0},{6,3},{7,2},{8,13},{9,12},{10,... | collective-permute-start | bytes 12296 | tf_op jit(solution)/shard_map/ppermute | solution.py:31
  6.1 5.0 %collective-permute-start.3 = (bf16[8,256]{1,0:T(8,128)(2,1)}, bf16[8,256]{1,0:T(8,128)(2,1)S(1)}, u32[]{:S(2)}, u32[]{:S(2)}) collective-permute-start(bf16[8,256]{1,0:T(8,128)(2,1)} %tokens.1), channel_id=1, source_target_pairs={{0,7},{1,6},{2,5},{3,4},{4,3},{5,2},{6,1},{7,0},{8,15},{9,14},{10,... | collective-permute-start | bytes 12296 | tf_op jit(solution)/shard_map/ppermute | solution.py:31
  6.2 16.4 %collective-permute-start.10 = (f32[12,128,128]{2,1,0:T(8,128)}, f32[12,128,128]{2,1,0:T(8,128)S(1)}, u32[]{:S(2)}, u32[]{:S(2)}) collective-permute-start(f32[12,128,128]{2,1,0:T(8,128)} %bitcast.38), channel_id=1, source_target_pairs={{0,1},{1,0},{2,3},{3,2},{4,5},{5,4},{6,7},{7,6},{8,9},{9,8},{10,11... | collective-permute-start | bytes 2359304 | tf_op jit(solution)/shard_map/ppermute | solution.py:49
  7.8 21.5 %collective-permute-start.14 = (bf16[1536,256]{1,0:T(8,128)(2,1)S(1)}, bf16[1536,256]{1,0:T(8,128)(2,1)S(1)}, u32[]{:S(2)}, u32[]{:S(2)}) collective-permute-start(bf16[1536,256]{1,0:T(8,128)(2,1)S(1)} %copy-done.8), channel_id=1, source_target_pairs={{0,1},{1,0},{2,3},{3,2},{4,5},{5,4},{6,7},{7,6},{8,9},{9,8},{10,11... | collective-permute-start | bytes 2359304 | tf_op jit(solution)/shard_map/ppermute | solution.py:49
  11.2 1.3 %collective-permute-start.4 = (bf16[3,8,256]{2,1,0:T(8,128)(2,1)S(1)}, bf16[3,8,256]{2,1,0:T(8,128)(2,1)S(1)}, u32[]{:S(2)}, u32[]{:S(2)}) collective-permute-start(bf16[3,8,256]{2,1,0:T(8,128)(2,1)S(1)} %pad_maximum_fusion.2), channel_id=1, source_target_pairs={{0,1},{1,0},{2,3},{3,2},{4,5},{5,4},{6,7},{7,6},{8,9},{9,8},{10,11... | collective-permute-start | bytes 36872 | tf_op jit(solution)/shard_map/ppermute | solution.py:49
  12.5 10.3 %copy-start.15 = (f32[128]{0:T(128)S(1)}, f32[128]{0:T(128)}, u32[]{:S(2)}) copy-start(f32[128]{0:T(128)} %param.27) | copy-start | bytes 1540
  12.9 5.4 %collective-permute-start.5 = (f32[3,2,768]{2,1,0:T(2,128)S(1)}, f32[3,2,768]{2,1,0:T(2,128)S(1)}, u32[]{:S(2)}, u32[]{:S(2)}) collective-permute-start(f32[3,2,768]{2,1,0:T(2,128)S(1)} %get-tuple-element.28), channel_id=1, source_target_pairs={{0,1},{1,0},{2,3},{3,2},{4,5},{5,4},{6,7},{7,6},{8,9},{9,8},{10,11... | collective-permute-start | bytes 55304 | tf_op jit(solution)/shard_map/ppermute | solution.py:49
  13.3 4.9 %collective-permute-start.8 = (f32[2,768]{1,0:T(2,128)S(1)}, f32[2,768]{1,0:T(2,128)S(1)}, u32[]{:S(2)}, u32[]{:S(2)}) collective-permute-start(f32[2,768]{1,0:T(2,128)S(1)} %get-tuple-element.29), channel_id=1, source_target_pairs={{0,7},{1,6},{2,5},{3,4},{4,3},{5,2},{6,1},{7,0},{8,15},{9,14},{10,... | collective-permute-start | bytes 18440 | tf_op jit(solution)/shard_map/ppermute | solution.py:31
  18.2 4.4 %collective-permute-start.9 = (f32[2,768]{1,0:T(2,128)S(1)}, f32[2,768]{1,0:T(2,128)S(1)}, u32[]{:S(2)}, u32[]{:S(2)}) collective-permute-start(f32[2,768]{1,0:T(2,128)S(1)} %collective-permute-done.8), channel_id=1, source_target_pairs={{0,1},{1,0},{2,3},{3,2},{4,5},{5,4},{6,7},{7,6},{8,9},{9,8},{10,11... | collective-permute-start | bytes 18440 | tf_op jit(solution)/shard_map/ppermute | solution.py:49
  18.4 3.2 %collective-permute-start.6 = (f32[2,2,768]{2,1,0:T(2,128)S(1)}, f32[2,2,768]{2,1,0:T(2,128)S(1)}, u32[]{:S(2)}, u32[]{:S(2)}) collective-permute-start(f32[2,2,768]{2,1,0:T(2,128)S(1)} %pad_maximum_fusion.3), channel_id=1, source_target_pairs={{0,3},{1,2},{2,1},{3,0},{4,7},{5,6},{6,5},{7,4},{8,11},{9,10},{10,... | collective-permute-start | bytes 36872 | tf_op jit(solution)/shard_map/ppermute | solution.py:31
  18.5 4.1 %collective-permute-start.7 = (f32[2,2,768]{2,1,0:T(2,128)S(1)}, f32[2,2,768]{2,1,0:T(2,128)S(1)}, u32[]{:S(2)}, u32[]{:S(2)}) collective-permute-start(f32[2,2,768]{2,1,0:T(2,128)S(1)} %pad_maximum_fusion.4), channel_id=1, source_target_pairs={{0,5},{1,4},{2,7},{3,6},{4,1},{5,0},{6,3},{7,2},{8,13},{9,12},{10,... | collective-permute-start | bytes 36872 | tf_op jit(solution)/shard_map/ppermute | solution.py:31
  23.3 4.7 %collective-permute-start.11 = (f32[2,1536]{1,0:T(2,128)S(1)}, f32[2,1536]{1,0:T(2,128)S(1)}, u32[]{:S(2)}, u32[]{:S(2)}) collective-permute-start(f32[2,1536]{1,0:T(2,128)S(1)} %get-tuple-element.36.refs_0_), channel_id=1, source_target_pairs={{0,4},{1,7},{2,6},{3,5},{4,0},{5,3},{6,2},{7,1},{8,12},{9,15},{10,... | collective-permute-start | bytes 36872 | tf_op jit(solution)/shard_map/ppermute | solution.py:41
  25.2 4.2 %collective-permute-start.12 = (f32[2,1536]{1,0:T(2,128)S(1)}, f32[2,1536]{1,0:T(2,128)S(1)}, u32[]{:S(2)}, u32[]{:S(2)}) collective-permute-start(f32[2,1536]{1,0:T(2,128)S(1)} %get-tuple-element.36.refs_0_), channel_id=1, source_target_pairs={{0,2},{1,3},{2,0},{3,1},{4,6},{5,7},{6,4},{7,5},{8,10},{9,11},{10,... | collective-permute-start | bytes 36872 | tf_op jit(solution)/shard_map/ppermute | solution.py:41
  28.0 1.4 %collective-permute-start.13 = (f32[2,1536]{1,0:T(2,128)S(1)}, f32[2,1536]{1,0:T(2,128)S(1)}, u32[]{:S(2)}, u32[]{:S(2)}) collective-permute-start(f32[2,1536]{1,0:T(2,128)S(1)} %collective-permute-done.11.refs_1_), channel_id=1, source_target_pairs={{0,1},{1,0},{2,3},{3,2},{4,5},{5,4},{6,7},{7,6},{8,9},{9,8},{10,11... | collective-permute-start | bytes 36872 | tf_op jit(solution)/shard_map/ppermute | solution.py:49
  29.7 4.6 %collective-permute-start.16 = (bf16[8,512]{1,0:T(8,128)(2,1)S(1)}, bf16[8,512]{1,0:T(8,128)(2,1)S(1)}, u32[]{:S(2)}, u32[]{:S(2)}) collective-permute-start(bf16[8,512]{1,0:T(8,128)(2,1)S(1)} %get-tuple-element.38.refs_0_), channel_id=1, source_target_pairs={{0,4},{1,7},{2,6},{3,5},{4,0},{5,3},{6,2},{7,1},{8,12},{9,15},{10,... | collective-permute-start | bytes 24584 | tf_op jit(solution)/shard_map/ppermute | solution.py:41
  31.4 3.7 %collective-permute-start.15 = (bf16[8,512]{1,0:T(8,128)(2,1)S(1)}, bf16[8,512]{1,0:T(8,128)(2,1)S(1)}, u32[]{:S(2)}, u32[]{:S(2)}) collective-permute-start(bf16[8,512]{1,0:T(8,128)(2,1)S(1)} %get-tuple-element.38.refs_0_), channel_id=1, source_target_pairs={{0,2},{1,3},{2,0},{3,1},{4,6},{5,7},{6,4},{7,5},{8,10},{9,11},{10,... | collective-permute-start | bytes 24584 | tf_op jit(solution)/shard_map/ppermute | solution.py:41
  34.2 1.2 %collective-permute-start.17 = (bf16[8,512]{1,0:T(8,128)(2,1)S(1)}, bf16[8,512]{1,0:T(8,128)(2,1)S(1)}, u32[]{:S(2)}, u32[]{:S(2)}) collective-permute-start(bf16[8,512]{1,0:T(8,128)(2,1)S(1)} %collective-permute-done.16.refs_0_), channel_id=1, source_target_pairs={{0,1},{1,0},{2,3},{3,2},{4,5},{5,4},{6,7},{7,6},{8,9},{9,8},{10,11... | collective-permute-start | bytes 24584 | tf_op jit(solution)/shard_map/ppermute | solution.py:49
  36.3 5.4 %collective-permute-start.18 = (bf16[3,8,256]{2,1,0:T(8,128)(2,1)S(1)}, bf16[3,8,256]{2,1,0:T(8,128)(2,1)S(1)}, u32[]{:S(2)}, u32[]{:S(2)}) collective-permute-start(bf16[3,8,256]{2,1,0:T(8,128)(2,1)S(1)} %get-tuple-element.44), channel_id=1, source_target_pairs={{0,1},{1,0},{2,3},{3,2},{4,5},{5,4},{6,7},{7,6},{8,9},{9,8},{10,11... | collective-permute-start | bytes 36872 | tf_op jit(solution)/shard_map/ppermute | solution.py:49
  36.4 4.9 %collective-permute-start.19 = (bf16[8,512]{1,0:T(8,128)(2,1)S(1)}, bf16[8,512]{1,0:T(8,128)(2,1)S(1)}, u32[]{:S(2)}, u32[]{:S(2)}) collective-permute-start(bf16[8,512]{1,0:T(8,128)(2,1)S(1)} %get-tuple-element.45), channel_id=1, source_target_pairs={{0,7},{1,6},{2,5},{3,4},{4,3},{5,2},{6,1},{7,0},{8,15},{9,14},{10,... | collective-permute-start | bytes 24584 | tf_op jit(solution)/shard_map/ppermute | solution.py:31
  41.4 4.4 %collective-permute-start.20 = (bf16[8,512]{1,0:T(8,128)(2,1)S(1)}, bf16[8,512]{1,0:T(8,128)(2,1)S(1)}, u32[]{:S(2)}, u32[]{:S(2)}) collective-permute-start(bf16[8,512]{1,0:T(8,128)(2,1)S(1)} %collective-permute-done.19.farthest), channel_id=1, source_target_pairs={{0,1},{1,0},{2,3},{3,2},{4,5},{5,4},{6,7},{7,6},{8,9},{9,8},{10,11... | collective-permute-start | bytes 24584 | tf_op jit(solution)/shard_map/ppermute | solution.py:49
  41.7 3.1 %collective-permute-start.21 = (bf16[8,256]{1,0:T(8,128)(2,1)S(1)}, bf16[8,256]{1,0:T(8,128)(2,1)S(1)}, u32[]{:S(2)}, u32[]{:S(2)}) collective-permute-start(bf16[8,256]{1,0:T(8,128)(2,1)S(1)} %get-tuple-element.61), channel_id=1, source_target_pairs={{0,3},{1,2},{2,1},{3,0},{4,7},{5,6},{6,5},{7,4},{8,11},{9,10},{10,... | collective-permute-start | bytes 12296 | tf_op jit(solution)/shard_map/ppermute | solution.py:31
  41.8 4.0 %collective-permute-start.22 = (bf16[8,256]{1,0:T(8,128)(2,1)S(1)}, bf16[8,256]{1,0:T(8,128)(2,1)S(1)}, u32[]{:S(2)}, u32[]{:S(2)}) collective-permute-start(bf16[8,256]{1,0:T(8,128)(2,1)S(1)} %get-tuple-element.60), channel_id=1, source_target_pairs={{0,5},{1,4},{2,7},{3,6},{4,1},{5,0},{6,3},{7,2},{8,13},{9,12},{10,... | collective-permute-start | bytes 12296 | tf_op jit(solution)/shard_map/ppermute | solution.py:31
  (15 other events, 80.2 us)

commit v5 on v4

--- a/solution.py
+++ b/solution.py
@@ -417,10 +417,9 @@
     farthest[...] = dot(hidden, down[:, across]).astype(jnp.bfloat16)
 
 
-def down_own(chips, hidden, down, staying):
-    size = staying.shape[2]
-    for d in range(chips - 1):
-        staying[d] = dot(hidden[...], down[:, span(mine_lane(d), size)])
+def down_own(d, hidden, down, arrived, total):
+    own = dot(hidden[...], down[:, span(mine_lane(d), total.shape[1])])
+    total[...] = (own + arrived[d].astype(jnp.float32)).astype(total.dtype)
 
 
 def add_up(middle, own, farthest, passed, *refs):
@@ -527,18 +526,20 @@
         [*got, *early, gain_mid, w_up, w_down],
     )
     arrived = near(leaving)
-    (staying,) = call(
-        functools.partial(down_own, chips),
-        [((chips - 1, rows, features), f32)],
-        [hidden, w_down],
-    )
-    sums = staying + arrived.astype(f32)
-    terms = [sums[d].astype(bf16) for d in range(chips - 1)] + [farthest]
+    terms = []
+    for d in range(chips - 1):
+        terms += call(
+            functools.partial(down_own, d),
+            [((rows, features), bf16 if d else f32)],
+            [hidden, w_down, arrived],
+        )
+    own = terms[0]
+    terms.append(farthest)
     *got, farthest = far(terms, chips)[1:]
     (layer_out,) = call(
         add_up,
         [((rows, features), bf16)],
-        [middle, sums[0], farthest, near(farthest), *got],
+        [middle, own, farthest, near(farthest), *got],
     )
     return (layer_out, updated.reshape(memory.shape))
 

time: 46.6 us -> 46.4 us (level)
  waiting for transfers between devices: 18.6 us -> 18.1 us
    ppermute x9, waiting for transfers between devices: 13.3 us -> 11.7 us  [far(): got.append(lax.ppermute(pieces[d], axes, pairs))]
    ppermute x4, waiting for transfers between devices: 4.77 us -> 5.59 us  [shared(): got = lax.ppermute(piece, axes, pairs)]
    pallas_call x14 -> x16, Pallas kernels: 6.1 us -> 6.34 us  [call(): pl.pallas_call(body, out_shape=[jax.ShapeDtypeStruct(shape, kind) for sha...]
  transfers between devices with their start and end apart: 23 -> 23, of which waited for: 12 -> 14; matrix products, arithmetic and copies ran while one was open for 0% -> 0% of each run, Pallas kernels for 9% -> 10%
where the time goes in v5:
time: 46.4 us; the launch traced here: 46.2 us
  starting transfers between devices  19.9 us (43%)
  waiting for transfers between devices  18.1 us (39%)
  Pallas kernels  6.34 us (14%)
  local copies, waits for them, and re-layouts  1.03 us (2%)
  between operations  0.87 us (2%)
    ppermute x9, starting transfers between devices, far(): got.append(lax.ppermute(pieces[d], axes, pairs))  12.3 us
    ppermute x9, waiting for transfers between devices, far(): got.append(lax.ppermute(pieces[d], axes, pairs))  11.7 us
    pallas_call x16, Pallas kernels, call(): pl.pallas_call(body, out_shape=[jax.ShapeDtypeStruct(shape, kind) for sha...  6.34 us
    ppermute x4, waiting for transfers between devices, shared(): got = lax.ppermute(piece, axes, pairs)  5.59 us
    ppermute x4, starting transfers between devices, shared(): got = lax.ppermute(piece, axes, pairs)  4.78 us
    ppermute x10, starting transfers between devices, near(): return lax.ppermute(value, 'tp', [(0, 1), (1, 0)])  2.81 us
    unnamed x32, local copies, waits for them, and re-layouts  1.02 us
  transfers between devices with their start and end apart: 23, of which 14 were waited for; matrix products, arithmetic and copies ran while one was open for 0% of the time, Pallas kernels for 10%

profile of v5, /device:TPU:0, one launch (start us, length us, event | category | flops | bytes accessed | tf_op | source)
XLA Modules:
  0.0 46.2 jit_solution(2448569320327919991)
XLA Ops:
  1.2 2.7 %collective-permute-start.1 = (bf16[8,256]{1,0:T(8,128)(2,1)}, bf16[8,256]{1,0:T(8,128)(2,1)S(1)}, u32[]{:S(2)}, u32[]{:S(2)}) collective-permute-start(bf16[8,256]{1,0:T(8,128)(2,1)} %tokens.1), channel_id=1, source_target_pairs={{0,3},{1,2},{2,1},{3,0},{4,7},{5,6},{6,5},{7,4},{8,11},{9,10},{10,... | collective-permute-start | bytes 12296 | tf_op jit(solution)/shard_map/ppermute | solution.py:31
  3.9 2.3 %collective-permute-start.2 = (bf16[8,256]{1,0:T(8,128)(2,1)}, bf16[8,256]{1,0:T(8,128)(2,1)S(1)}, u32[]{:S(2)}, u32[]{:S(2)}) collective-permute-start(bf16[8,256]{1,0:T(8,128)(2,1)} %tokens.1), channel_id=1, source_target_pairs={{0,5},{1,4},{2,7},{3,6},{4,1},{5,0},{6,3},{7,2},{8,13},{9,12},{10,... | collective-permute-start | bytes 12296 | tf_op jit(solution)/shard_map/ppermute | solution.py:31
  6.7 0.9 %copy-done.12 = bf16[8,256]{1,0:T(8,128)(2,1)S(1)} copy-done((bf16[8,256]{1,0:T(8,128)(2,1)S(1)}, bf16[8,256]{1,0:T(8,128)(2,1)}, u32[]{:S(2)}) %copy-start.12) | copy-done | bytes 4120
  8.0 3.2 %collective-permute-done.3.refs_2_ = bf16[8,256]{1,0:T(8,128)(2,1)S(1)} collective-permute-done((bf16[8,256]{1,0:T(8,128)(2,1)}, bf16[8,256]{1,0:T(8,128)(2,1)S(1)}, u32[]{:S(2)}, u32[]{:S(2)}) %collective-permute-start.3) | collective-permute-done | bytes 4128 | tf_op jit(solution)/shard_map/ppermute | solution.py:31
  11.7 0.7 %shard_map.168 = (f32[8,768]{1,0:T(8,128)S(1)}, f32[8,128]{1,0:T(8,128)S(1)}, bf16[8,2048]{1,0:T(8,128)(2,1)S(1)}) custom-call(bf16[8,256]{1,0:T(8,128)(2,1)S(1)} %shard_map.167.tokens, bf16[8,256]{1,0:T(8,128)(2,1)S(1)} %collective-permute-done.partner.partner_tokens, bf16[8,256]{1,0:T(8,128)(2,1)S(1)} %collective-permute-done.1.refs_0_, ...), custom_call_target="tpu_custom_call" | custom-call | flops 1000000000 | tf_op jit(solution)/shard_map/pallas_call | solution.py:206
  13.3 1.1 %collective-permute-start.8 = (f32[2,768]{1,0:T(2,128)S(1)}, f32[2,768]{1,0:T(2,128)S(1)}, u32[]{:S(2)}, u32[]{:S(2)}) collective-permute-start(f32[2,768]{1,0:T(2,128)S(1)} %get-tuple-element.29), channel_id=1, source_target_pairs={{0,7},{1,6},{2,5},{3,4},{4,3},{5,2},{6,1},{7,0},{8,15},{9,14},{10,... | collective-permute-start | bytes 18440 | tf_op jit(solution)/shard_map/ppermute | solution.py:31
  14.8 3.4 %collective-permute-done.8 = f32[2,768]{1,0:T(2,128)S(1)} collective-permute-done((f32[2,768]{1,0:T(2,128)S(1)}, f32[2,768]{1,0:T(2,128)S(1)}, u32[]{:S(2)}, u32[]{:S(2)}) %collective-permute-start.8) | collective-permute-done | bytes 6176 | tf_op jit(solution)/shard_map/ppermute | solution.py:31
  18.5 1.6 %collective-permute-start.7 = (f32[2,2,768]{2,1,0:T(2,128)S(1)}, f32[2,2,768]{2,1,0:T(2,128)S(1)}, u32[]{:S(2)}, u32[]{:S(2)}) collective-permute-start(f32[2,2,768]{2,1,0:T(2,128)S(1)} %pad_maximum_fusion.4), channel_id=1, source_target_pairs={{0,5},{1,4},{2,7},{3,6},{4,1},{5,0},{6,3},{7,2},{8,13},{9,12},{10,... | collective-permute-start | bytes 36872 | tf_op jit(solution)/shard_map/ppermute | solution.py:31
  20.1 1.5 %collective-permute-done.6 = f32[2,2,768]{2,1,0:T(2,128)S(1)} collective-permute-done((f32[2,2,768]{2,1,0:T(2,128)S(1)}, f32[2,2,768]{2,1,0:T(2,128)S(1)}, u32[]{:S(2)}, u32[]{:S(2)}) %collective-permute-start.6) | collective-permute-done | bytes 12320 | tf_op jit(solution)/shard_map/ppermute | solution.py:31
  21.6 1.0 %collective-permute-done.7 = f32[2,2,768]{2,1,0:T(2,128)S(1)} collective-permute-done((f32[2,2,768]{2,1,0:T(2,128)S(1)}, f32[2,2,768]{2,1,0:T(2,128)S(1)}, u32[]{:S(2)}, u32[]{:S(2)}) %collective-permute-start.7) | collective-permute-done | bytes 12320 | tf_op jit(solution)/shard_map/ppermute | solution.py:31
  23.3 1.8 %collective-permute-start.11 = (f32[2,1536]{1,0:T(2,128)S(1)}, f32[2,1536]{1,0:T(2,128)S(1)}, u32[]{:S(2)}, u32[]{:S(2)}) collective-permute-start(f32[2,1536]{1,0:T(2,128)S(1)} %get-tuple-element.36.refs_0_), channel_id=1, source_target_pairs={{0,4},{1,7},{2,6},{3,5},{4,0},{5,3},{6,2},{7,1},{8,12},{9,15},{10,... | collective-permute-start | bytes 36872 | tf_op jit(solution)/shard_map/ppermute | solution.py:41
  25.4 2.6 %collective-permute-done.11.refs_1_ = f32[2,1536]{1,0:T(2,128)S(1)} collective-permute-done((f32[2,1536]{1,0:T(2,128)S(1)}, f32[2,1536]{1,0:T(2,128)S(1)}, u32[]{:S(2)}, u32[]{:S(2)}) %collective-permute-start.11) | collective-permute-done | bytes 12320 | tf_op jit(solution)/shard_map/ppermute | solution.py:41
  28.1 0.8 %collective-permute-done.12.refs_2_ = f32[2,1536]{1,0:T(2,128)S(1)} collective-permute-done((f32[2,1536]{1,0:T(2,128)S(1)}, f32[2,1536]{1,0:T(2,128)S(1)}, u32[]{:S(2)}, u32[]{:S(2)}) %collective-permute-start.12) | collective-permute-done | bytes 12320 | tf_op jit(solution)/shard_map/ppermute | solution.py:41
  29.5 1.8 %collective-permute-start.16 = (bf16[8,512]{1,0:T(8,128)(2,1)S(1)}, bf16[8,512]{1,0:T(8,128)(2,1)S(1)}, u32[]{:S(2)}, u32[]{:S(2)}) collective-permute-start(bf16[8,512]{1,0:T(8,128)(2,1)S(1)} %get-tuple-element.38.refs_0_), channel_id=1, source_target_pairs={{0,4},{1,7},{2,6},{3,5},{4,0},{5,3},{6,2},{7,1},{8,12},{9,15},{10,... | collective-permute-start | bytes 24584 | tf_op jit(solution)/shard_map/ppermute | solution.py:41
  31.3 1.0 %collective-permute-start.15 = (bf16[8,512]{1,0:T(8,128)(2,1)S(1)}, bf16[8,512]{1,0:T(8,128)(2,1)S(1)}, u32[]{:S(2)}, u32[]{:S(2)}) collective-permute-start(bf16[8,512]{1,0:T(8,128)(2,1)S(1)} %get-tuple-element.38.refs_0_), channel_id=1, source_target_pairs={{0,2},{1,3},{2,0},{3,1},{4,6},{5,7},{6,4},{7,5},{8,10},{9,11},{10,... | collective-permute-start | bytes 24584 | tf_op jit(solution)/shard_map/ppermute | solution.py:41
  32.5 1.6 %collective-permute-done.16.refs_0_ = bf16[8,512]{1,0:T(8,128)(2,1)S(1)} collective-permute-done((bf16[8,512]{1,0:T(8,128)(2,1)S(1)}, bf16[8,512]{1,0:T(8,128)(2,1)S(1)}, u32[]{:S(2)}, u32[]{:S(2)}) %collective-permute-start.16) | collective-permute-done | bytes 8224 | tf_op jit(solution)/shard_map/ppermute | solution.py:41
  34.3 0.6 %collective-permute-done.15.refs_0_ = bf16[8,512]{1,0:T(8,128)(2,1)S(1)} collective-permute-done((bf16[8,512]{1,0:T(8,128)(2,1)S(1)}, bf16[8,512]{1,0:T(8,128)(2,1)S(1)}, u32[]{:S(2)}, u32[]{:S(2)}) %collective-permute-start.15) | collective-permute-done | bytes 8224 | tf_op jit(solution)/shard_map/ppermute | solution.py:41
  35.2 0.8 %shard_map.177 = (bf16[8,1024]{1,0:T(8,128)(2,1)S(1)}, bf16[3,8,256]{2,1,0:T(8,128)(2,1)S(1)}, bf16[8,512]{1,0:T(8,128)(2,1)S(1)}) custom-call(bf16[8,512]{1,0:T(8,128)(2,1)S(1)} %collective-permute-done.15.refs_0_, bf16[8,512]{1,0:T(8,128)(2,1)S(1)} %collective-permute-done.17.refs_1_, f32[8,1024]{1,0:T(8,128)S(1)} %get-tuple-element.39.refs_2_, ...), custom_call_target="tpu_custom_call" | custom-call | flops 1000000000 | tf_op jit(solution)/shard_map/pallas_call | solution.py:206
  36.2 2.1 %collective-permute-start.19 = (bf16[8,512]{1,0:T(8,128)(2,1)S(1)}, bf16[8,512]{1,0:T(8,128)(2,1)S(1)}, u32[]{:S(2)}, u32[]{:S(2)}) collective-permute-start(bf16[8,512]{1,0:T(8,128)(2,1)S(1)} %get-tuple-element.45), channel_id=1, source_target_pairs={{0,7},{1,6},{2,5},{3,4},{4,3},{5,2},{6,1},{7,0},{8,15},{9,14},{10,... | collective-permute-start | bytes 24584 | tf_op jit(solution)/shard_map/ppermute | solution.py:31
  38.4 1.3 %shard_map.182 = f32[12,128,128]{2,1,0:T(8,128)} custom-call(f32[12,128,128]{2,1,0:T(8,128)S(1)} %bitcast.34, f32[12,128]{1,0:T(8,128)S(1)} %get-tuple-element.46.key, f32[12,128]{1,0:T(8,128)S(1)} %get-tuple-element.47.write, f32[12,128]{1,0:T(8,128)S(1)} %get-tuple-element.33.refs_1_.retain), custom_call_target="tpu_custom_call" | custom-call | flops 500000000 | tf_op jit(solution)/shard_map/pallas_call | solution.py:206
  39.6 1.5 %collective-permute-done.19.farthest = bf16[8,512]{1,0:T(8,128)(2,1)S(1)} collective-permute-done((bf16[8,512]{1,0:T(8,128)(2,1)S(1)}, bf16[8,512]{1,0:T(8,128)(2,1)S(1)}, u32[]{:S(2)}, u32[]{:S(2)}) %collective-permute-start.19) | collective-permute-done | bytes 8224 | tf_op jit(solution)/shard_map/ppermute | solution.py:31
  41.8 2.5 %collective-permute-start.21 = (bf16[8,256]{1,0:T(8,128)(2,1)S(1)}, bf16[8,256]{1,0:T(8,128)(2,1)S(1)}, u32[]{:S(2)}, u32[]{:S(2)}) collective-permute-start(bf16[8,256]{1,0:T(8,128)(2,1)S(1)} %shard_map.179), channel_id=1, source_target_pairs={{0,3},{1,2},{2,1},{3,0},{4,7},{5,6},{6,5},{7,4},{8,11},{9,10},{10,... | collective-permute-start | bytes 12296 | tf_op jit(solution)/shard_map/ppermute | solution.py:31
  44.5 1.1 %collective-permute-done.22.refs_1_ = bf16[8,256]{1,0:T(8,128)(2,1)S(1)} collective-permute-done((bf16[8,256]{1,0:T(8,128)(2,1)S(1)}, bf16[8,256]{1,0:T(8,128)(2,1)S(1)}, u32[]{:S(2)}, u32[]{:S(2)}) %collective-permute-start.22) | collective-permute-done | bytes 4128 | tf_op jit(solution)/shard_map/ppermute | solution.py:31
  45.6 0.6 %shard_map.181 = bf16[8,256]{1,0:T(8,128)(2,1)} custom-call(bf16[8,256]{1,0:T(8,128)(2,1)S(1)} %get-tuple-element.37.middle, f32[8,256]{1,0:T(8,128)S(1)} %shard_map.178.own, bf16[8,512]{1,0:T(8,128)(2,1)S(1)} %collective-permute-done.19.farthest, bf16[8,512]{1,0:T(8,128)(2,1)S(1)} %collective-permute-done.20.passed, ...), custom_call_target="tpu_custom_call" | custom-call | flops 1000000000 | tf_op jit(solution)/shard_map/pallas_call | solution.py:206
  (79 shorter events, 7.0 us)
Async XLA Ops:
  0.6 11.0 %collective-permute-start = (bf16[8,256]{1,0:T(8,128)(2,1)}, bf16[8,256]{1,0:T(8,128)(2,1)S(1)}, u32[]{:S(2)}, u32[]{:S(2)}) collective-permute-start(bf16[8,256]{1,0:T(8,128)(2,1)} %tokens.1), channel_id=1, source_target_pairs={{0,1},{1,0},{2,3},{3,2},{4,5},{5,4},{6,7},{7,6},{8,9},{9,8},{10,11... | collective-permute-start | bytes 12296 | tf_op jit(solution)/shard_map/ppermute | solution.py:49
  1.2 6.6 %collective-permute-start.1 = (bf16[8,256]{1,0:T(8,128)(2,1)}, bf16[8,256]{1,0:T(8,128)(2,1)S(1)}, u32[]{:S(2)}, u32[]{:S(2)}) collective-permute-start(bf16[8,256]{1,0:T(8,128)(2,1)} %tokens.1), channel_id=1, source_target_pairs={{0,3},{1,2},{2,1},{3,0},{4,7},{5,6},{6,5},{7,4},{8,11},{9,10},{10,... | collective-permute-start | bytes 12296 | tf_op jit(solution)/shard_map/ppermute | solution.py:31
  3.9 4.1 %collective-permute-start.2 = (bf16[8,256]{1,0:T(8,128)(2,1)}, bf16[8,256]{1,0:T(8,128)(2,1)S(1)}, u32[]{:S(2)}, u32[]{:S(2)}) collective-permute-start(bf16[8,256]{1,0:T(8,128)(2,1)} %tokens.1), channel_id=1, source_target_pairs={{0,5},{1,4},{2,7},{3,6},{4,1},{5,0},{6,3},{7,2},{8,13},{9,12},{10,... | collective-permute-start | bytes 12296 | tf_op jit(solution)/shard_map/ppermute | solution.py:31
  6.1 5.0 %collective-permute-start.3 = (bf16[8,256]{1,0:T(8,128)(2,1)}, bf16[8,256]{1,0:T(8,128)(2,1)S(1)}, u32[]{:S(2)}, u32[]{:S(2)}) collective-permute-start(bf16[8,256]{1,0:T(8,128)(2,1)} %tokens.1), channel_id=1, source_target_pairs={{0,7},{1,6},{2,5},{3,4},{4,3},{5,2},{6,1},{7,0},{8,15},{9,14},{10,... | collective-permute-start | bytes 12296 | tf_op jit(solution)/shard_map/ppermute | solution.py:31
  6.2 16.4 %collective-permute-start.10 = (f32[12,128,128]{2,1,0:T(8,128)}, f32[12,128,128]{2,1,0:T(8,128)S(1)}, u32[]{:S(2)}, u32[]{:S(2)}) collective-permute-start(f32[12,128,128]{2,1,0:T(8,128)} %bitcast.32), channel_id=1, source_target_pairs={{0,1},{1,0},{2,3},{3,2},{4,5},{5,4},{6,7},{7,6},{8,9},{9,8},{10,11... | collective-permute-start | bytes 2359304 | tf_op jit(solution)/shard_map/ppermute | solution.py:49
  7.8 20.2 %collective-permute-start.14 = (bf16[1536,256]{1,0:T(8,128)(2,1)S(1)}, bf16[1536,256]{1,0:T(8,128)(2,1)S(1)}, u32[]{:S(2)}, u32[]{:S(2)}) collective-permute-start(bf16[1536,256]{1,0:T(8,128)(2,1)S(1)} %copy-done.7), channel_id=1, source_target_pairs={{0,1},{1,0},{2,3},{3,2},{4,5},{5,4},{6,7},{7,6},{8,9},{9,8},{10,11... | collective-permute-start | bytes 2359304 | tf_op jit(solution)/shard_map/ppermute | solution.py:49
  11.2 1.3 %collective-permute-start.4 = (bf16[3,8,256]{2,1,0:T(8,128)(2,1)S(1)}, bf16[3,8,256]{2,1,0:T(8,128)(2,1)S(1)}, u32[]{:S(2)}, u32[]{:S(2)}) collective-permute-start(bf16[3,8,256]{2,1,0:T(8,128)(2,1)S(1)} %pad_maximum_fusion.2), channel_id=1, source_target_pairs={{0,1},{1,0},{2,3},{3,2},{4,5},{5,4},{6,7},{7,6},{8,9},{9,8},{10,11... | collective-permute-start | bytes 36872 | tf_op jit(solution)/shard_map/ppermute | solution.py:49
  12.5 10.3 %copy-start.15 = (f32[128]{0:T(128)S(1)}, f32[128]{0:T(128)}, u32[]{:S(2)}) copy-start(f32[128]{0:T(128)} %param.27) | copy-start | bytes 1540
  12.9 5.4 %collective-permute-start.5 = (f32[3,2,768]{2,1,0:T(2,128)S(1)}, f32[3,2,768]{2,1,0:T(2,128)S(1)}, u32[]{:S(2)}, u32[]{:S(2)}) collective-permute-start(f32[3,2,768]{2,1,0:T(2,128)S(1)} %get-tuple-element.28), channel_id=1, source_target_pairs={{0,1},{1,0},{2,3},{3,2},{4,5},{5,4},{6,7},{7,6},{8,9},{9,8},{10,11... | collective-permute-start | bytes 55304 | tf_op jit(solution)/shard_map/ppermute | solution.py:49
  13.3 4.9 %collective-permute-start.8 = (f32[2,768]{1,0:T(2,128)S(1)}, f32[2,768]{1,0:T(2,128)S(1)}, u32[]{:S(2)}, u32[]{:S(2)}) collective-permute-start(f32[2,768]{1,0:T(2,128)S(1)} %get-tuple-element.29), channel_id=1, source_target_pairs={{0,7},{1,6},{2,5},{3,4},{4,3},{5,2},{6,1},{7,0},{8,15},{9,14},{10,... | collective-permute-start | bytes 18440 | tf_op jit(solution)/shard_map/ppermute | solution.py:31
  18.2 4.4 %collective-permute-start.9 = (f32[2,768]{1,0:T(2,128)S(1)}, f32[2,768]{1,0:T(2,128)S(1)}, u32[]{:S(2)}, u32[]{:S(2)}) collective-permute-start(f32[2,768]{1,0:T(2,128)S(1)} %collective-permute-done.8), channel_id=1, source_target_pairs={{0,1},{1,0},{2,3},{3,2},{4,5},{5,4},{6,7},{7,6},{8,9},{9,8},{10,11... | collective-permute-start | bytes 18440 | tf_op jit(solution)/shard_map/ppermute | solution.py:49
  18.4 3.2 %collective-permute-start.6 = (f32[2,2,768]{2,1,0:T(2,128)S(1)}, f32[2,2,768]{2,1,0:T(2,128)S(1)}, u32[]{:S(2)}, u32[]{:S(2)}) collective-permute-start(f32[2,2,768]{2,1,0:T(2,128)S(1)} %pad_maximum_fusion.3), channel_id=1, source_target_pairs={{0,3},{1,2},{2,1},{3,0},{4,7},{5,6},{6,5},{7,4},{8,11},{9,10},{10,... | collective-permute-start | bytes 36872 | tf_op jit(solution)/shard_map/ppermute | solution.py:31
  18.5 4.1 %collective-permute-start.7 = (f32[2,2,768]{2,1,0:T(2,128)S(1)}, f32[2,2,768]{2,1,0:T(2,128)S(1)}, u32[]{:S(2)}, u32[]{:S(2)}) collective-permute-start(f32[2,2,768]{2,1,0:T(2,128)S(1)} %pad_maximum_fusion.4), channel_id=1, source_target_pairs={{0,5},{1,4},{2,7},{3,6},{4,1},{5,0},{6,3},{7,2},{8,13},{9,12},{10,... | collective-permute-start | bytes 36872 | tf_op jit(solution)/shard_map/ppermute | solution.py:31
  23.3 4.7 %collective-permute-start.11 = (f32[2,1536]{1,0:T(2,128)S(1)}, f32[2,1536]{1,0:T(2,128)S(1)}, u32[]{:S(2)}, u32[]{:S(2)}) collective-permute-start(f32[2,1536]{1,0:T(2,128)S(1)} %get-tuple-element.36.refs_0_), channel_id=1, source_target_pairs={{0,4},{1,7},{2,6},{3,5},{4,0},{5,3},{6,2},{7,1},{8,12},{9,15},{10,... | collective-permute-start | bytes 36872 | tf_op jit(solution)/shard_map/ppermute | solution.py:41
  25.2 3.7 %collective-permute-start.12 = (f32[2,1536]{1,0:T(2,128)S(1)}, f32[2,1536]{1,0:T(2,128)S(1)}, u32[]{:S(2)}, u32[]{:S(2)}) collective-permute-start(f32[2,1536]{1,0:T(2,128)S(1)} %get-tuple-element.36.refs_0_), channel_id=1, source_target_pairs={{0,2},{1,3},{2,0},{3,1},{4,6},{5,7},{6,4},{7,5},{8,10},{9,11},{10,... | collective-permute-start | bytes 36872 | tf_op jit(solution)/shard_map/ppermute | solution.py:41
  28.0 1.2 %collective-permute-start.13 = (f32[2,1536]{1,0:T(2,128)S(1)}, f32[2,1536]{1,0:T(2,128)S(1)}, u32[]{:S(2)}, u32[]{:S(2)}) collective-permute-start(f32[2,1536]{1,0:T(2,128)S(1)} %collective-permute-done.11.refs_1_), channel_id=1, source_target_pairs={{0,1},{1,0},{2,3},{3,2},{4,5},{5,4},{6,7},{7,6},{8,9},{9,8},{10,11... | collective-permute-start | bytes 36872 | tf_op jit(solution)/shard_map/ppermute | solution.py:49
  29.5 4.6 %collective-permute-start.16 = (bf16[8,512]{1,0:T(8,128)(2,1)S(1)}, bf16[8,512]{1,0:T(8,128)(2,1)S(1)}, u32[]{:S(2)}, u32[]{:S(2)}) collective-permute-start(bf16[8,512]{1,0:T(8,128)(2,1)S(1)} %get-tuple-element.38.refs_0_), channel_id=1, source_target_pairs={{0,4},{1,7},{2,6},{3,5},{4,0},{5,3},{6,2},{7,1},{8,12},{9,15},{10,... | collective-permute-start | bytes 24584 | tf_op jit(solution)/shard_map/ppermute | solution.py:41
  31.3 3.7 %collective-permute-start.15 = (bf16[8,512]{1,0:T(8,128)(2,1)S(1)}, bf16[8,512]{1,0:T(8,128)(2,1)S(1)}, u32[]{:S(2)}, u32[]{:S(2)}) collective-permute-start(bf16[8,512]{1,0:T(8,128)(2,1)S(1)} %get-tuple-element.38.refs_0_), channel_id=1, source_target_pairs={{0,2},{1,3},{2,0},{3,1},{4,6},{5,7},{6,4},{7,5},{8,10},{9,11},{10,... | collective-permute-start | bytes 24584 | tf_op jit(solution)/shard_map/ppermute | solution.py:41
  34.0 1.2 %collective-permute-start.17 = (bf16[8,512]{1,0:T(8,128)(2,1)S(1)}, bf16[8,512]{1,0:T(8,128)(2,1)S(1)}, u32[]{:S(2)}, u32[]{:S(2)}) collective-permute-start(bf16[8,512]{1,0:T(8,128)(2,1)S(1)} %collective-permute-done.16.refs_0_), channel_id=1, source_target_pairs={{0,1},{1,0},{2,3},{3,2},{4,5},{5,4},{6,7},{7,6},{8,9},{9,8},{10,11... | collective-permute-start | bytes 24584 | tf_op jit(solution)/shard_map/ppermute | solution.py:49
  36.1 5.4 %collective-permute-start.18 = (bf16[3,8,256]{2,1,0:T(8,128)(2,1)S(1)}, bf16[3,8,256]{2,1,0:T(8,128)(2,1)S(1)}, u32[]{:S(2)}, u32[]{:S(2)}) collective-permute-start(bf16[3,8,256]{2,1,0:T(8,128)(2,1)S(1)} %get-tuple-element.44), channel_id=1, source_target_pairs={{0,1},{1,0},{2,3},{3,2},{4,5},{5,4},{6,7},{7,6},{8,9},{9,8},{10,11... | collective-permute-start | bytes 36872 | tf_op jit(solution)/shard_map/ppermute | solution.py:49
  36.2 4.9 %collective-permute-start.19 = (bf16[8,512]{1,0:T(8,128)(2,1)S(1)}, bf16[8,512]{1,0:T(8,128)(2,1)S(1)}, u32[]{:S(2)}, u32[]{:S(2)}) collective-permute-start(bf16[8,512]{1,0:T(8,128)(2,1)S(1)} %get-tuple-element.45), channel_id=1, source_target_pairs={{0,7},{1,6},{2,5},{3,4},{4,3},{5,2},{6,1},{7,0},{8,15},{9,14},{10,... | collective-permute-start | bytes 24584 | tf_op jit(solution)/shard_map/ppermute | solution.py:31
  41.1 4.5 %collective-permute-start.20 = (bf16[8,512]{1,0:T(8,128)(2,1)S(1)}, bf16[8,512]{1,0:T(8,128)(2,1)S(1)}, u32[]{:S(2)}, u32[]{:S(2)}) collective-permute-start(bf16[8,512]{1,0:T(8,128)(2,1)S(1)} %collective-permute-done.19.farthest), channel_id=1, source_target_pairs={{0,1},{1,0},{2,3},{3,2},{4,5},{5,4},{6,7},{7,6},{8,9},{9,8},{10,11... | collective-permute-start | bytes 24584 | tf_op jit(solution)/shard_map/ppermute | solution.py:49
  41.6 3.9 %collective-permute-start.22 = (bf16[8,256]{1,0:T(8,128)(2,1)S(1)}, bf16[8,256]{1,0:T(8,128)(2,1)S(1)}, u32[]{:S(2)}, u32[]{:S(2)}) collective-permute-start(bf16[8,256]{1,0:T(8,128)(2,1)S(1)} %shard_map.180), channel_id=1, source_target_pairs={{0,5},{1,4},{2,7},{3,6},{4,1},{5,0},{6,3},{7,2},{8,13},{9,12},{10,... | collective-permute-start | bytes 12296 | tf_op jit(solution)/shard_map/ppermute | solution.py:31
  41.8 3.8 %collective-permute-start.21 = (bf16[8,256]{1,0:T(8,128)(2,1)S(1)}, bf16[8,256]{1,0:T(8,128)(2,1)S(1)}, u32[]{:S(2)}, u32[]{:S(2)}) collective-permute-start(bf16[8,256]{1,0:T(8,128)(2,1)S(1)} %shard_map.179), channel_id=1, source_target_pairs={{0,3},{1,2},{2,1},{3,0},{4,7},{5,6},{6,5},{7,4},{8,11},{9,10},{10,... | collective-permute-start | bytes 12296 | tf_op jit(solution)/shard_map/ppermute | solution.py:31
  (15 other events, 80.3 us)

commit v6 on v5

--- a/solution.py
+++ b/solution.py
@@ -306,11 +306,12 @@
                 parts[t, h : h + 1, :] = pair[:, i * size : (i + 1) * size]
     query, key, value, gate = parts[0], parts[1], parts[2], parts[3]
     shrink = lax.rsqrt(jnp.sum(key * key, axis=1, keepdims=True) + epsilon)
+    pair_of = lambda h: terms[h] if terms.dtype == jnp.bfloat16 else two_terms(terms[h])
     padded = -(-heads // 16) * 16
     pad = [jnp.zeros((padded - heads, size), jnp.float32)] if padded > heads else []
     left = jnp.concatenate([key, *pad, query, *pad], axis=0).astype(jnp.bfloat16)
     at = lax.rem(lax.broadcasted_iota(jnp.int32, (2 * padded, 2 * size), 0), padded)
-    found = sum(jnp.where(at == h, dot(left, terms[h]), 0.0) for h in range(heads))
+    found = sum(jnp.where(at == h, dot(left, pair_of(h)), 0.0) for h in range(heads))
     found = found[:, :size] + found[:, size:]
     recall, read = found[:heads] * shrink, found[padded : padded + heads]
     write = shrink * strength[...] * (value - retain[...] * recall)
@@ -336,6 +337,12 @@
             mixed[c : c + 1, h * size : (h + 1) * size] = ordered[c][h : h + 1]
     key_ref[...] = rows[0][1]
     write_ref[...] = rows[0][2]
+
+
+def two_terms(matrix):
+    high = matrix.astype(jnp.bfloat16)
+    low = (matrix - high.astype(jnp.float32)).astype(jnp.bfloat16)
+    return jnp.concatenate([high, low], axis=1)
 
 
 def split_memory(memory, terms):
@@ -491,11 +498,10 @@
     shape = ((heads, size, 2 * size), bf16)
     (terms,) = call(split_memory, [shape], [matrix], work=5e8)
     moved = near(matrix)
-    (partner_terms,) = call(split_memory, [shape], [moved], work=5e8)
     mixed, key, write = call(
         functools.partial(read_memory, chips),
         [((2, heads * size), f32), ((heads, size), f32), ((heads, size), f32)],
-        [mine, other, strength, retain, terms, partner_strength, partner_retain, partner_terms]
+        [mine, other, strength, retain, terms, partner_strength, partner_retain, moved]
         + [head_gain.reshape(1, size)],
         [pltpu.VMEM((2, 4, heads, size), f32)],
     )

time: 46.4 us -> 45.1 us (0.972)
  waiting for transfers between devices: 18.1 us -> 16.6 us
    ppermute x9, waiting for transfers between devices: 11.7 us -> 10.3 us  [far(): got.append(lax.ppermute(pieces[d], axes, pairs))]
    pallas_call x16 -> x15, Pallas kernels: 6.34 us -> 6.21 us  [call(): pl.pallas_call(body, out_shape=[jax.ShapeDtypeStruct(shape, kind) for sha...]
  transfers between devices with their start and end apart: 23 -> 23, of which waited for: 14 -> 15; matrix products, arithmetic and copies ran while one was open for 0% -> 0% of each run, Pallas kernels for 10% -> 10%
where the time goes in v6:
time: 45.1 us; the launch traced here: 44.9 us
  starting transfers between devices  20.1 us (45%)
  waiting for transfers between devices  16.6 us (37%)
  Pallas kernels  6.21 us (14%)
  local copies, waits for them, and re-layouts  1.07 us (2%)
  between operations  0.86 us (2%)
    ppermute x9, starting transfers between devices, far(): got.append(lax.ppermute(pieces[d], axes, pairs))  12.2 us
    ppermute x9, waiting for transfers between devices, far(): got.append(lax.ppermute(pieces[d], axes, pairs))  10.3 us
    pallas_call x15, Pallas kernels, call(): pl.pallas_call(body, out_shape=[jax.ShapeDtypeStruct(shape, kind) for sha...  6.21 us
    ppermute x4, waiting for transfers between devices, shared(): got = lax.ppermute(piece, axes, pairs)  5.83 us
    ppermute x4, starting transfers between devices, shared(): got = lax.ppermute(piece, axes, pairs)  4.84 us
    ppermute x10, starting transfers between devices, near(): return lax.ppermute(value, 'tp', [(0, 1), (1, 0)])  3.03 us
    unnamed x32, local copies, waits for them, and re-layouts  1.05 us
  transfers between devices with their start and end apart: 23, of which 15 were waited for; matrix products, arithmetic and copies ran while one was open for 0% of the time, Pallas kernels for 10%

profile of v6, /device:TPU:0, one launch (start us, length us, event | category | flops | bytes accessed | tf_op | source)
XLA Modules:
  0.0 44.9 jit_solution(17453989099464563390)
XLA Ops:
  0.6 2.6 %collective-permute-start.1 = (bf16[8,256]{1,0:T(8,128)(2,1)}, bf16[8,256]{1,0:T(8,128)(2,1)S(1)}, u32[]{:S(2)}, u32[]{:S(2)}) collective-permute-start(bf16[8,256]{1,0:T(8,128)(2,1)} %tokens.1), channel_id=1, source_target_pairs={{0,3},{1,2},{2,1},{3,0},{4,7},{5,6},{6,5},{7,4},{8,11},{9,10},{10,... | collective-permute-start | bytes 12296 | tf_op jit(solution)/shard_map/ppermute | solution.py:31
  3.2 0.7 %collective-permute-start = (bf16[8,256]{1,0:T(8,128)(2,1)}, bf16[8,256]{1,0:T(8,128)(2,1)S(1)}, u32[]{:S(2)}, u32[]{:S(2)}) collective-permute-start(bf16[8,256]{1,0:T(8,128)(2,1)} %tokens.1), channel_id=1, source_target_pairs={{0,1},{1,0},{2,3},{3,2},{4,5},{5,4},{6,7},{7,6},{8,9},{9,8},{10,11... | collective-permute-start | bytes 12296 | tf_op jit(solution)/shard_map/ppermute | solution.py:49
  3.9 2.1 %collective-permute-start.3 = (bf16[8,256]{1,0:T(8,128)(2,1)}, bf16[8,256]{1,0:T(8,128)(2,1)S(1)}, u32[]{:S(2)}, u32[]{:S(2)}) collective-permute-start(bf16[8,256]{1,0:T(8,128)(2,1)} %tokens.1), channel_id=1, source_target_pairs={{0,7},{1,6},{2,5},{3,4},{4,3},{5,2},{6,1},{7,0},{8,15},{9,14},{10,... | collective-permute-start | bytes 12296 | tf_op jit(solution)/shard_map/ppermute | solution.py:31
  6.7 1.0 %copy-done.12 = bf16[8,256]{1,0:T(8,128)(2,1)S(1)} copy-done((bf16[8,256]{1,0:T(8,128)(2,1)S(1)}, bf16[8,256]{1,0:T(8,128)(2,1)}, u32[]{:S(2)}) %copy-start.12) | copy-done | bytes 4120
  8.0 0.9 %collective-permute-done.3.refs_2_ = bf16[8,256]{1,0:T(8,128)(2,1)S(1)} collective-permute-done((bf16[8,256]{1,0:T(8,128)(2,1)}, bf16[8,256]{1,0:T(8,128)(2,1)S(1)}, u32[]{:S(2)}, u32[]{:S(2)}) %collective-permute-start.3) | collective-permute-done | bytes 4128 | tf_op jit(solution)/shard_map/ppermute | solution.py:31
  8.9 1.2 %collective-permute-done.2.refs_1_ = bf16[8,256]{1,0:T(8,128)(2,1)S(1)} collective-permute-done((bf16[8,256]{1,0:T(8,128)(2,1)}, bf16[8,256]{1,0:T(8,128)(2,1)S(1)}, u32[]{:S(2)}, u32[]{:S(2)}) %collective-permute-start.2) | collective-permute-done | bytes 4128 | tf_op jit(solution)/shard_map/ppermute | solution.py:31
  12.3 1.2 %collective-permute-start.8 = (f32[2,768]{1,0:T(2,128)S(1)}, f32[2,768]{1,0:T(2,128)S(1)}, u32[]{:S(2)}, u32[]{:S(2)}) collective-permute-start(f32[2,768]{1,0:T(2,128)S(1)} %get-tuple-element.29), channel_id=1, source_target_pairs={{0,7},{1,6},{2,5},{3,4},{4,3},{5,2},{6,1},{7,0},{8,15},{9,14},{10,... | collective-permute-start | bytes 18440 | tf_op jit(solution)/shard_map/ppermute | solution.py:31
  14.0 3.2 %collective-permute-done.8 = f32[2,768]{1,0:T(2,128)S(1)} collective-permute-done((f32[2,768]{1,0:T(2,128)S(1)}, f32[2,768]{1,0:T(2,128)S(1)}, u32[]{:S(2)}, u32[]{:S(2)}) %collective-permute-start.8) | collective-permute-done | bytes 6176 | tf_op jit(solution)/shard_map/ppermute | solution.py:31
  17.5 1.7 %collective-permute-start.7 = (f32[2,2,768]{2,1,0:T(2,128)S(1)}, f32[2,2,768]{2,1,0:T(2,128)S(1)}, u32[]{:S(2)}, u32[]{:S(2)}) collective-permute-start(f32[2,2,768]{2,1,0:T(2,128)S(1)} %pad_maximum_fusion.4), channel_id=1, source_target_pairs={{0,5},{1,4},{2,7},{3,6},{4,1},{5,0},{6,3},{7,2},{8,13},{9,12},{10,... | collective-permute-start | bytes 36872 | tf_op jit(solution)/shard_map/ppermute | solution.py:31
  19.2 1.4 %collective-permute-done.6 = f32[2,2,768]{2,1,0:T(2,128)S(1)} collective-permute-done((f32[2,2,768]{2,1,0:T(2,128)S(1)}, f32[2,2,768]{2,1,0:T(2,128)S(1)}, u32[]{:S(2)}, u32[]{:S(2)}) %collective-permute-start.6) | collective-permute-done | bytes 12320 | tf_op jit(solution)/shard_map/ppermute | solution.py:31
  20.6 1.0 %collective-permute-done.7 = f32[2,2,768]{2,1,0:T(2,128)S(1)} collective-permute-done((f32[2,2,768]{2,1,0:T(2,128)S(1)}, f32[2,2,768]{2,1,0:T(2,128)S(1)}, u32[]{:S(2)}, u32[]{:S(2)}) %collective-permute-start.7) | collective-permute-done | bytes 12320 | tf_op jit(solution)/shard_map/ppermute | solution.py:31
  22.2 2.0 %collective-permute-start.11 = (f32[2,1536]{1,0:T(2,128)S(1)}, f32[2,1536]{1,0:T(2,128)S(1)}, u32[]{:S(2)}, u32[]{:S(2)}) collective-permute-start(f32[2,1536]{1,0:T(2,128)S(1)} %get-tuple-element.36.refs_0_), channel_id=1, source_target_pairs={{0,4},{1,7},{2,6},{3,5},{4,0},{5,3},{6,2},{7,1},{8,12},{9,15},{10,... | collective-permute-start | bytes 36872 | tf_op jit(solution)/shard_map/ppermute | solution.py:41
  24.2 2.6 %collective-permute-done.11.refs_1_ = f32[2,1536]{1,0:T(2,128)S(1)} collective-permute-done((f32[2,1536]{1,0:T(2,128)S(1)}, f32[2,1536]{1,0:T(2,128)S(1)}, u32[]{:S(2)}, u32[]{:S(2)}) %collective-permute-start.11) | collective-permute-done | bytes 12320 | tf_op jit(solution)/shard_map/ppermute | solution.py:41
  26.9 0.9 %collective-permute-done.12.refs_2_ = f32[2,1536]{1,0:T(2,128)S(1)} collective-permute-done((f32[2,1536]{1,0:T(2,128)S(1)}, f32[2,1536]{1,0:T(2,128)S(1)}, u32[]{:S(2)}, u32[]{:S(2)}) %collective-permute-start.12) | collective-permute-done | bytes 12320 | tf_op jit(solution)/shard_map/ppermute | solution.py:41
  28.3 1.9 %collective-permute-start.16 = (bf16[8,512]{1,0:T(8,128)(2,1)S(1)}, bf16[8,512]{1,0:T(8,128)(2,1)S(1)}, u32[]{:S(2)}, u32[]{:S(2)}) collective-permute-start(bf16[8,512]{1,0:T(8,128)(2,1)S(1)} %get-tuple-element.38.refs_0_), channel_id=1, source_target_pairs={{0,4},{1,7},{2,6},{3,5},{4,0},{5,3},{6,2},{7,1},{8,12},{9,15},{10,... | collective-permute-start | bytes 24584 | tf_op jit(solution)/shard_map/ppermute | solution.py:41
  30.2 0.8 %collective-permute-start.15 = (bf16[8,512]{1,0:T(8,128)(2,1)S(1)}, bf16[8,512]{1,0:T(8,128)(2,1)S(1)}, u32[]{:S(2)}, u32[]{:S(2)}) collective-permute-start(bf16[8,512]{1,0:T(8,128)(2,1)S(1)} %get-tuple-element.38.refs_0_), channel_id=1, source_target_pairs={{0,2},{1,3},{2,0},{3,1},{4,6},{5,7},{6,4},{7,5},{8,10},{9,11},{10,... | collective-permute-start | bytes 24584 | tf_op jit(solution)/shard_map/ppermute | solution.py:41
  31.3 1.6 %collective-permute-done.16.refs_0_ = bf16[8,512]{1,0:T(8,128)(2,1)S(1)} collective-permute-done((bf16[8,512]{1,0:T(8,128)(2,1)S(1)}, bf16[8,512]{1,0:T(8,128)(2,1)S(1)}, u32[]{:S(2)}, u32[]{:S(2)}) %collective-permute-start.16) | collective-permute-done | bytes 8224 | tf_op jit(solution)/shard_map/ppermute | solution.py:41
  33.1 0.8 %collective-permute-done.15.refs_0_ = bf16[8,512]{1,0:T(8,128)(2,1)S(1)} collective-permute-done((bf16[8,512]{1,0:T(8,128)(2,1)S(1)}, bf16[8,512]{1,0:T(8,128)(2,1)S(1)}, u32[]{:S(2)}, u32[]{:S(2)}) %collective-permute-start.15) | collective-permute-done | bytes 8224 | tf_op jit(solution)/shard_map/ppermute | solution.py:41
  34.0 0.8 %shard_map.176 = (bf16[8,1024]{1,0:T(8,128)(2,1)S(1)}, bf16[3,8,256]{2,1,0:T(8,128)(2,1)S(1)}, bf16[8,512]{1,0:T(8,128)(2,1)S(1)}) custom-call(bf16[8,512]{1,0:T(8,128)(2,1)S(1)} %collective-permute-done.15.refs_0_, bf16[8,512]{1,0:T(8,128)(2,1)S(1)} %collective-permute-done.17.refs_1_, f32[8,1024]{1,0:T(8,128)S(1)} %get-tuple-element.39.refs_2_, ...), custom_call_target="tpu_custom_call" | custom-call | flops 1000000000 | tf_op jit(solution)/shard_map/pallas_call | solution.py:206
  34.9 2.0 %collective-permute-start.19 = (bf16[8,512]{1,0:T(8,128)(2,1)S(1)}, bf16[8,512]{1,0:T(8,128)(2,1)S(1)}, u32[]{:S(2)}, u32[]{:S(2)}) collective-permute-start(bf16[8,512]{1,0:T(8,128)(2,1)S(1)} %get-tuple-element.45), channel_id=1, source_target_pairs={{0,7},{1,6},{2,5},{3,4},{4,3},{5,2},{6,1},{7,0},{8,15},{9,14},{10,... | collective-permute-start | bytes 24584 | tf_op jit(solution)/shard_map/ppermute | solution.py:31
  37.2 1.3 %shard_map.181 = f32[12,128,128]{2,1,0:T(8,128)} custom-call(f32[12,128,128]{2,1,0:T(8,128)S(1)} %bitcast.34, f32[12,128]{1,0:T(8,128)S(1)} %get-tuple-element.46.key, f32[12,128]{1,0:T(8,128)S(1)} %get-tuple-element.47.write, f32[12,128]{1,0:T(8,128)S(1)} %get-tuple-element.33.refs_1_.retain), custom_call_target="tpu_custom_call" | custom-call | flops 500000000 | tf_op jit(solution)/shard_map/pallas_call | solution.py:206
  38.5 1.3 %collective-permute-done.19.farthest = bf16[8,512]{1,0:T(8,128)(2,1)S(1)} collective-permute-done((bf16[8,512]{1,0:T(8,128)(2,1)S(1)}, bf16[8,512]{1,0:T(8,128)(2,1)S(1)}, u32[]{:S(2)}, u32[]{:S(2)}) %collective-permute-start.19) | collective-permute-done | bytes 8224 | tf_op jit(solution)/shard_map/ppermute | solution.py:31
  40.4 2.4 %collective-permute-start.22 = (bf16[8,256]{1,0:T(8,128)(2,1)S(1)}, bf16[8,256]{1,0:T(8,128)(2,1)S(1)}, u32[]{:S(2)}, u32[]{:S(2)}) collective-permute-start(bf16[8,256]{1,0:T(8,128)(2,1)S(1)} %shard_map.179), channel_id=1, source_target_pairs={{0,5},{1,4},{2,7},{3,6},{4,1},{5,0},{6,3},{7,2},{8,13},{9,12},{10,... | collective-permute-start | bytes 12296 | tf_op jit(solution)/shard_map/ppermute | solution.py:31
  43.2 1.1 %collective-permute-done.22.refs_1_ = bf16[8,256]{1,0:T(8,128)(2,1)S(1)} collective-permute-done((bf16[8,256]{1,0:T(8,128)(2,1)S(1)}, bf16[8,256]{1,0:T(8,128)(2,1)S(1)}, u32[]{:S(2)}, u32[]{:S(2)}) %collective-permute-start.22) | collective-permute-done | bytes 4128 | tf_op jit(solution)/shard_map/ppermute | solution.py:31
  (78 shorter events, 7.5 us)
Async XLA Ops:
  0.6 7.2 %collective-permute-start.1 = (bf16[8,256]{1,0:T(8,128)(2,1)}, bf16[8,256]{1,0:T(8,128)(2,1)S(1)}, u32[]{:S(2)}, u32[]{:S(2)}) collective-permute-start(bf16[8,256]{1,0:T(8,128)(2,1)} %tokens.1), channel_id=1, source_target_pairs={{0,3},{1,2},{2,1},{3,0},{4,7},{5,6},{6,5},{7,4},{8,11},{9,10},{10,... | collective-permute-start | bytes 12296 | tf_op jit(solution)/shard_map/ppermute | solution.py:31
  3.2 7.4 %collective-permute-start = (bf16[8,256]{1,0:T(8,128)(2,1)}, bf16[8,256]{1,0:T(8,128)(2,1)S(1)}, u32[]{:S(2)}, u32[]{:S(2)}) collective-permute-start(bf16[8,256]{1,0:T(8,128)(2,1)} %tokens.1), channel_id=1, source_target_pairs={{0,1},{1,0},{2,3},{3,2},{4,5},{5,4},{6,7},{7,6},{8,9},{9,8},{10,11... | collective-permute-start | bytes 12296 | tf_op jit(solution)/shard_map/ppermute | solution.py:49
  3.9 5.0 %collective-permute-start.3 = (bf16[8,256]{1,0:T(8,128)(2,1)}, bf16[8,256]{1,0:T(8,128)(2,1)S(1)}, u32[]{:S(2)}, u32[]{:S(2)}) collective-permute-start(bf16[8,256]{1,0:T(8,128)(2,1)} %tokens.1), channel_id=1, source_target_pairs={{0,7},{1,6},{2,5},{3,4},{4,3},{5,2},{6,1},{7,0},{8,15},{9,14},{10,... | collective-permute-start | bytes 12296 | tf_op jit(solution)/shard_map/ppermute | solution.py:31
  6.0 4.1 %collective-permute-start.2 = (bf16[8,256]{1,0:T(8,128)(2,1)}, bf16[8,256]{1,0:T(8,128)(2,1)S(1)}, u32[]{:S(2)}, u32[]{:S(2)}) collective-permute-start(bf16[8,256]{1,0:T(8,128)(2,1)} %tokens.1), channel_id=1, source_target_pairs={{0,5},{1,4},{2,7},{3,6},{4,1},{5,0},{6,3},{7,2},{8,13},{9,12},{10,... | collective-permute-start | bytes 12296 | tf_op jit(solution)/shard_map/ppermute | solution.py:31
  6.1 15.5 %collective-permute-start.10 = (f32[12,128,128]{2,1,0:T(8,128)}, f32[12,128,128]{2,1,0:T(8,128)S(1)}, u32[]{:S(2)}, u32[]{:S(2)}) collective-permute-start(f32[12,128,128]{2,1,0:T(8,128)} %bitcast.32), channel_id=1, source_target_pairs={{0,1},{1,0},{2,3},{3,2},{4,5},{5,4},{6,7},{7,6},{8,9},{9,8},{10,11... | collective-permute-start | bytes 2359304 | tf_op jit(solution)/shard_map/ppermute | solution.py:49
  7.9 19.0 %collective-permute-start.14 = (bf16[1536,256]{1,0:T(8,128)(2,1)S(1)}, bf16[1536,256]{1,0:T(8,128)(2,1)S(1)}, u32[]{:S(2)}, u32[]{:S(2)}) collective-permute-start(bf16[1536,256]{1,0:T(8,128)(2,1)S(1)} %copy-done.7), channel_id=1, source_target_pairs={{0,1},{1,0},{2,3},{3,2},{4,5},{5,4},{6,7},{7,6},{8,9},{9,8},{10,11... | collective-permute-start | bytes 2359304 | tf_op jit(solution)/shard_map/ppermute | solution.py:49
  10.1 1.3 %collective-permute-start.4 = (bf16[3,8,256]{2,1,0:T(8,128)(2,1)S(1)}, bf16[3,8,256]{2,1,0:T(8,128)(2,1)S(1)}, u32[]{:S(2)}, u32[]{:S(2)}) collective-permute-start(bf16[3,8,256]{2,1,0:T(8,128)(2,1)S(1)} %pad_maximum_fusion.2), channel_id=1, source_target_pairs={{0,1},{1,0},{2,3},{3,2},{4,5},{5,4},{6,7},{7,6},{8,9},{9,8},{10,11... | collective-permute-start | bytes 36872 | tf_op jit(solution)/shard_map/ppermute | solution.py:49
  11.9 5.4 %collective-permute-start.5 = (f32[3,2,768]{2,1,0:T(2,128)S(1)}, f32[3,2,768]{2,1,0:T(2,128)S(1)}, u32[]{:S(2)}, u32[]{:S(2)}) collective-permute-start(f32[3,2,768]{2,1,0:T(2,128)S(1)} %get-tuple-element.28), channel_id=1, source_target_pairs={{0,1},{1,0},{2,3},{3,2},{4,5},{5,4},{6,7},{7,6},{8,9},{9,8},{10,11... | collective-permute-start | bytes 55304 | tf_op jit(solution)/shard_map/ppermute | solution.py:49
  12.3 4.9 %collective-permute-start.8 = (f32[2,768]{1,0:T(2,128)S(1)}, f32[2,768]{1,0:T(2,128)S(1)}, u32[]{:S(2)}, u32[]{:S(2)}) collective-permute-start(f32[2,768]{1,0:T(2,128)S(1)} %get-tuple-element.29), channel_id=1, source_target_pairs={{0,7},{1,6},{2,5},{3,4},{4,3},{5,2},{6,1},{7,0},{8,15},{9,14},{10,... | collective-permute-start | bytes 18440 | tf_op jit(solution)/shard_map/ppermute | solution.py:31
  13.9 17.1 %copy-start.1 = (bf16[2048,1024]{1,0:T(8,128)(2,1)S(1)}, bf16[2048,1024]{1,0:T(8,128)(2,1)}, u32[]{:S(2)}) copy-start(bf16[2048,1024]{1,0:T(8,128)(2,1)} %refs_7_.1) | copy-start | bytes 12582916
  17.2 4.4 %collective-permute-start.9 = (f32[2,768]{1,0:T(2,128)S(1)}, f32[2,768]{1,0:T(2,128)S(1)}, u32[]{:S(2)}, u32[]{:S(2)}) collective-permute-start(f32[2,768]{1,0:T(2,128)S(1)} %collective-permute-done.8), channel_id=1, source_target_pairs={{0,1},{1,0},{2,3},{3,2},{4,5},{5,4},{6,7},{7,6},{8,9},{9,8},{10,11... | collective-permute-start | bytes 18440 | tf_op jit(solution)/shard_map/ppermute | solution.py:49
  17.4 3.2 %collective-permute-start.6 = (f32[2,2,768]{2,1,0:T(2,128)S(1)}, f32[2,2,768]{2,1,0:T(2,128)S(1)}, u32[]{:S(2)}, u32[]{:S(2)}) collective-permute-start(f32[2,2,768]{2,1,0:T(2,128)S(1)} %pad_maximum_fusion.3), channel_id=1, source_target_pairs={{0,3},{1,2},{2,1},{3,0},{4,7},{5,6},{6,5},{7,4},{8,11},{9,10},{10,... | collective-permute-start | bytes 36872 | tf_op jit(solution)/shard_map/ppermute | solution.py:31
  17.5 4.1 %collective-permute-start.7 = (f32[2,2,768]{2,1,0:T(2,128)S(1)}, f32[2,2,768]{2,1,0:T(2,128)S(1)}, u32[]{:S(2)}, u32[]{:S(2)}) collective-permute-start(f32[2,2,768]{2,1,0:T(2,128)S(1)} %pad_maximum_fusion.4), channel_id=1, source_target_pairs={{0,5},{1,4},{2,7},{3,6},{4,1},{5,0},{6,3},{7,2},{8,13},{9,12},{10,... | collective-permute-start | bytes 36872 | tf_op jit(solution)/shard_map/ppermute | solution.py:31
  22.2 4.7 %collective-permute-start.11 = (f32[2,1536]{1,0:T(2,128)S(1)}, f32[2,1536]{1,0:T(2,128)S(1)}, u32[]{:S(2)}, u32[]{:S(2)}) collective-permute-start(f32[2,1536]{1,0:T(2,128)S(1)} %get-tuple-element.36.refs_0_), channel_id=1, source_target_pairs={{0,4},{1,7},{2,6},{3,5},{4,0},{5,3},{6,2},{7,1},{8,12},{9,15},{10,... | collective-permute-start | bytes 36872 | tf_op jit(solution)/shard_map/ppermute | solution.py:41
  24.1 3.7 %collective-permute-start.12 = (f32[2,1536]{1,0:T(2,128)S(1)}, f32[2,1536]{1,0:T(2,128)S(1)}, u32[]{:S(2)}, u32[]{:S(2)}) collective-permute-start(f32[2,1536]{1,0:T(2,128)S(1)} %get-tuple-element.36.refs_0_), channel_id=1, source_target_pairs={{0,2},{1,3},{2,0},{3,1},{4,6},{5,7},{6,4},{7,5},{8,10},{9,11},{10,... | collective-permute-start | bytes 36872 | tf_op jit(solution)/shard_map/ppermute | solution.py:41
  26.8 1.2 %collective-permute-start.13 = (f32[2,1536]{1,0:T(2,128)S(1)}, f32[2,1536]{1,0:T(2,128)S(1)}, u32[]{:S(2)}, u32[]{:S(2)}) collective-permute-start(f32[2,1536]{1,0:T(2,128)S(1)} %collective-permute-done.11.refs_1_), channel_id=1, source_target_pairs={{0,1},{1,0},{2,3},{3,2},{4,5},{5,4},{6,7},{7,6},{8,9},{9,8},{10,11... | collective-permute-start | bytes 36872 | tf_op jit(solution)/shard_map/ppermute | solution.py:49
  28.3 4.6 %collective-permute-start.16 = (bf16[8,512]{1,0:T(8,128)(2,1)S(1)}, bf16[8,512]{1,0:T(8,128)(2,1)S(1)}, u32[]{:S(2)}, u32[]{:S(2)}) collective-permute-start(bf16[8,512]{1,0:T(8,128)(2,1)S(1)} %get-tuple-element.38.refs_0_), channel_id=1, source_target_pairs={{0,4},{1,7},{2,6},{3,5},{4,0},{5,3},{6,2},{7,1},{8,12},{9,15},{10,... | collective-permute-start | bytes 24584 | tf_op jit(solution)/shard_map/ppermute | solution.py:41
  30.2 3.7 %collective-permute-start.15 = (bf16[8,512]{1,0:T(8,128)(2,1)S(1)}, bf16[8,512]{1,0:T(8,128)(2,1)S(1)}, u32[]{:S(2)}, u32[]{:S(2)}) collective-permute-start(bf16[8,512]{1,0:T(8,128)(2,1)S(1)} %get-tuple-element.38.refs_0_), channel_id=1, source_target_pairs={{0,2},{1,3},{2,0},{3,1},{4,6},{5,7},{6,4},{7,5},{8,10},{9,11},{10,... | collective-permute-start | bytes 24584 | tf_op jit(solution)/shard_map/ppermute | solution.py:41
  32.9 1.2 %collective-permute-start.17 = (bf16[8,512]{1,0:T(8,128)(2,1)S(1)}, bf16[8,512]{1,0:T(8,128)(2,1)S(1)}, u32[]{:S(2)}, u32[]{:S(2)}) collective-permute-start(bf16[8,512]{1,0:T(8,128)(2,1)S(1)} %collective-permute-done.16.refs_0_), channel_id=1, source_target_pairs={{0,1},{1,0},{2,3},{3,2},{4,5},{5,4},{6,7},{7,6},{8,9},{9,8},{10,11... | collective-permute-start | bytes 24584 | tf_op jit(solution)/shard_map/ppermute | solution.py:49
  34.9 4.9 %collective-permute-start.19 = (bf16[8,512]{1,0:T(8,128)(2,1)S(1)}, bf16[8,512]{1,0:T(8,128)(2,1)S(1)}, u32[]{:S(2)}, u32[]{:S(2)}) collective-permute-start(bf16[8,512]{1,0:T(8,128)(2,1)S(1)} %get-tuple-element.45), channel_id=1, source_target_pairs={{0,7},{1,6},{2,5},{3,4},{4,3},{5,2},{6,1},{7,0},{8,15},{9,14},{10,... | collective-permute-start | bytes 24584 | tf_op jit(solution)/shard_map/ppermute | solution.py:31
  36.9 3.1 %collective-permute-start.18 = (bf16[3,8,256]{2,1,0:T(8,128)(2,1)S(1)}, bf16[3,8,256]{2,1,0:T(8,128)(2,1)S(1)}, u32[]{:S(2)}, u32[]{:S(2)}) collective-permute-start(bf16[3,8,256]{2,1,0:T(8,128)(2,1)S(1)} %get-tuple-element.44), channel_id=1, source_target_pairs={{0,1},{1,0},{2,3},{3,2},{4,5},{5,4},{6,7},{7,6},{8,9},{9,8},{10,11... | collective-permute-start | bytes 36872 | tf_op jit(solution)/shard_map/ppermute | solution.py:49
  39.8 4.5 %collective-permute-start.20 = (bf16[8,512]{1,0:T(8,128)(2,1)S(1)}, bf16[8,512]{1,0:T(8,128)(2,1)S(1)}, u32[]{:S(2)}, u32[]{:S(2)}) collective-permute-start(bf16[8,512]{1,0:T(8,128)(2,1)S(1)} %collective-permute-done.19.farthest), channel_id=1, source_target_pairs={{0,1},{1,0},{2,3},{3,2},{4,5},{5,4},{6,7},{7,6},{8,9},{9,8},{10,11... | collective-permute-start | bytes 24584 | tf_op jit(solution)/shard_map/ppermute | solution.py:49
  40.1 3.0 %collective-permute-start.21 = (bf16[8,256]{1,0:T(8,128)(2,1)S(1)}, bf16[8,256]{1,0:T(8,128)(2,1)S(1)}, u32[]{:S(2)}, u32[]{:S(2)}) collective-permute-start(bf16[8,256]{1,0:T(8,128)(2,1)S(1)} %shard_map.178), channel_id=1, source_target_pairs={{0,3},{1,2},{2,1},{3,0},{4,7},{5,6},{6,5},{7,4},{8,11},{9,10},{10,... | collective-permute-start | bytes 12296 | tf_op jit(solution)/shard_map/ppermute | solution.py:31
  40.4 3.9 %collective-permute-start.22 = (bf16[8,256]{1,0:T(8,128)(2,1)S(1)}, bf16[8,256]{1,0:T(8,128)(2,1)S(1)}, u32[]{:S(2)}, u32[]{:S(2)}) collective-permute-start(bf16[8,256]{1,0:T(8,128)(2,1)S(1)} %shard_map.179), channel_id=1, source_target_pairs={{0,5},{1,4},{2,7},{3,6},{4,1},{5,0},{6,3},{7,2},{8,13},{9,12},{10,... | collective-permute-start | bytes 12296 | tf_op jit(solution)/shard_map/ppermute | solution.py:31
  (15 other events, 80.5 us)
